TPU v7x, 256 devices: a 4x2x16 block of a 4x16x16 slice. The times are simulated.
256 devices in a mesh: grp: 2 (over y), sp: 16 (over z), tp: 8 (over x, core).
Axes of the slice: x: 4, y: 2, z: 16, core: 2. Of those that a mesh axis runs over, the one named last changes fastest.
The devices are a block of a 4x16x16 slice.
Arguments:
- layer_input: bfloat16 [64, 6144, 2048], P(('grp', 'tp'), 'sp'), parts along dimension 0, may hold values from -6 to 6
- input_gain: float32 [2048], replicated, may hold values from 0.1 to 1.9
- key_weight: bfloat16 [2048, 512], replicated, may hold values from -0.125 to 0.125
- value_weight: bfloat16 [2048, 512], replicated, may hold values from -0.125 to 0.125
- stick_offsets: bfloat16 [4, 64, 6144], P(None, ('grp', 'tp'), 'sp'), parts along dimension 1
- head_bias: float32 [16], replicated
- queries: bfloat16 [16, 16, 512], P(('grp', 'tp'), 'sp'), parts along dimension 0, may hold values from -6 to 6
Outputs:
- key_cache: bfloat16 [16, 16, 6144, 128], P(('grp', 'tp'), 'sp'), parts along dimension 0
- value_cache: bfloat16 [16, 16, 6144, 128], P(('grp', 'tp'), 'sp'), parts along dimension 0
- offset_cache: bfloat16 [16, 16, 6144], P(('grp', 'tp'), 'sp'), parts along dimension 0
- first_read: bfloat16 [16, 16, 512], P(('grp', 'tp'), 'sp'), parts along dimension 0
There are 2 independent parts, one for each index of `grp`. A program takes and returns all parts, laid end to end along the dimension named above; an argument that names none is the same for every part. Nothing has to cross between parts.
All inputs are finite; a program needn't handle non-finite values.
Results may differ from a plain program's by a relative error of at most 0.014.
Values may be sent and summed in bfloat16 or wider, within the bound.
No kernel may reach another device: no remote copies, remote signals or barrier semaphores. Data moves between devices by JAX's collectives and lax.ppermute only.
A program may use at most 64 MiB of HBM per device.

v0:
```python
import math

import jax
import jax.numpy as jnp
from jax import lax
from jax.sharding import PartitionSpec as P

H = 16
KVH = 4
HD = 128


EPSILON = 1e-06


def rms_scale(matrix):
    return matrix * lax.rsqrt(jnp.mean(matrix * matrix, axis=-1, keepdims=True) + EPSILON)


def stick_weights(scores, spread, carried):
    inside = lax.cumsum(spread, axis=scores.ndim - 1, reverse=True) - spread
    return jnp.exp(jax.nn.log_sigmoid(scores) - inside - carried)


def normalize(rows, input_gain):
    return (rms_scale(rows.astype(jnp.float32)) * input_gain).astype(jnp.bfloat16)


def project(normed_rows, weight):
    return jnp.dot(normed_rows, weight, preferred_element_type=jnp.float32).astype(jnp.bfloat16)


def shards(layer_input, input_gain, key_weight, value_weight, stick_offsets, head_bias, queries):
    seq_count, block_len, model_width = layer_input.shape
    sp_count = lax.axis_size("sp")
    group_size = H // KVH
    length = sp_count * block_len
    offset_lookup_matrix = head_bias.reshape(KVH, group_size)
    offset_parts = jnp.transpose(stick_offsets, (1, 0, 2)).reshape(sp_count, block_len)
    head_index = lax.axis_index("sp") % KVH
    normed_rows = normalize(layer_input.reshape(seq_count * block_len, model_width), input_gain)
    key_rows = project(normed_rows, key_weight).reshape(seq_count, block_len, KVH, HD)
    value_rows = project(normed_rows, value_weight).reshape(seq_count, block_len, KVH, HD)
    key_rows, value_rows = (key_rows, value_rows)
    key_parts = jnp.transpose(key_rows, (0, 2, 1, 3)).reshape(sp_count, block_len, HD)
    value_parts = jnp.transpose(value_rows, (0, 2, 1, 3)).reshape(sp_count, block_len, HD)
    key_cache, value_cache, offset_cache = (
        lax.all_to_all(key_parts, "sp", split_axis=0, concat_axis=1, tiled=True),
        lax.all_to_all(value_parts, "sp", split_axis=0, concat_axis=1, tiled=True),
        lax.all_to_all(offset_parts, "sp", split_axis=0, concat_axis=1, tiled=True),
    )
    key_cache = key_cache.reshape(1, 1, length, HD)
    value_cache = value_cache.reshape(1, 1, length, HD)
    offset_cache = offset_cache.reshape(1, 1, length)
    bias_row = lax.dynamic_index_in_dim(offset_lookup_matrix, head_index, 0, keepdims=False)
    own_query = queries.reshape(group_size, HD)
    scores = lax.dot_general(
        own_query,
        key_cache.reshape(length, HD),
        (((1,), (1,)), ((), ())),
        preferred_element_type=jnp.float32,
    )
    scores = (
        scores / math.sqrt(HD)
        + bias_row[:, None]
        + offset_cache.reshape(1, length).astype(jnp.float32)
    )
    spread = jax.nn.softplus(scores)
    weights = stick_weights(scores, spread, 0.0).astype(jnp.bfloat16)
    mixture = jnp.dot(weights, value_cache.reshape(length, HD), preferred_element_type=jnp.float32)
    first_read = rms_scale(mixture).astype(jnp.bfloat16).reshape(1, 1, group_size * HD)
    return (key_cache, value_cache, offset_cache, first_read)


def solution(mesh):
    placed = (
        P(("grp", "tp"), "sp", None),
        P(),
        P(),
        P(),
        P(None, ("grp", "tp"), "sp"),
        P(),
        P(("grp", "tp"), "sp", None),
    )
    return jax.shard_map(
        shards,
        mesh=mesh,
        in_specs=placed,
        out_specs=(
            P(("grp", "tp"), "sp", None, None),
            P(("grp", "tp"), "sp", None, None),
            P(("grp", "tp"), "sp", None),
            P(("grp", "tp"), "sp", None),
        ),
        check_vma=False,
    )
```

profile of v0, /device:TPU:36, one launch (start us, length us, event | category | flops | bytes accessed | tf_op | source)
XLA Modules:
  0.0 223.7 jit_solution(14037182767658850946)
XLA Ops:
  0.6 0.0 copy-start
  0.6 0.9 copy.16
  1.5 0.5 broadcast.51
  2.0 0.7 reduce.4
  2.8 0.7 reshape.127
  3.4 24.0 %all-to-all-start.2 = ((bf16[16,2,192]{2,1,0:T(2,128)(2,1)}), bf16[16,2,192]{2,1,0:T(2,128)(2,1)S(1)}, u32[]{:S(2)}, u32[]{:S(2)}) async-start(bf16[16,2,192]{2,1,0:T(2,128)(2,1)} %reshape.127), calls=%async_computation.2 | async-start | bytes 32768 | tf_op jit(solution)/shard_map/all_to_all | solution.py:50
  27.4 0.0 copy-start.3
  27.4 4.1 %multiply_reduce_fusion = f32[4,384]{1,0:T(4,128)S(1)} fusion(bf16[4,384,2048]{2,1,0:T(8,128)(2,1)} %param.7), kind=kLoop, calls=%fused_computation.3 | loop fusion | flops 9435648 | bytes 6297600 | tf_op jit(solution)/shard_map/reduce_sum | solution.py:17
  31.6 0.0 copy-done.3
  31.6 4.3 %fusion.1 = bf16[1536,2048]{1,0:T(8,128)(2,1)S(1)} fusion(f32[2048]{0:T(1024)S(1)} %copy-done.3, f32[1536]{0:T(1024)S(1)} %rsqrt.20, bf16[4,384,2048]{2,1,0:T(8,128)(2,1)} %param.7), kind=kLoop, calls=%fused_computation.2 | loop fusion | flops 12582912 | bytes 12597248 | tf_op jit(solution)/shard_map/convert_element_type | solution.py:26
  35.8 0.0 copy-start.1
  35.9 2.7 %copy-done.1 = bf16[1536,2048]{1,0:T(8,128)(2,1)} copy-done((bf16[1536,2048]{1,0:T(8,128)(2,1)}, bf16[1536,2048]{1,0:T(8,128)(2,1)S(1)}, u32[]{:S(2)}) %copy-start.1) | copy-done | bytes 6291480
  38.5 0.0 copy-done
  38.5 4.5 %convolution_convert_fusion.1 = bf16[1536,512]{1,0:T(8,128)(2,1)} fusion(bf16[1536,2048]{1,0:T(8,128)(2,1)S(1)} %fusion.1, bf16[2048,512]{1,0:T(8,128)(2,1)S(1)} %copy-done), kind=kOutput, calls=%fused_computation.9 | convolution fusion | flops 3222011904 | bytes 9961472 | tf_op jit(solution)/shard_map/dot_general | solution.py:30
  43.0 3.5 %reshape.111 = bf16[4,384,4,128]{3,2,1,0:T(4,128)(2,1)} reshape(bf16[1536,512]{1,0:T(8,128)(2,1)} %convolution_convert_fusion.1) | data formatting | bytes 3145728 | tf_op jit(solution)/shard_map/reshape | solution.py:42
  46.5 2.9 %copy.14 = bf16[4,384,4,128]{3,1,2,0:T(8,128)(2,1)} copy(bf16[4,384,4,128]{3,2,1,0:T(4,128)(2,1)} %reshape.111) | data formatting | bytes 3145728 | tf_op jit(solution)/shard_map/reshape | solution.py:42
  49.4 0.0 all-to-all-done.2
  49.4 12.0 %all-to-all-start = ((bf16[16,384,128]{2,1,0:T(8,128)(2,1)}), bf16[16,384,128]{2,1,0:T(8,128)(2,1)}, u32[]{:S(2)}, u32[]{:S(2)}) async-start(bf16[16,384,128]{2,1,0:T(8,128)(2,1)} %bitcast.47), calls=%async_computation | async-start | bytes 3145728 | tf_op jit(solution)/shard_map/all_to_all | solution.py:48
  61.4 8.0 %convolution_convert_fusion = bf16[1536,512]{1,0:T(8,128)(2,1)} fusion(bf16[1536,2048]{1,0:T(8,128)(2,1)} %copy-done.1, bf16[2048,512]{1,0:T(8,128)(2,1)} %param.10), kind=kOutput, calls=%fused_computation.8 | convolution fusion | flops 3222011904 | bytes 9961472 | tf_op jit(solution)/shard_map/dot_general | solution.py:30
  69.4 3.5 %reshape.114 = bf16[4,384,4,128]{3,2,1,0:T(4,128)(2,1)} reshape(bf16[1536,512]{1,0:T(8,128)(2,1)} %convolution_convert_fusion) | data formatting | bytes 3145728 | tf_op jit(solution)/shard_map/reshape | solution.py:43
  72.9 2.9 %copy.15 = bf16[4,384,4,128]{3,1,2,0:T(8,128)(2,1)} copy(bf16[4,384,4,128]{3,2,1,0:T(4,128)(2,1)} %reshape.114) | data formatting | bytes 3145728 | tf_op jit(solution)/shard_map/reshape | solution.py:43
  75.8 0.0 copy-start.4
  75.8 0.0 copy-start.5
  75.8 59.2 %all-to-all-done = bf16[16,384,128]{2,1,0:T(8,128)(2,1)} async-done(((bf16[16,384,128]{2,1,0:T(8,128)(2,1)}), bf16[16,384,128]{2,1,0:T(8,128)(2,1)}, u32[]{:S(2)}, u32[]{:S(2)}) %all-to-all-start) | async-done | bytes 1572896 | tf_op jit(solution)/shard_map/all_to_all | solution.py:48
  135.0 6.4 %all-to-all-start.1 = ((bf16[16,384,128]{2,1,0:T(8,128)(2,1)}), bf16[16,384,128]{2,1,0:T(8,128)(2,1)}, u32[]{:S(2)}, u32[]{:S(2)}) async-start(bf16[16,384,128]{2,1,0:T(8,128)(2,1)} %bitcast.46), calls=%async_computation.1 | async-start | bytes 3145728 | tf_op jit(solution)/shard_map/all_to_all | solution.py:49
  141.4 0.0 copy-done.4
  141.4 0.0 copy-done.5
  141.4 0.1 reshape.119
  141.5 0.1 reshape.128
  141.6 0.0 copy-start.2
  141.7 1.9 fusion.4
  143.6 0.1 fusion.12
  143.7 5.0 %reduce-window.6 = f32[4,48,128]{2,1,0:T(8,128)S(1)} reduce-window(f32[4,48,128]{2,1,0:T(8,128)S(1)} %bitcast.48, f32[]{:T(128)} %constant.33.clone.1), window={size=1x1x128 pad=0_0x0_0x0_127}, to_apply=%region_1.2 | reduce-window | flops 3121152 | bytes 196612 | tf_op jit(solution)/shard_map/reduce-window
  148.8 0.1 slice_reduce_fusion
  148.9 0.3 reduce-window.9
  149.2 0.1 slice.7
  149.3 0.1 add_bitcast_fusion
  149.4 66.3 %all-to-all-done.1 = bf16[16,384,128]{2,1,0:T(8,128)(2,1)} async-done(((bf16[16,384,128]{2,1,0:T(8,128)(2,1)}), bf16[16,384,128]{2,1,0:T(8,128)(2,1)}, u32[]{:S(2)}, u32[]{:S(2)}) %all-to-all-start.1) | async-done | bytes 1572896 | tf_op jit(solution)/shard_map/all_to_all | solution.py:49
  215.7 2.0 multiply_reduce_fusion.1
  217.7 0.0 copy-done.2
  217.7 0.1 multiply_convert_fusion
  217.8 0.6 reshape.122
  218.4 2.7 %copy.28 = bf16[1,1,6144,128]{3,2,1,0:T(8,128)(2,1)} copy(bf16[1,1,6144,128]{3,2,1,0:T(8,128)(2,1)} %bitcast.3) | data formatting | bytes 3145728
  221.0 2.7 %copy.29 = bf16[1,1,6144,128]{3,2,1,0:T(8,128)(2,1)} copy(bf16[1,1,6144,128]{3,2,1,0:T(8,128)(2,1)} %bitcast.6) | data formatting | bytes 3145728
  (8 shorter events, 0.1 us)
Async XLA Ops:
  0.6 37.9 %copy-start = (bf16[2048,512]{1,0:T(8,128)(2,1)S(1)}, bf16[2048,512]{1,0:T(8,128)(2,1)}, u32[]{:S(2)}) copy-start(bf16[2048,512]{1,0:T(8,128)(2,1)} %param.9) | copy-start | bytes 6291460
  3.4 45.9 %all-to-all-start.2 = ((bf16[16,2,192]{2,1,0:T(2,128)(2,1)}), bf16[16,2,192]{2,1,0:T(2,128)(2,1)S(1)}, u32[]{:S(2)}, u32[]{:S(2)}) async-start(bf16[16,2,192]{2,1,0:T(2,128)(2,1)} %reshape.127), calls=%async_computation.2 | async-start | bytes 32768 | tf_op jit(solution)/shard_map/all_to_all | solution.py:50
  27.4 4.1 %copy-start.3 = (f32[2048]{0:T(1024)S(1)}, f32[2048]{0:T(1024)}, u32[]{:S(2)}) copy-start(f32[2048]{0:T(1024)} %param.8) | copy-start | bytes 24580
  35.8 2.7 %copy-start.1 = (bf16[1536,2048]{1,0:T(8,128)(2,1)}, bf16[1536,2048]{1,0:T(8,128)(2,1)S(1)}, u32[]{:S(2)}) copy-start(bf16[1536,2048]{1,0:T(8,128)(2,1)S(1)} %fusion.1) | copy-start | bytes 18874372
  49.4 85.6 %all-to-all-start = ((bf16[16,384,128]{2,1,0:T(8,128)(2,1)}), bf16[16,384,128]{2,1,0:T(8,128)(2,1)}, u32[]{:S(2)}, u32[]{:S(2)}) async-start(bf16[16,384,128]{2,1,0:T(8,128)(2,1)} %bitcast.47), calls=%async_computation | async-start | bytes 3145728 | tf_op jit(solution)/shard_map/all_to_all | solution.py:48
  75.8 65.6 %copy-start.4 = (bf16[1,1,512]{2,1,0:T(2,128)(2,1)S(1)}, bf16[1,1,512]{2,1,0:T(2,128)(2,1)}, u32[]{:S(2)}) copy-start(bf16[1,1,512]{2,1,0:T(2,128)(2,1)} %param.13) | copy-start | bytes 3076
  75.8 65.6 %copy-start.5 = (f32[16]{0:T(128)S(1)}, f32[16]{0:T(128)}, u32[]{:S(2)}) copy-start(f32[16]{0:T(128)} %param.12) | copy-start | bytes 196
  135.0 80.8 %all-to-all-start.1 = ((bf16[16,384,128]{2,1,0:T(8,128)(2,1)}), bf16[16,384,128]{2,1,0:T(8,128)(2,1)}, u32[]{:S(2)}, u32[]{:S(2)}) async-start(bf16[16,384,128]{2,1,0:T(8,128)(2,1)} %bitcast.46), calls=%async_computation.1 | async-start | bytes 3145728 | tf_op jit(solution)/shard_map/all_to_all | solution.py:49
  141.6 76.1 %copy-start.2 = (bf16[16,1,384]{2,1,0:T(2,128)(2,1)}, bf16[16,1,384]{2,1,0:T(2,128)(2,1)S(1)}, u32[]{:S(2)}) copy-start(bf16[16,1,384]{2,1,0:T(2,128)(2,1)S(1)} %reshape.128) | copy-start | bytes 36868
where the time goes:
time: 224 us
  waiting for transfers between devices  126 us (56%)
  starting transfers between devices  42.4 us (19%)
  local copies, waits for them, and re-layouts  23.8 us (11%)
  matrix products  16.4 us (7%)
  other arithmetic  14.8 us (7%)
    all_to_all x1, waiting for transfers between devices, shards(): lax.all_to_all(value_parts, 'sp', split_axis=0, concat_axis=1, tiled=True)  66.3 us
    all_to_all x1, waiting for transfers between devices, shards(): lax.all_to_all(key_parts, 'sp', split_axis=0, concat_axis=1, tiled=True)  59.2 us
    all_to_all x1, starting transfers between devices, shards(): lax.all_to_all(offset_parts, 'sp', split_axis=0, concat_axis=1, tiled=True)  24 us
    dot_general x2, matrix products, project(): jnp.dot(normed_rows, weight, preferred_element_type=jnp.float32)  12.5 us
    all_to_all x1, starting transfers between devices, shards(): lax.all_to_all(key_parts, 'sp', split_axis=0, concat_axis=1, tiled=True)  12 us
    unnamed x17, local copies, waits for them, and re-layouts  8.78 us
    all_to_all x1, starting transfers between devices, shards(): lax.all_to_all(value_parts, 'sp', split_axis=0, concat_axis=1, tiled=True)  6.41 us
    reshape x2, local copies, waits for them, and re-layouts, shards(): project(normed_rows, value_weight).reshape(seq_count, block_len, KVH, HD)  6.38 us
  transfers between devices with their start and end apart: 3, of which 2 were waited for; matrix products, arithmetic and copies ran while one was open for 19% of the time, Pallas kernels for 0%

commit v1 on v0

v1 whole, which is shorter than its diff:
```python
import functools
import math

import jax
import jax.numpy as jnp
from jax import lax
from jax.experimental import pallas as pl
from jax.experimental.pallas import tpu as pltpu
from jax.sharding import PartitionSpec as P


H = 16
KVH = 4
HD = 128
QG = H // KVH
EPSILON = 1e-06
ROWS = 8

ORDER = tuple((c, k) for c in (2, 1, 3, 0) for k in range(KVH) if c or k)
FIRST = ORDER[0][0]
LATE = 3

ANY = pl.BlockSpec(memory_space=pltpu.HBM)
VMEM = pl.BlockSpec(memory_space=pltpu.VMEM)
SMEM = pl.BlockSpec(memory_space=pltpu.SMEM)


def split_index():
    z = lax.axis_index("sp")
    return lax.div(z, KVH), lax.rem(z, KVH)


def project_kernel(classes, x_ref, gain_ref, key_ref, value_ref, *rest):
    count = len(classes)
    outs = rest[: count * KVH]
    rows, wk, wv, normed, parts, x_sems, w_sems, o_sems = rest[count * KVH :]
    group, member = split_index()
    block_len = x_ref.shape[1]
    loads = [
        pltpu.make_async_copy(x_ref.at[group ^ c], rows.at[n], x_sems.at[n]) for n, c in enumerate(classes)
    ]
    weights = [
        pltpu.make_async_copy(key_ref, wk, w_sems.at[0]),
        pltpu.make_async_copy(value_ref, wv, w_sems.at[1]),
    ]
    loads[0].start()
    weights[0].start()
    weights[1].start()
    for load in loads[1:]:
        load.start()
    gain = gain_ref[...].reshape(1, -1)
    stores = []
    for n in range(count):
        loads[n].wait()
        step = 64

        def normalize(r, _, n=n):
            start = pl.multiple_of(r * step, step)
            wide = rows[n, pl.ds(start, step), :].astype(jnp.float32)
            mean = jnp.mean(wide * wide, axis=-1, keepdims=True)
            normed[pl.ds(start, step), :] = (wide * lax.rsqrt(mean + EPSILON) * gain).astype(jnp.bfloat16)
            return 0

        lax.fori_loop(0, block_len // step, normalize, 0, unroll=True)
        for w, weight in enumerate((wk, wv)):
            if n == 0:
                weights[w].wait()
            product = jnp.dot(normed[...], weight[...], preferred_element_type=jnp.float32).astype(jnp.bfloat16)
            for h in range(KVH):
                parts[n, h, w * block_len : (w + 1) * block_len, :] = product[:, h * HD : (h + 1) * HD]
        for k in range(KVH):
            i = n * KVH + k
            store = pltpu.make_async_copy(parts.at[n, member ^ k], outs[i], o_sems.at[i])
            store.start()
            stores.append(store)
    for store in stores:
        store.wait()


def project(classes, layer_input, input_gain, key_weight, value_weight):
    _, block_len, width = layer_input.shape
    columns = key_weight.shape[1]
    count = len(classes)
    piece = jax.ShapeDtypeStruct((2 * block_len, HD), jnp.bfloat16)
    return pl.pallas_call(
        functools.partial(project_kernel, classes),
        out_shape=[piece] * (count * KVH),
        in_specs=[ANY, VMEM, ANY, ANY],
        out_specs=[ANY] * (count * KVH),
        scratch_shapes=[
            pltpu.VMEM((count, block_len, width), jnp.bfloat16),
            pltpu.VMEM((width, columns), jnp.bfloat16),
            pltpu.VMEM((width, columns), jnp.bfloat16),
            pltpu.VMEM((block_len, width), jnp.bfloat16),
            pltpu.VMEM((count, KVH, 2 * block_len, HD), jnp.bfloat16),
            pltpu.SemaphoreType.DMA((count,)),
            pltpu.SemaphoreType.DMA((2,)),
            pltpu.SemaphoreType.DMA((count * KVH,)),
        ],
        compiler_params=pltpu.CompilerParams(vmem_limit_bytes=48 * 1024 * 1024),
        cost_estimate=pl.CostEstimate(
            flops=4 * count * block_len * width * columns,
            bytes_accessed=count * block_len * width * 2 + 4 * width * columns,
            transcendentals=0,
        ),
        name="project",
    )(layer_input, input_gain, key_weight, value_weight)


def read_kernel(pieces, final, q_ref, bias_ref, offset_ref, *rest):
    count = len(pieces)
    piece_refs = rest[:count]
    rest = rest[count:]
    if final:
        total_in, mixed_in, _, _, key_out, value_out, read_out, totals, mixed = rest[:9]
        rest = rest[9:]
    else:
        key_out, value_out, totals, mixed = rest[:4]
        rest = rest[4:]
    held, scores, in_sems, out_sems = rest
    block_len = held.shape[1] // 2
    group, member = split_index()
    blocks = [(group ^ c) * KVH + (member ^ k) for c, k in pieces]
    loads = [pltpu.make_async_copy(piece_refs[i], held.at[i], in_sems.at[i]) for i in range(count)]
    for load in loads:
        load.start()
    line = lax.broadcasted_iota(jnp.int32, (ROWS, 1), 0)
    bias = jnp.zeros((ROWS, 1), jnp.float32)
    query = jnp.zeros((ROWS, HD), jnp.float32)
    for g in range(QG):
        bias = jnp.where(line == g, bias_ref[member * QG + g], bias)
        query = jnp.where(line == g, q_ref[0, :, g * HD : (g + 1) * HD].astype(jnp.float32), query)
    query = query.astype(jnp.bfloat16)
    if final:
        totals[...] = total_in[...]
        mixed[...] = mixed_in[...]
    stores = []
    for i in range(count):
        loads[i].wait()
        place = pl.ds(pl.multiple_of(blocks[i] * block_len, block_len), block_len)
        for w, out in enumerate((key_out, value_out)):
            store = pltpu.make_async_copy(
                held.at[i, pl.ds(w * block_len, block_len)], out.at[0, 0, place], out_sems.at[2 * i + w]
            )
            store.start()
            stores.append(store)
        found = lax.dot_general(
            query, held[i, :block_len], (((1,), (1,)), ((), ())), preferred_element_type=jnp.float32
        )
        scores[i * ROWS : (i + 1) * ROWS, :] = found / math.sqrt(HD) + bias + offset_ref[pl.ds(blocks[i], 1), :]
    z = scores[...]
    soft = jnp.log1p(jnp.exp(-jnp.abs(z)))
    spread = jnp.maximum(z, 0.0) + soft
    after = (
        lax.broadcasted_iota(jnp.int32, (block_len, block_len), 0)
        > lax.broadcasted_iota(jnp.int32, (block_len, block_len), 1)
    ).astype(jnp.bfloat16)
    high = spread.astype(jnp.bfloat16)
    left = spread - high.astype(jnp.float32)
    middle = left.astype(jnp.bfloat16)
    low = (left - middle.astype(jnp.float32)).astype(jnp.bfloat16)
    inside = (
        jnp.dot(low, after, preferred_element_type=jnp.float32)
        + jnp.dot(middle, after, preferred_element_type=jnp.float32)
        + jnp.dot(high, after, preferred_element_type=jnp.float32)
    )
    weights = jnp.exp(jnp.minimum(z, 0.0) - soft - inside).astype(jnp.bfloat16)
    sums = jnp.sum(spread, axis=-1, keepdims=True)
    for i in range(count):
        lines = slice(i * ROWS, (i + 1) * ROWS)
        totals[blocks[i]] = jnp.broadcast_to(sums[lines], (ROWS, HD))
        mixed[blocks[i]] = jnp.dot(weights[lines], held[i, block_len:], preferred_element_type=jnp.float32)
    if final:
        carried = jnp.zeros((ROWS, HD), jnp.float32)
        mixture = jnp.zeros((ROWS, HD), jnp.float32)
        for block in reversed(range(totals.shape[0])):
            mixture = mixture + jnp.exp(-carried) * mixed[block]
            carried = carried + totals[block]
        mean = jnp.mean(mixture * mixture, axis=-1, keepdims=True)
        read = (mixture * lax.rsqrt(mean + EPSILON)).astype(jnp.bfloat16)
        for g in range(QG):
            read_out[0, :, g * HD : (g + 1) * HD] = read[g : g + 1, :]
    for store in stores:
        store.wait()


def read(pieces, queries, head_bias, offsets, values, earlier=()):
    final = bool(earlier)
    count = len(pieces)
    sp_count, block_len = offsets.shape
    caches = [jax.ShapeDtypeStruct((1, 1, sp_count * block_len, HD), jnp.bfloat16)] * 2
    partial = jax.ShapeDtypeStruct((sp_count, ROWS, HD), jnp.float32)
    scratch = [
        pltpu.VMEM((count, 2 * block_len, HD), jnp.bfloat16),
        pltpu.VMEM((count * ROWS, block_len), jnp.float32),
        pltpu.SemaphoreType.DMA((count,)),
        pltpu.SemaphoreType.DMA((2 * count,)),
    ]
    held = [pltpu.VMEM(partial.shape, partial.dtype)] * 2
    return pl.pallas_call(
        functools.partial(read_kernel, pieces, final),
        out_shape=caches + ([jax.ShapeDtypeStruct(queries.shape, jnp.bfloat16)] if final else [partial] * 2),
        in_specs=[VMEM, SMEM, VMEM] + [ANY] * count + ([VMEM, VMEM, ANY, ANY] if final else []),
        out_specs=[ANY, ANY] + ([VMEM] if final else [VMEM] * 2),
        scratch_shapes=(held if final else []) + scratch,
        input_output_aliases={3 + count + 2: 0, 3 + count + 3: 1} if final else {},
        compiler_params=pltpu.CompilerParams(vmem_limit_bytes=32 * 1024 * 1024),
        cost_estimate=pl.CostEstimate(
            flops=64 * count * block_len * HD, bytes_accessed=8 * count * block_len * HD, transcendentals=0
        ),
        name="read",
    )(queries, head_bias, offsets, *values, *earlier)


def shards(layer_input, input_gain, key_weight, value_weight, stick_offsets, head_bias, queries):
    _, block_len, _ = layer_input.shape
    sp_count = lax.axis_size("sp")
    length = sp_count * block_len
    others = tuple(dict.fromkeys(c for c, _ in ORDER if c != FIRST))

    def pairs(c, k):
        return [(z, ((z // KVH) ^ c) * KVH + ((z % KVH) ^ k)) for z in range(sp_count)]

    args = (layer_input, input_gain, key_weight, value_weight)
    made = {}
    for k, piece in enumerate(project((FIRST,), *args)):
        made[FIRST, k] = piece
    for i, piece in enumerate(project(others, *args)):
        made[others[i // KVH], i % KVH] = piece
    got = {(0, 0): made[0, 0]}
    for c, k in ORDER:
        got[c, k] = lax.ppermute(made[c, k], "sp", pairs(c, k))
    offset_parts = jnp.transpose(stick_offsets, (1, 0, 2)).reshape(sp_count, block_len)
    offset_rows = lax.all_to_all(offset_parts, "sp", split_axis=0, concat_axis=0, tiled=True)
    offset_cache = offset_rows.reshape(1, 1, length)
    offset_rows = offset_rows.astype(jnp.float32)
    early = ((0, 0),) + ORDER[:-LATE]
    late = ORDER[-LATE:]
    key_cache, value_cache, totals, mixed = read(
        early, queries, head_bias, offset_rows, [got[piece] for piece in early]
    )
    key_cache, value_cache, first_read = read(
        late,
        queries,
        head_bias,
        offset_rows,
        [got[piece] for piece in late],
        (totals, mixed, key_cache, value_cache),
    )
    return key_cache, value_cache, offset_cache, first_read


def solution(mesh):
    row = P(("grp", "tp"), "sp", None)
    return jax.shard_map(
        shards,
        mesh=mesh,
        in_specs=(row, P(), P(), P(), P(None, ("grp", "tp"), "sp"), P(), row),
        out_specs=(
            P(("grp", "tp"), "sp", None, None),
            P(("grp", "tp"), "sp", None, None),
            row,
            row,
        ),
        check_vma=False,
    )
```

time: 224 us -> 240 us (1.071)
  starting transfers between devices: 42.4 us -> 111 us
  waiting for transfers between devices: 126 us -> 64 us
  Pallas kernels: 0 us -> 26.3 us
  blocking collectives: 0 us -> 24.8 us
  matrix products: 16.4 us -> 0 us
  local copies, waits for them, and re-layouts: 23.8 us -> 9.14 us
  other arithmetic: 14.8 us -> 2.78 us
    all_to_all x3 -> x0, waiting for transfers between devices: 126 us -> none  [the longest x1 66.3 us: shards(): lax.all_to_all(value_parts, 'sp', split_axis=0, concat_axis=1, tiled=True)]
    ppermute x0 -> x15, starting transfers between devices: none -> 111 us  [shards(): got[c, k] = lax.ppermute(made[c, k], 'sp', pairs(c, k))]
    ppermute x0 -> x15, waiting for transfers between devices: none -> 64 us  [shards(): got[c, k] = lax.ppermute(made[c, k], 'sp', pairs(c, k))]
    all_to_all x3 -> x0, starting transfers between devices: 42.4 us -> none  [the longest x1 24 us: shards(): lax.all_to_all(offset_parts, 'sp', split_axis=0, concat_axis=1, tiled=True)]
    pallas_call x0 -> x4, Pallas kernels: none -> 26.3 us  [the longest x2 15.8 us: project(): pl.pallas_call(functools.partial(project_kernel, classes), out_shape=[pie...]
    all_to_all x0 -> x1, blocking collectives: none -> 24.8 us  [shards(): lax.all_to_all(offset_parts, 'sp', split_axis=0, concat_axis=0, tiled=True)]
    dot_general x4 -> x0, matrix products: 16.4 us -> none  [the longest x2 12.5 us: project(): jnp.dot(normed_rows, weight, preferred_element_type=jnp.float32)]
    reshape x6 -> x0, local copies, waits for them, and re-layouts: 13.4 us -> none  [the longest x2 6.38 us: shards(): project(normed_rows, value_weight).reshape(seq_count, block_len, KVH, HD)]
  transfers between devices with their start and end apart: 3 -> 15, of which waited for: 2 -> 4; matrix products, arithmetic and copies ran while one was open for 19% -> 3% of each run, Pallas kernels for 0% -> 8%
where the time goes in v1:
time: 240 us; the launch traced here: 239 us
  starting transfers between devices  111 us (46%)
  waiting for transfers between devices  64 us (27%)
  Pallas kernels  26.3 us (11%)
  blocking collectives  24.8 us (10%)
  local copies, waits for them, and re-layouts  9.14 us (4%)
  other arithmetic  2.78 us (1%)
    ppermute x15, starting transfers between devices, shards(): got[c, k] = lax.ppermute(made[c, k], 'sp', pairs(c, k))  111 us
    ppermute x15, waiting for transfers between devices, shards(): got[c, k] = lax.ppermute(made[c, k], 'sp', pairs(c, k))  64 us
    all_to_all x1, blocking collectives, shards(): lax.all_to_all(offset_parts, 'sp', split_axis=0, concat_axis=0, tiled=True)  24.8 us
    pallas_call x2, Pallas kernels, project(): pl.pallas_call(functools.partial(project_kernel, classes), out_shape=[pie...  15.8 us
    pallas_call x2, Pallas kernels, read(): pl.pallas_call(functools.partial(read_kernel, pieces, final), out_shape=c...  10.5 us
    unnamed x14, local copies, waits for them, and re-layouts  6.7 us
  transfers between devices with their start and end apart: 15, of which 4 were waited for; matrix products, arithmetic and copies ran while one was open for 3% of the time, Pallas kernels for 8%

profile of v1, /device:TPU:36, one launch (start us, length us, event | category | flops | bytes accessed | tf_op | source)
XLA Modules:
  0.0 238.6 jit_solution(7420917503144884810)
XLA Ops:
  0.6 0.0 copy-start
  0.6 1.6 copy-done
  2.2 0.0 copy-start.1
  2.2 1.6 copy-done.1
  3.8 0.0 copy-start.3
  3.8 0.7 copy-done.3
  4.5 5.0 %project.3 = (bf16[768,128]{1,0:T(8,128)(2,1)S(1)}, bf16[768,128]{1,0:T(8,128)(2,1)S(1)}, bf16[768,128]{1,0:T(8,128)(2,1)S(1)}, bf16[768,128]{1,0:T(8,128)(2,1)S(1)}) custom-call(bf16[4,384,2048]{2,1,0:T(8,128)(2,1)} %x_ref.3, f32[2048]{0:T(1024)S(1)} %copy-done.3, bf16[2048,512]{1,0:T(8,128)(2,1)S(1)} %copy-done, bf16[2048,512]{1,0:T(8,128)(2,1)S(1)} %copy-done.1), custom_call_target="tpu_custom_call" | custom-call | flops 1610612736 | bytes 5767168 | tf_op jit(solution)/shard_map/project/pallas_call | solution.py:85
  9.6 20.8 %collective-permute-start.3 = (bf16[768,128]{1,0:T(8,128)(2,1)S(1)}, bf16[768,128]{1,0:T(8,128)(2,1)S(1)}, u32[]{:S(2)}, u32[]{:S(2)}) collective-permute-start(bf16[768,128]{1,0:T(8,128)(2,1)S(1)} %get-tuple-element.31), channel_id=1, source_target_pairs={{0,64},{8,72},{16,80},{24,88},{32,96},{40,104},{48,112},{56,120},{... | collective-permute-start | bytes 589832 | tf_op jit(solution)/shard_map/ppermute | solution.py:232
  30.4 0.6 collective-permute-start.4
  30.9 11.4 %collective-permute-start.5 = (bf16[768,128]{1,0:T(8,128)(2,1)S(1)}, bf16[768,128]{1,0:T(8,128)(2,1)S(1)}, u32[]{:S(2)}, u32[]{:S(2)}) collective-permute-start(bf16[768,128]{1,0:T(8,128)(2,1)S(1)} %get-tuple-element.33), channel_id=1, source_target_pairs={{0,80},{8,88},{16,64},{24,72},{32,112},{40,120},{48,96},{56,104},{... | collective-permute-start | bytes 589832 | tf_op jit(solution)/shard_map/ppermute | solution.py:232
  42.4 0.0 copy-start.5
  42.4 0.0 copy-start.2
  42.4 0.0 copy-start.4
  42.4 0.0 collective-permute-start.6
  42.4 10.8 %project.2 = (bf16[768,128]{1,0:T(8,128)(2,1)S(1)}, bf16[768,128]{1,0:T(8,128)(2,1)}, bf16[768,128]{1,0:T(8,128)(2,1)}, bf16[768,128]{1,0:T(8,128)(2,1)}, bf16[7...) custom-call(bf16[4,384,2048]{2,1,0:T(8,128)(2,1)} %x_ref.3, ...), custom_call_target="tpu_custom_call" | custom-call | flops 4831838208 | bytes 8912896 | tf_op jit(solution)/shard_map/project/pallas_call | solution.py:85
  53.2 5.9 %collective-permute-start.7 = (bf16[768,128]{1,0:T(8,128)(2,1)S(1)}, bf16[768,128]{1,0:T(8,128)(2,1)S(1)}, u32[]{:S(2)}, u32[]{:S(2)}) collective-permute-start(bf16[768,128]{1,0:T(8,128)(2,1)S(1)} %get-tuple-element.35), channel_id=1, source_target_pairs={{0,32},{8,40},{16,48},{24,56},{32,0},{40,8},{48,16},{56,24},{64,96... | collective-permute-start | bytes 589832 | tf_op jit(solution)/shard_map/ppermute | solution.py:232
  59.1 0.0 collective-permute-done.3.rest_1_
  59.1 37.3 %collective-permute-start.8 = (bf16[768,128]{1,0:T(8,128)(2,1)}, bf16[768,128]{1,0:T(8,128)(2,1)S(1)}, u32[]{:S(2)}, u32[]{:S(2)}) collective-permute-start(bf16[768,128]{1,0:T(8,128)(2,1)} %get-tuple-element.36), channel_id=1, source_target_pairs={{0,40},{8,32},{16,56},{24,48},{32,8},{40,0},{48,24},{56,16},{64,10... | collective-permute-start | bytes 589832 | tf_op jit(solution)/shard_map/ppermute | solution.py:232
  96.4 0.0 collective-permute-done.4.rest_2_
  96.4 0.0 collective-permute-start.9
  96.5 0.0 collective-permute-done.5.rest_3_
  96.5 16.7 %collective-permute-start.10 = (bf16[768,128]{1,0:T(8,128)(2,1)}, bf16[768,128]{1,0:T(8,128)(2,1)S(1)}, u32[]{:S(2)}, u32[]{:S(2)}) collective-permute-start(bf16[768,128]{1,0:T(8,128)(2,1)} %get-tuple-element.38), channel_id=1, source_target_pairs={{0,56},{8,48},{16,40},{24,32},{32,24},{40,16},{48,8},{56,0},{64,12... | collective-permute-start | bytes 589832 | tf_op jit(solution)/shard_map/ppermute | solution.py:232
  113.2 24.2 %collective-permute-done.6.rest_4_ = bf16[768,128]{1,0:T(8,128)(2,1)S(1)} collective-permute-done((bf16[768,128]{1,0:T(8,128)(2,1)S(1)}, bf16[768,128]{1,0:T(8,128)(2,1)S(1)}, u32[]{:S(2)}, u32[]{:S(2)}) %collective-permute-start.6) | collective-permute-done | bytes 196640 | tf_op jit(solution)/shard_map/ppermute | solution.py:232
  137.4 9.3 %collective-permute-start.11 = (bf16[768,128]{1,0:T(8,128)(2,1)S(1)}, bf16[768,128]{1,0:T(8,128)(2,1)S(1)}, u32[]{:S(2)}, u32[]{:S(2)}) collective-permute-start(bf16[768,128]{1,0:T(8,128)(2,1)S(1)} %get-tuple-element.39), channel_id=1, source_target_pairs={{0,96},{8,104},{16,112},{24,120},{32,64},{40,72},{48,80},{56,88},{... | collective-permute-start | bytes 589832 | tf_op jit(solution)/shard_map/ppermute | solution.py:232
  146.7 8.2 %collective-permute-done.7.rest_5_ = bf16[768,128]{1,0:T(8,128)(2,1)S(1)} collective-permute-done((bf16[768,128]{1,0:T(8,128)(2,1)S(1)}, bf16[768,128]{1,0:T(8,128)(2,1)S(1)}, u32[]{:S(2)}, u32[]{:S(2)}) %collective-permute-start.7) | collective-permute-done | bytes 196640 | tf_op jit(solution)/shard_map/ppermute | solution.py:232
  154.9 0.0 collective-permute-start.12
  154.9 0.0 copy-done.5
  154.9 0.6 copy.16
  155.5 1.3 all_to_all.8
  156.8 0.5 broadcast
  157.3 2.0 reduce
  159.3 1.4 reshape.20
  160.7 24.8 %all_to_all.10 = bf16[16,2,192]{2,1,0:T(2,128)(2,1)} all-to-all(bf16[16,2,192]{2,1,0:T(2,128)(2,1)} %reshape.20), channel_id=1, replica_groups=mesh['grp'=2,'sp'=16,'tp'=8] {'sp'}, dimensions={0} | all-to-all | bytes 24576 | tf_op jit(solution)/shard_map/all_to_all | solution.py:234
  185.6 1.4 reshape.21
  187.0 0.0 collective-permute-done.8.rest_6_
  187.0 2.5 %collective-permute-start = (bf16[768,128]{1,0:T(8,128)(2,1)S(1)}, bf16[768,128]{1,0:T(8,128)(2,1)S(1)}, u32[]{:S(2)}, u32[]{:S(2)}) collective-permute-start(bf16[768,128]{1,0:T(8,128)(2,1)S(1)} %get-tuple-element.27), channel_id=1, source_target_pairs={{0,8},{8,0},{16,24},{24,16},{32,40},{40,32},{48,56},{56,48},{64,72... | collective-permute-start | bytes 589832 | tf_op jit(solution)/shard_map/ppermute | solution.py:232
  189.5 0.0 collective-permute-done.9.rest_7_
  189.5 1.3 collective-permute-start.1
  190.7 0.0 collective-permute-done.10.rest_8_
  190.7 1.2 collective-permute-start.2
  192.0 0.0 collective-permute-done.11.rest_9_
  192.0 2.9 %collective-permute-start.13 = (bf16[768,128]{1,0:T(8,128)(2,1)S(1)}, bf16[768,128]{1,0:T(8,128)(2,1)S(1)}, u32[]{:S(2)}, u32[]{:S(2)}) collective-permute-start(bf16[768,128]{1,0:T(8,128)(2,1)S(1)} %get-tuple-element.41), channel_id=1, source_target_pairs={{0,112},{8,120},{16,96},{24,104},{32,80},{40,88},{48,64},{56,72},{... | collective-permute-start | bytes 589832 | tf_op jit(solution)/shard_map/ppermute | solution.py:232
  194.8 0.0 collective-permute-done.12.rest_10_
  194.8 0.8 collective-permute-start.14
  195.6 0.7 bitcast_convert_fusion.offset_ref
  196.4 21.8 %collective-permute-done.13.rest_11_ = bf16[768,128]{1,0:T(8,128)(2,1)S(1)} collective-permute-done((bf16[768,128]{1,0:T(8,128)(2,1)S(1)}, bf16[768,128]{1,0:T(8,128)(2,1)S(1)}, u32[]{:S(2)}, u32[]{:S(2)}) %collective-permute-start.13) | collective-permute-done | bytes 196640 | tf_op jit(solution)/shard_map/ppermute | solution.py:232
  218.2 9.8 %collective-permute-done.14.rest_12_ = bf16[768,128]{1,0:T(8,128)(2,1)S(1)} collective-permute-done((bf16[768,128]{1,0:T(8,128)(2,1)S(1)}, bf16[768,128]{1,0:T(8,128)(2,1)S(1)}, u32[]{:S(2)}, u32[]{:S(2)}) %collective-permute-start.14) | collective-permute-done | bytes 196640 | tf_op jit(solution)/shard_map/ppermute | solution.py:232
  227.9 0.0 copy-done.2
  227.9 0.0 copy-done.4
  227.9 7.5 %read.2 = (bf16[1,1,6144,128]{3,2,1,0:T(8,128)(2,1)}, bf16[1,1,6144,128]{3,2,1,0:T(8,128)(2,1)}, f32[16,8,128]{2,1,0:T(8,128)S(1)}, f32[16,8,128]{2,1,0:T(8,128)S(1)}) custom-call(bf16[1,1,512]{2,1,0:T(2,128)(2,1)S(1)} %copy-done.2, f32[16]{0:T(128)S(1)} %copy-done.4, f32[16,384]{1,0:T(8,128)S(1)} %bitcast_convert_fusion.offset_ref, ...), custom_call_target="tpu_custom_call" | custom-call | flops 40894464 | bytes 5111808 | tf_op jit(solution)/shard_map/read/pallas_call | solution.py:200
  235.4 0.0 collective-permute-done.rest_0_
  235.4 0.0 collective-permute-done.1.rest_1_
  235.4 0.0 collective-permute-done.2.rest_2_
  235.4 3.0 %read.3 = (bf16[1,1,6144,128]{3,2,1,0:T(8,128)(2,1)}, bf16[1,1,6144,128]{3,2,1,0:T(8,128)(2,1)}, bf16[1,1,512]{2,1,0:T(2,128)(2,1)}) custom-call(bf16[1,1,512]{2,1,0:T(2,128)(2,1)S(1)} %copy-done.2, f32[16]{0:T(128)S(1)} %copy-done.4, f32[16,384]{1,0:T(8,128)S(1)} %bitcast_convert_fusion.offset_ref, ...), custom_call_target="tpu_custom_call", output_to_operand_aliasing={{0}: (8, {}), {1}: (9, {})} | custom-call | flops 9437184 | bytes 1179648 | tf_op jit(solution)/shard_map/read/pallas_call | solution.py:200
Async XLA Ops:
  0.6 1.6 copy-start
  2.2 1.6 copy-start.1
  3.8 0.7 copy-start.3
  9.6 49.5 %collective-permute-start.3 = (bf16[768,128]{1,0:T(8,128)(2,1)S(1)}, bf16[768,128]{1,0:T(8,128)(2,1)S(1)}, u32[]{:S(2)}, u32[]{:S(2)}) collective-permute-start(bf16[768,128]{1,0:T(8,128)(2,1)S(1)} %get-tuple-element.31), channel_id=1, source_target_pairs={{0,64},{8,72},{16,80},{24,88},{32,96},{40,104},{48,112},{56,120},{... | collective-permute-start | bytes 589832 | tf_op jit(solution)/shard_map/ppermute | solution.py:232
  30.4 66.1 %collective-permute-start.4 = (bf16[768,128]{1,0:T(8,128)(2,1)S(1)}, bf16[768,128]{1,0:T(8,128)(2,1)S(1)}, u32[]{:S(2)}, u32[]{:S(2)}) collective-permute-start(bf16[768,128]{1,0:T(8,128)(2,1)S(1)} %get-tuple-element.32), channel_id=1, source_target_pairs={{0,72},{8,64},{16,88},{24,80},{32,104},{40,96},{48,120},{56,112},{... | collective-permute-start | bytes 589832 | tf_op jit(solution)/shard_map/ppermute | solution.py:232
  30.9 65.6 %collective-permute-start.5 = (bf16[768,128]{1,0:T(8,128)(2,1)S(1)}, bf16[768,128]{1,0:T(8,128)(2,1)S(1)}, u32[]{:S(2)}, u32[]{:S(2)}) collective-permute-start(bf16[768,128]{1,0:T(8,128)(2,1)S(1)} %get-tuple-element.33), channel_id=1, source_target_pairs={{0,80},{8,88},{16,64},{24,72},{32,112},{40,120},{48,96},{56,104},{... | collective-permute-start | bytes 589832 | tf_op jit(solution)/shard_map/ppermute | solution.py:232
  42.4 112.5 %copy-start.5 = (bf16[4,4,384]{2,1,0:T(4,128)(2,1)S(1)}, bf16[4,4,384]{2,1,0:T(4,128)(2,1)}, u32[]{:S(2)}) copy-start(bf16[4,4,384]{2,1,0:T(4,128)(2,1)} %param.11) | copy-start | bytes 36868
  42.4 185.6 %copy-start.2 = (bf16[1,1,512]{2,1,0:T(2,128)(2,1)S(1)}, bf16[1,1,512]{2,1,0:T(2,128)(2,1)}, u32[]{:S(2)}) copy-start(bf16[1,1,512]{2,1,0:T(2,128)(2,1)} %q_ref.3) | copy-start | bytes 3076
  42.4 185.6 %copy-start.4 = (f32[16]{0:T(128)S(1)}, f32[16]{0:T(128)}, u32[]{:S(2)}) copy-start(f32[16]{0:T(128)} %bias_ref.3) | copy-start | bytes 196
  42.4 95.1 %collective-permute-start.6 = (bf16[768,128]{1,0:T(8,128)(2,1)S(1)}, bf16[768,128]{1,0:T(8,128)(2,1)S(1)}, u32[]{:S(2)}, u32[]{:S(2)}) collective-permute-start(bf16[768,128]{1,0:T(8,128)(2,1)S(1)} %get-tuple-element.34), channel_id=1, source_target_pairs={{0,88},{8,80},{16,72},{24,64},{32,120},{40,112},{48,104},{56,96},{... | collective-permute-start | bytes 589832 | tf_op jit(solution)/shard_map/ppermute | solution.py:232
  53.2 101.7 %collective-permute-start.7 = (bf16[768,128]{1,0:T(8,128)(2,1)S(1)}, bf16[768,128]{1,0:T(8,128)(2,1)S(1)}, u32[]{:S(2)}, u32[]{:S(2)}) collective-permute-start(bf16[768,128]{1,0:T(8,128)(2,1)S(1)} %get-tuple-element.35), channel_id=1, source_target_pairs={{0,32},{8,40},{16,48},{24,56},{32,0},{40,8},{48,16},{56,24},{64,96... | collective-permute-start | bytes 589832 | tf_op jit(solution)/shard_map/ppermute | solution.py:232
  59.1 127.9 %collective-permute-start.8 = (bf16[768,128]{1,0:T(8,128)(2,1)}, bf16[768,128]{1,0:T(8,128)(2,1)S(1)}, u32[]{:S(2)}, u32[]{:S(2)}) collective-permute-start(bf16[768,128]{1,0:T(8,128)(2,1)} %get-tuple-element.36), channel_id=1, source_target_pairs={{0,40},{8,32},{16,56},{24,48},{32,8},{40,0},{48,24},{56,16},{64,10... | collective-permute-start | bytes 589832 | tf_op jit(solution)/shard_map/ppermute | solution.py:232
  96.4 93.0 %collective-permute-start.9 = (bf16[768,128]{1,0:T(8,128)(2,1)}, bf16[768,128]{1,0:T(8,128)(2,1)S(1)}, u32[]{:S(2)}, u32[]{:S(2)}) collective-permute-start(bf16[768,128]{1,0:T(8,128)(2,1)} %get-tuple-element.37), channel_id=1, source_target_pairs={{0,48},{8,56},{16,32},{24,40},{32,16},{40,24},{48,0},{56,8},{64,11... | collective-permute-start | bytes 589832 | tf_op jit(solution)/shard_map/ppermute | solution.py:232
  96.5 94.2 %collective-permute-start.10 = (bf16[768,128]{1,0:T(8,128)(2,1)}, bf16[768,128]{1,0:T(8,128)(2,1)S(1)}, u32[]{:S(2)}, u32[]{:S(2)}) collective-permute-start(bf16[768,128]{1,0:T(8,128)(2,1)} %get-tuple-element.38), channel_id=1, source_target_pairs={{0,56},{8,48},{16,40},{24,32},{32,24},{40,16},{48,8},{56,0},{64,12... | collective-permute-start | bytes 589832 | tf_op jit(solution)/shard_map/ppermute | solution.py:232
  137.4 54.5 %collective-permute-start.11 = (bf16[768,128]{1,0:T(8,128)(2,1)S(1)}, bf16[768,128]{1,0:T(8,128)(2,1)S(1)}, u32[]{:S(2)}, u32[]{:S(2)}) collective-permute-start(bf16[768,128]{1,0:T(8,128)(2,1)S(1)} %get-tuple-element.39), channel_id=1, source_target_pairs={{0,96},{8,104},{16,112},{24,120},{32,64},{40,72},{48,80},{56,88},{... | collective-permute-start | bytes 589832 | tf_op jit(solution)/shard_map/ppermute | solution.py:232
  154.9 40.0 %collective-permute-start.12 = (bf16[768,128]{1,0:T(8,128)(2,1)S(1)}, bf16[768,128]{1,0:T(8,128)(2,1)S(1)}, u32[]{:S(2)}, u32[]{:S(2)}) collective-permute-start(bf16[768,128]{1,0:T(8,128)(2,1)S(1)} %get-tuple-element.40), channel_id=1, source_target_pairs={{0,104},{8,96},{16,120},{24,112},{32,72},{40,64},{48,88},{56,80},{... | collective-permute-start | bytes 589832 | tf_op jit(solution)/shard_map/ppermute | solution.py:232
  187.0 48.4 %collective-permute-start = (bf16[768,128]{1,0:T(8,128)(2,1)S(1)}, bf16[768,128]{1,0:T(8,128)(2,1)S(1)}, u32[]{:S(2)}, u32[]{:S(2)}) collective-permute-start(bf16[768,128]{1,0:T(8,128)(2,1)S(1)} %get-tuple-element.27), channel_id=1, source_target_pairs={{0,8},{8,0},{16,24},{24,16},{32,40},{40,32},{48,56},{56,48},{64,72... | collective-permute-start | bytes 589832 | tf_op jit(solution)/shard_map/ppermute | solution.py:232
  189.5 46.0 %collective-permute-start.1 = (bf16[768,128]{1,0:T(8,128)(2,1)S(1)}, bf16[768,128]{1,0:T(8,128)(2,1)S(1)}, u32[]{:S(2)}, u32[]{:S(2)}) collective-permute-start(bf16[768,128]{1,0:T(8,128)(2,1)S(1)} %get-tuple-element.28), channel_id=1, source_target_pairs={{0,16},{8,24},{16,0},{24,8},{32,48},{40,56},{48,32},{56,40},{64,80... | collective-permute-start | bytes 589832 | tf_op jit(solution)/shard_map/ppermute | solution.py:232
  190.7 44.7 %collective-permute-start.2 = (bf16[768,128]{1,0:T(8,128)(2,1)S(1)}, bf16[768,128]{1,0:T(8,128)(2,1)S(1)}, u32[]{:S(2)}, u32[]{:S(2)}) collective-permute-start(bf16[768,128]{1,0:T(8,128)(2,1)S(1)} %get-tuple-element.29), channel_id=1, source_target_pairs={{0,24},{8,16},{16,8},{24,0},{32,56},{40,48},{48,40},{56,32},{64,88... | collective-permute-start | bytes 589832 | tf_op jit(solution)/shard_map/ppermute | solution.py:232
  192.0 26.2 %collective-permute-start.13 = (bf16[768,128]{1,0:T(8,128)(2,1)S(1)}, bf16[768,128]{1,0:T(8,128)(2,1)S(1)}, u32[]{:S(2)}, u32[]{:S(2)}) collective-permute-start(bf16[768,128]{1,0:T(8,128)(2,1)S(1)} %get-tuple-element.41), channel_id=1, source_target_pairs={{0,112},{8,120},{16,96},{24,104},{32,80},{40,88},{48,64},{56,72},{... | collective-permute-start | bytes 589832 | tf_op jit(solution)/shard_map/ppermute | solution.py:232
  194.8 33.1 %collective-permute-start.14 = (bf16[768,128]{1,0:T(8,128)(2,1)S(1)}, bf16[768,128]{1,0:T(8,128)(2,1)S(1)}, u32[]{:S(2)}, u32[]{:S(2)}) collective-permute-start(bf16[768,128]{1,0:T(8,128)(2,1)S(1)} %get-tuple-element.42), channel_id=1, source_target_pairs={{0,120},{8,112},{16,104},{24,96},{32,88},{40,80},{48,72},{56,64},{... | collective-permute-start | bytes 589832 | tf_op jit(solution)/shard_map/ppermute | solution.py:232

commit v2 on v1

v2 whole, which is shorter than its diff:
```python
import functools
import math

import jax
import jax.numpy as jnp
from jax import lax
from jax.experimental import pallas as pl
from jax.experimental.pallas import tpu as pltpu
from jax.sharding import PartitionSpec as P


H = 16
KVH = 4
HD = 128
QG = H // KVH
EPSILON = 1e-06
ROWS = 8
EXTRA = 8

ORDER = tuple((c, k) for c in (2, 1, 3, 0) for k in range(KVH) if c or k)
FIRST = ORDER[0][0]
LATE = 3

ANY = pl.BlockSpec(memory_space=pltpu.HBM)
VMEM = pl.BlockSpec(memory_space=pltpu.VMEM)
SMEM = pl.BlockSpec(memory_space=pltpu.SMEM)


def split_index():
    z = lax.axis_index("sp")
    return lax.div(z, KVH), lax.rem(z, KVH)


def project_kernel(classes, x_ref, gain_ref, key_ref, value_ref, offset_ref, *rest):
    count = len(classes)
    outs = rest[: count * KVH]
    rows, wk, wv, gains, offsets, normed, parts, x_sems, w_sems, o_sems = rest[count * KVH :]
    group, member = split_index()
    block_len = x_ref.shape[1]
    loads = [
        pltpu.make_async_copy(x_ref.at[group ^ c], rows.at[n], x_sems.at[n]) for n, c in enumerate(classes)
    ]
    weights = [
        pltpu.make_async_copy(key_ref, wk, w_sems.at[0]),
        pltpu.make_async_copy(value_ref, wv, w_sems.at[1]),
    ]
    small = [
        pltpu.make_async_copy(gain_ref, gains, w_sems.at[2]),
        pltpu.make_async_copy(offset_ref, offsets, w_sems.at[3]),
    ]
    for load in small:
        load.start()
    loads[0].start()
    weights[0].start()
    weights[1].start()
    for load in loads[1:]:
        load.start()
    for load in small:
        load.wait()
    gain = gains[...].reshape(1, -1)
    line = lax.broadcasted_iota(jnp.int32, (EXTRA, HD), 0)
    prompt = lax.broadcasted_iota(jnp.int32, (x_ref.shape[0], 1), 0)
    for n, c in enumerate(classes):
        for h in range(KVH):
            own = offsets[h].astype(jnp.float32)
            own = jnp.sum(jnp.where(prompt == (group ^ c), own, 0.0), axis=0, keepdims=True)
            extra = jnp.zeros((EXTRA, HD), jnp.float32)
            for j in range(block_len // HD):
                extra = jnp.where(line == j, own[:, j * HD : (j + 1) * HD], extra)
            parts[n, h, 2 * block_len :, :] = extra.astype(jnp.bfloat16)
    stores = []
    for n in range(count):
        loads[n].wait()
        step = 64

        def normalize(r, _, n=n):
            start = pl.multiple_of(r * step, step)
            wide = rows[n, pl.ds(start, step), :].astype(jnp.float32)
            mean = jnp.mean(wide * wide, axis=-1, keepdims=True)
            normed[pl.ds(start, step), :] = (wide * lax.rsqrt(mean + EPSILON) * gain).astype(jnp.bfloat16)
            return 0

        lax.fori_loop(0, block_len // step, normalize, 0, unroll=True)
        for w, weight in enumerate((wk, wv)):
            if n == 0:
                weights[w].wait()
            product = jnp.dot(normed[...], weight[...], preferred_element_type=jnp.float32).astype(jnp.bfloat16)
            for h in range(KVH):
                parts[n, h, w * block_len : (w + 1) * block_len, :] = product[:, h * HD : (h + 1) * HD]
        for k in range(KVH):
            i = n * KVH + k
            store = pltpu.make_async_copy(parts.at[n, member ^ k], outs[i], o_sems.at[i])
            store.start()
            stores.append(store)
    for store in stores:
        store.wait()


def project(classes, layer_input, input_gain, key_weight, value_weight, stick_offsets):
    _, block_len, width = layer_input.shape
    columns = key_weight.shape[1]
    count = len(classes)
    piece = jax.ShapeDtypeStruct((2 * block_len + EXTRA, HD), jnp.bfloat16)
    return pl.pallas_call(
        functools.partial(project_kernel, classes),
        out_shape=[piece] * (count * KVH),
        in_specs=[ANY] * 5,
        out_specs=[ANY] * (count * KVH),
        scratch_shapes=[
            pltpu.VMEM((count, block_len, width), jnp.bfloat16),
            pltpu.VMEM((width, columns), jnp.bfloat16),
            pltpu.VMEM((width, columns), jnp.bfloat16),
            pltpu.VMEM(input_gain.shape, input_gain.dtype),
            pltpu.VMEM(stick_offsets.shape, stick_offsets.dtype),
            pltpu.VMEM((block_len, width), jnp.bfloat16),
            pltpu.VMEM((count, KVH, 2 * block_len + EXTRA, HD), jnp.bfloat16),
            pltpu.SemaphoreType.DMA((count,)),
            pltpu.SemaphoreType.DMA((4,)),
            pltpu.SemaphoreType.DMA((count * KVH,)),
        ],
        compiler_params=pltpu.CompilerParams(vmem_limit_bytes=48 * 1024 * 1024),
        cost_estimate=pl.CostEstimate(
            flops=4 * count * block_len * width * columns,
            bytes_accessed=count * block_len * width * 2 + 4 * width * columns,
            transcendentals=0,
        ),
        name="project",
    )(
        *(
            pltpu.with_memory_space_constraint(value, pltpu.HBM)
            for value in (layer_input, input_gain, key_weight, value_weight, stick_offsets)
        )
    )


def read_kernel(pieces, final, q_ref, bias_ref, *rest):
    count = len(pieces)
    held = rest[:count]
    rest = rest[count:]
    if final:
        total_in, mixed_in, row_in, _, _, key_out, value_out, offset_out, read_out, totals, mixed, rows = rest[:12]
        rest = rest[12:]
    else:
        key_out, value_out, totals, mixed, rows = rest[:5]
        rest = rest[5:]
    scores, out_sems = rest
    block_len = rows.shape[2]
    group, member = split_index()
    blocks = [(group ^ c) * KVH + (member ^ k) for c, k in pieces]
    stores = []
    for i in range(count):
        place = pl.ds(pl.multiple_of(blocks[i] * block_len, block_len), block_len)
        for w, out in enumerate((key_out, value_out)):
            store = pltpu.make_async_copy(
                held[i].at[pl.ds(w * block_len, block_len)], out.at[0, 0, place], out_sems.at[2 * i + w]
            )
            store.start()
            stores.append(store)
    line = lax.broadcasted_iota(jnp.int32, (ROWS, 1), 0)
    bias = jnp.zeros((ROWS, 1), jnp.float32)
    query = jnp.zeros((ROWS, HD), jnp.float32)
    for g in range(QG):
        bias = jnp.where(line == g, bias_ref[member * QG + g], bias)
        query = jnp.where(line == g, q_ref[0, :, g * HD : (g + 1) * HD].astype(jnp.float32), query)
    query = query.astype(jnp.bfloat16)
    if final:
        totals[...] = total_in[...]
        mixed[...] = mixed_in[...]
        rows[...] = row_in[...]
    for i in range(count):
        extra = held[i][2 * block_len :, :].astype(jnp.float32)
        offset = jnp.concatenate([extra[j : j + 1, :] for j in range(block_len // HD)], axis=1)
        rows[blocks[i]] = offset
        found = lax.dot_general(
            query, held[i][:block_len, :], (((1,), (1,)), ((), ())), preferred_element_type=jnp.float32
        )
        scores[i * ROWS : (i + 1) * ROWS, :] = found / math.sqrt(HD) + bias + offset
    z = scores[...]
    soft = jnp.log1p(jnp.exp(-jnp.abs(z)))
    spread = jnp.maximum(z, 0.0) + soft
    after = (
        lax.broadcasted_iota(jnp.int32, (block_len, block_len), 0)
        > lax.broadcasted_iota(jnp.int32, (block_len, block_len), 1)
    ).astype(jnp.bfloat16)
    high = spread.astype(jnp.bfloat16)
    left = spread - high.astype(jnp.float32)
    middle = left.astype(jnp.bfloat16)
    low = (left - middle.astype(jnp.float32)).astype(jnp.bfloat16)
    inside = (
        jnp.dot(low, after, preferred_element_type=jnp.float32)
        + jnp.dot(middle, after, preferred_element_type=jnp.float32)
        + jnp.dot(high, after, preferred_element_type=jnp.float32)
    )
    weights = jnp.exp(jnp.minimum(z, 0.0) - soft - inside).astype(jnp.bfloat16)
    sums = jnp.sum(spread, axis=-1, keepdims=True)
    for i in range(count):
        lines = slice(i * ROWS, (i + 1) * ROWS)
        totals[blocks[i]] = jnp.broadcast_to(sums[lines], (ROWS, HD))
        mixed[blocks[i]] = jnp.dot(
            weights[lines], held[i][block_len : 2 * block_len, :], preferred_element_type=jnp.float32
        )
    if final:
        carried = jnp.zeros((ROWS, HD), jnp.float32)
        mixture = jnp.zeros((ROWS, HD), jnp.float32)
        for block in reversed(range(totals.shape[0])):
            mixture = mixture + jnp.exp(-carried) * mixed[block]
            carried = carried + totals[block]
            offset_out[0, :, block * block_len : (block + 1) * block_len] = rows[block].astype(jnp.bfloat16)
        mean = jnp.mean(mixture * mixture, axis=-1, keepdims=True)
        read = (mixture * lax.rsqrt(mean + EPSILON)).astype(jnp.bfloat16)
        for g in range(QG):
            read_out[0, :, g * HD : (g + 1) * HD] = read[g : g + 1, :]
    for store in stores:
        store.wait()


def read(pieces, queries, head_bias, sp_count, block_len, values, earlier=()):
    final = bool(earlier)
    count = len(pieces)
    length = sp_count * block_len
    caches = [jax.ShapeDtypeStruct((1, 1, length, HD), jnp.bfloat16)] * 2
    partial = [jax.ShapeDtypeStruct((sp_count, ROWS, HD), jnp.float32)] * 2
    partial.append(jax.ShapeDtypeStruct((sp_count, 1, block_len), jnp.float32))
    results = [jax.ShapeDtypeStruct((1, 1, length), jnp.bfloat16), jax.ShapeDtypeStruct(queries.shape, jnp.bfloat16)]
    return pl.pallas_call(
        functools.partial(read_kernel, pieces, final),
        out_shape=caches + (results if final else partial),
        in_specs=[VMEM, SMEM] + [VMEM] * count + ([VMEM, VMEM, VMEM, ANY, ANY] if final else []),
        out_specs=[ANY, ANY] + [VMEM] * (2 if final else 3),
        scratch_shapes=([pltpu.VMEM(p.shape, p.dtype) for p in partial] if final else [])
        + [
            pltpu.VMEM((count * ROWS, block_len), jnp.float32),
            pltpu.SemaphoreType.DMA((2 * count,)),
        ],
        input_output_aliases={2 + count + 3: 0, 2 + count + 4: 1} if final else {},
        compiler_params=pltpu.CompilerParams(vmem_limit_bytes=32 * 1024 * 1024),
        cost_estimate=pl.CostEstimate(
            flops=64 * count * block_len * HD, bytes_accessed=8 * count * block_len * HD, transcendentals=0
        ),
        name="read",
    )(queries, head_bias, *(pltpu.with_memory_space_constraint(value, pltpu.VMEM) for value in values), *earlier)


def shards(layer_input, input_gain, key_weight, value_weight, stick_offsets, head_bias, queries):
    _, block_len, _ = layer_input.shape
    sp_count = lax.axis_size("sp")
    others = tuple(dict.fromkeys(c for c, _ in ORDER if c != FIRST))

    def pairs(c, k):
        return [(z, ((z // KVH) ^ c) * KVH + ((z % KVH) ^ k)) for z in range(sp_count)]

    args = (layer_input, input_gain, key_weight, value_weight, stick_offsets)
    made = {}
    for k, piece in enumerate(project((FIRST,), *args)):
        made[FIRST, k] = piece
    for i, piece in enumerate(project(others, *args)):
        made[others[i // KVH], i % KVH] = piece
    got = {(0, 0): made[0, 0]}
    for c, k in ORDER:
        got[c, k] = lax.ppermute(made[c, k], "sp", pairs(c, k))
    early = ((0, 0),) + ORDER[:-LATE]
    late = ORDER[-LATE:]
    *caches, totals, mixed, rows = read(early, queries, head_bias, sp_count, block_len, [got[piece] for piece in early])
    return tuple(
        read(
            late,
            queries,
            head_bias,
            sp_count,
            block_len,
            [got[piece] for piece in late],
            (totals, mixed, rows, *caches),
        )
    )


def solution(mesh):
    row = P(("grp", "tp"), "sp", None)
    return jax.shard_map(
        shards,
        mesh=mesh,
        in_specs=(row, P(), P(), P(), P(None, ("grp", "tp"), "sp"), P(), row),
        out_specs=(
            P(("grp", "tp"), "sp", None, None),
            P(("grp", "tp"), "sp", None, None),
            row,
            row,
        ),
        check_vma=False,
    )
```

time: 240 us -> 226 us (0.942)
  starting transfers between devices: 111 us -> 170 us
  waiting for transfers between devices: 64 us -> 29.9 us
  blocking collectives: 24.8 us -> 0 us
  local copies, waits for them, and re-layouts: 9.14 us -> 0.01 us
  other arithmetic: 2.78 us -> 0 us
    ppermute x15, starting transfers between devices: 111 us -> 170 us  [shards(): got[c, k] = lax.ppermute(made[c, k], 'sp', pairs(c, k))]
    ppermute x15, waiting for transfers between devices: 64 us -> 29.9 us  [shards(): got[c, k] = lax.ppermute(made[c, k], 'sp', pairs(c, k))]
    all_to_all x1 -> x0, blocking collectives: 24.8 us -> none  [shards(): lax.all_to_all(offset_parts, 'sp', split_axis=0, concat_axis=0, tiled=True)]
    unnamed x14 -> x4, local copies, waits for them, and re-layouts: 6.7 us -> 0.01 us
    pallas_call x2, Pallas kernels: 10.5 us -> 5.91 us  [read(): pl.pallas_call(functools.partial(read_kernel, pieces, final), out_shape=c...]
    pallas_call x2, Pallas kernels: 15.8 us -> 19.3 us  [project(): pl.pallas_call(functools.partial(project_kernel, classes), out_shape=[pie...]
  transfers between devices with their start and end apart: 15 -> 15, of which waited for: 4 -> 4; matrix products, arithmetic and copies ran while one was open for 3% -> 0% of each run, Pallas kernels for 8% -> 7%
where the time goes in v2:
time: 226 us
  starting transfers between devices  170 us (75%)
  waiting for transfers between devices  29.9 us (13%)
  Pallas kernels  25.2 us (11%)
    ppermute x15, starting transfers between devices, shards(): got[c, k] = lax.ppermute(made[c, k], 'sp', pairs(c, k))  170 us
    ppermute x15, waiting for transfers between devices, shards(): got[c, k] = lax.ppermute(made[c, k], 'sp', pairs(c, k))  29.9 us
    pallas_call x2, Pallas kernels, project(): pl.pallas_call(functools.partial(project_kernel, classes), out_shape=[pie...  19.3 us
    pallas_call x2, Pallas kernels, read(): pl.pallas_call(functools.partial(read_kernel, pieces, final), out_shape=c...  5.91 us
  transfers between devices with their start and end apart: 15, of which 4 were waited for; matrix products, arithmetic and copies ran while one was open for 0% of the time, Pallas kernels for 7%

profile of v2, /device:TPU:36, one launch (start us, length us, event | category | flops | bytes accessed | tf_op | source)
XLA Modules:
  0.0 225.9 jit_solution(3463814791641441208)
XLA Ops:
  0.6 6.4 %project.3 = (bf16[776,128]{1,0:T(8,128)(2,1)S(1)}, bf16[776,128]{1,0:T(8,128)(2,1)S(1)}, bf16[776,128]{1,0:T(8,128)(2,1)S(1)}, bf16[776,128]{1,0:T(8,128)(2,1)S(1)}) custom-call(bf16[4,384,2048]{2,1,0:T(8,128)(2,1)} %x_ref.3, f32[2048]{0:T(1024)} %gain_ref.3, bf16[2048,512]{1,0:T(8,128)(2,1)} %key_ref.3, bf16[2048,512]{1,0:T(8,128)(2,1)} %value_ref.3, ...), custom_call_target="tpu_custom_call" | custom-call | flops 1610612736 | bytes 5767168 | tf_op jit(solution)/shard_map/project/pallas_call | solution.py:104
  7.0 20.8 %collective-permute-start.3 = (bf16[776,128]{1,0:T(8,128)(2,1)S(1)}, bf16[776,128]{1,0:T(8,128)(2,1)S(1)}, u32[]{:S(2)}, u32[]{:S(2)}) collective-permute-start(bf16[776,128]{1,0:T(8,128)(2,1)S(1)} %get-tuple-element.29), channel_id=1, source_target_pairs={{0,64},{8,72},{16,80},{24,88},{32,96},{40,104},{48,112},{56,120},{... | collective-permute-start | bytes 595976 | tf_op jit(solution)/shard_map/ppermute | solution.py:260
  27.8 0.6 collective-permute-start.4
  28.4 11.4 %collective-permute-start.5 = (bf16[776,128]{1,0:T(8,128)(2,1)S(1)}, bf16[776,128]{1,0:T(8,128)(2,1)S(1)}, u32[]{:S(2)}, u32[]{:S(2)}) collective-permute-start(bf16[776,128]{1,0:T(8,128)(2,1)S(1)} %get-tuple-element.31), channel_id=1, source_target_pairs={{0,80},{8,88},{16,64},{24,72},{32,112},{40,120},{48,96},{56,104},{... | collective-permute-start | bytes 595976 | tf_op jit(solution)/shard_map/ppermute | solution.py:260
  39.8 0.0 copy-start
  39.8 0.0 copy-start.1
  39.8 0.0 collective-permute-start.6
  39.8 12.9 %project.2 = (bf16[776,128]{1,0:T(8,128)(2,1)S(1)}, bf16[776,128]{1,0:T(8,128)(2,1)S(1)}, bf16[776,128]{1,0:T(8,128)(2,1)S(1)}, bf16[776,128]{1,0:T(8,128)(2,1)S...) custom-call(bf16[4,384,2048]{2,1,0:T(8,128)(2,1)} %x_ref.3, ...), custom_call_target="tpu_custom_call" | custom-call | flops 4831838208 | bytes 8912896 | tf_op jit(solution)/shard_map/project/pallas_call | solution.py:104
  52.7 5.9 %collective-permute-start.7 = (bf16[776,128]{1,0:T(8,128)(2,1)S(1)}, bf16[776,128]{1,0:T(8,128)(2,1)S(1)}, u32[]{:S(2)}, u32[]{:S(2)}) collective-permute-start(bf16[776,128]{1,0:T(8,128)(2,1)S(1)} %get-tuple-element.33), channel_id=1, source_target_pairs={{0,32},{8,40},{16,48},{24,56},{32,0},{40,8},{48,16},{56,24},{64,96... | collective-permute-start | bytes 595976 | tf_op jit(solution)/shard_map/ppermute | solution.py:260
  58.7 0.0 collective-permute-done.3.rest_1_
  58.7 35.7 %collective-permute-start.8 = (bf16[776,128]{1,0:T(8,128)(2,1)S(1)}, bf16[776,128]{1,0:T(8,128)(2,1)S(1)}, u32[]{:S(2)}, u32[]{:S(2)}) collective-permute-start(bf16[776,128]{1,0:T(8,128)(2,1)S(1)} %get-tuple-element.34), channel_id=1, source_target_pairs={{0,40},{8,32},{16,56},{24,48},{32,8},{40,0},{48,24},{56,16},{64,10... | collective-permute-start | bytes 595976 | tf_op jit(solution)/shard_map/ppermute | solution.py:260
  94.3 0.0 collective-permute-done.4.rest_2_
  94.3 1.3 collective-permute-start.9
  95.7 0.0 collective-permute-done.5.rest_3_
  95.7 15.8 %collective-permute-start.10 = (bf16[776,128]{1,0:T(8,128)(2,1)S(1)}, bf16[776,128]{1,0:T(8,128)(2,1)S(1)}, u32[]{:S(2)}, u32[]{:S(2)}) collective-permute-start(bf16[776,128]{1,0:T(8,128)(2,1)S(1)} %get-tuple-element.36), channel_id=1, source_target_pairs={{0,56},{8,48},{16,40},{24,32},{32,24},{40,16},{48,8},{56,0},{64,12... | collective-permute-start | bytes 595976 | tf_op jit(solution)/shard_map/ppermute | solution.py:260
  111.4 0.0 collective-permute-done.6.rest_4_
  111.4 33.9 %collective-permute-start.11 = (bf16[776,128]{1,0:T(8,128)(2,1)S(1)}, bf16[776,128]{1,0:T(8,128)(2,1)S(1)}, u32[]{:S(2)}, u32[]{:S(2)}) collective-permute-start(bf16[776,128]{1,0:T(8,128)(2,1)S(1)} %get-tuple-element.37), channel_id=1, source_target_pairs={{0,96},{8,104},{16,112},{24,120},{32,64},{40,72},{48,80},{56,88},{... | collective-permute-start | bytes 595976 | tf_op jit(solution)/shard_map/ppermute | solution.py:260
  145.3 8.3 %collective-permute-done.7.rest_5_ = bf16[776,128]{1,0:T(8,128)(2,1)S(1)} collective-permute-done((bf16[776,128]{1,0:T(8,128)(2,1)S(1)}, bf16[776,128]{1,0:T(8,128)(2,1)S(1)}, u32[]{:S(2)}, u32[]{:S(2)}) %collective-permute-start.7) | collective-permute-done | bytes 198688 | tf_op jit(solution)/shard_map/ppermute | solution.py:260
  153.6 0.0 collective-permute-start.12
  153.6 0.0 collective-permute-done.8.rest_6_
  153.6 5.2 %collective-permute-start.13 = (bf16[776,128]{1,0:T(8,128)(2,1)S(1)}, bf16[776,128]{1,0:T(8,128)(2,1)S(1)}, u32[]{:S(2)}, u32[]{:S(2)}) collective-permute-start(bf16[776,128]{1,0:T(8,128)(2,1)S(1)} %get-tuple-element.39), channel_id=1, source_target_pairs={{0,112},{8,120},{16,96},{24,104},{32,80},{40,88},{48,64},{56,72},{... | collective-permute-start | bytes 595976 | tf_op jit(solution)/shard_map/ppermute | solution.py:260
  158.8 0.0 collective-permute-done.9.rest_7_
  158.8 2.3 %collective-permute-start.14 = (bf16[776,128]{1,0:T(8,128)(2,1)S(1)}, bf16[776,128]{1,0:T(8,128)(2,1)S(1)}, u32[]{:S(2)}, u32[]{:S(2)}) collective-permute-start(bf16[776,128]{1,0:T(8,128)(2,1)S(1)} %get-tuple-element.40), channel_id=1, source_target_pairs={{0,120},{8,112},{16,104},{24,96},{32,88},{40,80},{48,72},{56,64},{... | collective-permute-start | bytes 595976 | tf_op jit(solution)/shard_map/ppermute | solution.py:260
  161.1 0.0 collective-permute-done.10.rest_8_
  161.1 0.1 collective-permute-start
  161.3 3.5 %collective-permute-done.11.rest_9_ = bf16[776,128]{1,0:T(8,128)(2,1)S(1)} collective-permute-done((bf16[776,128]{1,0:T(8,128)(2,1)S(1)}, bf16[776,128]{1,0:T(8,128)(2,1)S(1)}, u32[]{:S(2)}, u32[]{:S(2)}) %collective-permute-start.11) | collective-permute-done | bytes 198688 | tf_op jit(solution)/shard_map/ppermute | solution.py:260
  164.8 21.8 %collective-permute-start.1 = (bf16[776,128]{1,0:T(8,128)(2,1)S(1)}, bf16[776,128]{1,0:T(8,128)(2,1)S(1)}, u32[]{:S(2)}, u32[]{:S(2)}) collective-permute-start(bf16[776,128]{1,0:T(8,128)(2,1)S(1)} %get-tuple-element.26), channel_id=1, source_target_pairs={{0,16},{8,24},{16,0},{24,8},{32,48},{40,56},{48,32},{56,40},{64,80... | collective-permute-start | bytes 595976 | tf_op jit(solution)/shard_map/ppermute | solution.py:260
  186.6 8.7 %collective-permute-done.12.rest_10_ = bf16[776,128]{1,0:T(8,128)(2,1)S(1)} collective-permute-done((bf16[776,128]{1,0:T(8,128)(2,1)S(1)}, bf16[776,128]{1,0:T(8,128)(2,1)S(1)}, u32[]{:S(2)}, u32[]{:S(2)}) %collective-permute-start.12) | collective-permute-done | bytes 198688 | tf_op jit(solution)/shard_map/ppermute | solution.py:260
  195.3 15.1 %collective-permute-start.2 = (bf16[776,128]{1,0:T(8,128)(2,1)S(1)}, bf16[776,128]{1,0:T(8,128)(2,1)S(1)}, u32[]{:S(2)}, u32[]{:S(2)}) collective-permute-start(bf16[776,128]{1,0:T(8,128)(2,1)S(1)} %get-tuple-element.27), channel_id=1, source_target_pairs={{0,24},{8,16},{16,8},{24,0},{32,56},{40,48},{48,40},{56,32},{64,88... | collective-permute-start | bytes 595976 | tf_op jit(solution)/shard_map/ppermute | solution.py:260
  210.4 0.0 collective-permute-done.13.rest_11_
  210.4 9.4 %collective-permute-done.14.rest_12_ = bf16[776,128]{1,0:T(8,128)(2,1)S(1)} collective-permute-done((bf16[776,128]{1,0:T(8,128)(2,1)S(1)}, bf16[776,128]{1,0:T(8,128)(2,1)S(1)}, u32[]{:S(2)}, u32[]{:S(2)}) %collective-permute-start.14) | collective-permute-done | bytes 198688 | tf_op jit(solution)/shard_map/ppermute | solution.py:260
  219.8 0.0 copy-done
  219.8 0.0 copy-done.1
  219.8 3.3 %read.2 = (bf16[1,1,6144,128]{3,2,1,0:T(8,128)(2,1)}, bf16[1,1,6144,128]{3,2,1,0:T(8,128)(2,1)}, f32[16,8,128]{2,1,0:T(8,128)S(1)}, f32[16,8,128]{2,1,0:T(8,128)S(1)}, f32[16,1,384]{2,1,0:T(1,128)S(1)}) custom-call(bf16[1,1,512]{2,1,0:T(2,128)(2,1)S(1)} %copy-done, f32[16]{0:T(128)S(1)} %copy-done.1, bf16[776,128]{1,0:T(8,128)(2,1)S(1)} %get-tuple-element.28.rest_0_, ...), custom_call_target="tpu_custom_call" | custom-call | flops 40894464 | bytes 5111808 | tf_op jit(solution)/shard_map/read/pallas_call | solution.py:225
  223.1 0.0 collective-permute-done.rest_0_
  223.1 0.0 collective-permute-done.1.rest_1_
  223.1 0.0 collective-permute-done.2.rest_2_
  223.1 2.6 %read.3 = (bf16[1,1,6144,128]{3,2,1,0:T(8,128)(2,1)}, bf16[1,1,6144,128]{3,2,1,0:T(8,128)(2,1)}, bf16[1,1,6144]{2,1,0:T(2,128)(2,1)}, bf16[1,1,512]{2,1,0:T(2,128)(2,1)}) custom-call(bf16[1,1,512]{2,1,0:T(2,128)(2,1)S(1)} %copy-done, f32[16]{0:T(128)S(1)} %copy-done.1, ...), custom_call_target="tpu_custom_call", output_to_operand_aliasing={{0}: (8, {}), {1}: (9, {})} | custom-call | flops 9437184 | bytes 1179648 | tf_op jit(solution)/shard_map/read/pallas_call | solution.py:225
Async XLA Ops:
  7.0 51.7 %collective-permute-start.3 = (bf16[776,128]{1,0:T(8,128)(2,1)S(1)}, bf16[776,128]{1,0:T(8,128)(2,1)S(1)}, u32[]{:S(2)}, u32[]{:S(2)}) collective-permute-start(bf16[776,128]{1,0:T(8,128)(2,1)S(1)} %get-tuple-element.29), channel_id=1, source_target_pairs={{0,64},{8,72},{16,80},{24,88},{32,96},{40,104},{48,112},{56,120},{... | collective-permute-start | bytes 595976 | tf_op jit(solution)/shard_map/ppermute | solution.py:260
  27.8 66.5 %collective-permute-start.4 = (bf16[776,128]{1,0:T(8,128)(2,1)S(1)}, bf16[776,128]{1,0:T(8,128)(2,1)S(1)}, u32[]{:S(2)}, u32[]{:S(2)}) collective-permute-start(bf16[776,128]{1,0:T(8,128)(2,1)S(1)} %get-tuple-element.30), channel_id=1, source_target_pairs={{0,72},{8,64},{16,88},{24,80},{32,104},{40,96},{48,120},{56,112},{... | collective-permute-start | bytes 595976 | tf_op jit(solution)/shard_map/ppermute | solution.py:260
  28.4 67.3 %collective-permute-start.5 = (bf16[776,128]{1,0:T(8,128)(2,1)S(1)}, bf16[776,128]{1,0:T(8,128)(2,1)S(1)}, u32[]{:S(2)}, u32[]{:S(2)}) collective-permute-start(bf16[776,128]{1,0:T(8,128)(2,1)S(1)} %get-tuple-element.31), channel_id=1, source_target_pairs={{0,80},{8,88},{16,64},{24,72},{32,112},{40,120},{48,96},{56,104},{... | collective-permute-start | bytes 595976 | tf_op jit(solution)/shard_map/ppermute | solution.py:260
  39.8 180.0 %copy-start = (bf16[1,1,512]{2,1,0:T(2,128)(2,1)S(1)}, bf16[1,1,512]{2,1,0:T(2,128)(2,1)}, u32[]{:S(2)}) copy-start(bf16[1,1,512]{2,1,0:T(2,128)(2,1)} %q_ref.3) | copy-start | bytes 3076
  39.8 180.0 %copy-start.1 = (f32[16]{0:T(128)S(1)}, f32[16]{0:T(128)}, u32[]{:S(2)}) copy-start(f32[16]{0:T(128)} %bias_ref.3) | copy-start | bytes 196
  39.8 71.6 %collective-permute-start.6 = (bf16[776,128]{1,0:T(8,128)(2,1)S(1)}, bf16[776,128]{1,0:T(8,128)(2,1)S(1)}, u32[]{:S(2)}, u32[]{:S(2)}) collective-permute-start(bf16[776,128]{1,0:T(8,128)(2,1)S(1)} %get-tuple-element.32), channel_id=1, source_target_pairs={{0,88},{8,80},{16,72},{24,64},{32,120},{40,112},{48,104},{56,96},{... | collective-permute-start | bytes 595976 | tf_op jit(solution)/shard_map/ppermute | solution.py:260
  52.7 100.9 %collective-permute-start.7 = (bf16[776,128]{1,0:T(8,128)(2,1)S(1)}, bf16[776,128]{1,0:T(8,128)(2,1)S(1)}, u32[]{:S(2)}, u32[]{:S(2)}) collective-permute-start(bf16[776,128]{1,0:T(8,128)(2,1)S(1)} %get-tuple-element.33), channel_id=1, source_target_pairs={{0,32},{8,40},{16,48},{24,56},{32,0},{40,8},{48,16},{56,24},{64,96... | collective-permute-start | bytes 595976 | tf_op jit(solution)/shard_map/ppermute | solution.py:260
  58.7 94.9 %collective-permute-start.8 = (bf16[776,128]{1,0:T(8,128)(2,1)S(1)}, bf16[776,128]{1,0:T(8,128)(2,1)S(1)}, u32[]{:S(2)}, u32[]{:S(2)}) collective-permute-start(bf16[776,128]{1,0:T(8,128)(2,1)S(1)} %get-tuple-element.34), channel_id=1, source_target_pairs={{0,40},{8,32},{16,56},{24,48},{32,8},{40,0},{48,24},{56,16},{64,10... | collective-permute-start | bytes 595976 | tf_op jit(solution)/shard_map/ppermute | solution.py:260
  94.3 64.5 %collective-permute-start.9 = (bf16[776,128]{1,0:T(8,128)(2,1)S(1)}, bf16[776,128]{1,0:T(8,128)(2,1)S(1)}, u32[]{:S(2)}, u32[]{:S(2)}) collective-permute-start(bf16[776,128]{1,0:T(8,128)(2,1)S(1)} %get-tuple-element.35), channel_id=1, source_target_pairs={{0,48},{8,56},{16,32},{24,40},{32,16},{40,24},{48,0},{56,8},{64,11... | collective-permute-start | bytes 595976 | tf_op jit(solution)/shard_map/ppermute | solution.py:260
  95.7 65.5 %collective-permute-start.10 = (bf16[776,128]{1,0:T(8,128)(2,1)S(1)}, bf16[776,128]{1,0:T(8,128)(2,1)S(1)}, u32[]{:S(2)}, u32[]{:S(2)}) collective-permute-start(bf16[776,128]{1,0:T(8,128)(2,1)S(1)} %get-tuple-element.36), channel_id=1, source_target_pairs={{0,56},{8,48},{16,40},{24,32},{32,24},{40,16},{48,8},{56,0},{64,12... | collective-permute-start | bytes 595976 | tf_op jit(solution)/shard_map/ppermute | solution.py:260
  111.4 53.3 %collective-permute-start.11 = (bf16[776,128]{1,0:T(8,128)(2,1)S(1)}, bf16[776,128]{1,0:T(8,128)(2,1)S(1)}, u32[]{:S(2)}, u32[]{:S(2)}) collective-permute-start(bf16[776,128]{1,0:T(8,128)(2,1)S(1)} %get-tuple-element.37), channel_id=1, source_target_pairs={{0,96},{8,104},{16,112},{24,120},{32,64},{40,72},{48,80},{56,88},{... | collective-permute-start | bytes 595976 | tf_op jit(solution)/shard_map/ppermute | solution.py:260
  153.6 41.7 %collective-permute-start.12 = (bf16[776,128]{1,0:T(8,128)(2,1)S(1)}, bf16[776,128]{1,0:T(8,128)(2,1)S(1)}, u32[]{:S(2)}, u32[]{:S(2)}) collective-permute-start(bf16[776,128]{1,0:T(8,128)(2,1)S(1)} %get-tuple-element.38), channel_id=1, source_target_pairs={{0,104},{8,96},{16,120},{24,112},{32,72},{40,64},{48,88},{56,80},{... | collective-permute-start | bytes 595976 | tf_op jit(solution)/shard_map/ppermute | solution.py:260
  153.6 56.8 %collective-permute-start.13 = (bf16[776,128]{1,0:T(8,128)(2,1)S(1)}, bf16[776,128]{1,0:T(8,128)(2,1)S(1)}, u32[]{:S(2)}, u32[]{:S(2)}) collective-permute-start(bf16[776,128]{1,0:T(8,128)(2,1)S(1)} %get-tuple-element.39), channel_id=1, source_target_pairs={{0,112},{8,120},{16,96},{24,104},{32,80},{40,88},{48,64},{56,72},{... | collective-permute-start | bytes 595976 | tf_op jit(solution)/shard_map/ppermute | solution.py:260
  158.8 61.0 %collective-permute-start.14 = (bf16[776,128]{1,0:T(8,128)(2,1)S(1)}, bf16[776,128]{1,0:T(8,128)(2,1)S(1)}, u32[]{:S(2)}, u32[]{:S(2)}) collective-permute-start(bf16[776,128]{1,0:T(8,128)(2,1)S(1)} %get-tuple-element.40), channel_id=1, source_target_pairs={{0,120},{8,112},{16,104},{24,96},{32,88},{40,80},{48,72},{56,64},{... | collective-permute-start | bytes 595976 | tf_op jit(solution)/shard_map/ppermute | solution.py:260
  161.1 62.0 %collective-permute-start = (bf16[776,128]{1,0:T(8,128)(2,1)S(1)}, bf16[776,128]{1,0:T(8,128)(2,1)S(1)}, u32[]{:S(2)}, u32[]{:S(2)}) collective-permute-start(bf16[776,128]{1,0:T(8,128)(2,1)S(1)} %get-tuple-element.25), channel_id=1, source_target_pairs={{0,8},{8,0},{16,24},{24,16},{32,40},{40,32},{48,56},{56,48},{64,72... | collective-permute-start | bytes 595976 | tf_op jit(solution)/shard_map/ppermute | solution.py:260
  164.8 58.3 %collective-permute-start.1 = (bf16[776,128]{1,0:T(8,128)(2,1)S(1)}, bf16[776,128]{1,0:T(8,128)(2,1)S(1)}, u32[]{:S(2)}, u32[]{:S(2)}) collective-permute-start(bf16[776,128]{1,0:T(8,128)(2,1)S(1)} %get-tuple-element.26), channel_id=1, source_target_pairs={{0,16},{8,24},{16,0},{24,8},{32,48},{40,56},{48,32},{56,40},{64,80... | collective-permute-start | bytes 595976 | tf_op jit(solution)/shard_map/ppermute | solution.py:260
  195.3 27.9 %collective-permute-start.2 = (bf16[776,128]{1,0:T(8,128)(2,1)S(1)}, bf16[776,128]{1,0:T(8,128)(2,1)S(1)}, u32[]{:S(2)}, u32[]{:S(2)}) collective-permute-start(bf16[776,128]{1,0:T(8,128)(2,1)S(1)} %get-tuple-element.27), channel_id=1, source_target_pairs={{0,24},{8,16},{16,8},{24,0},{32,56},{40,48},{48,40},{56,32},{64,88... | collective-permute-start | bytes 595976 | tf_op jit(solution)/shard_map/ppermute | solution.py:260

commit v3 on v2

--- a/solution.py
+++ b/solution.py
@@ -17,8 +17,13 @@
 ROWS = 8
 EXTRA = 8
 
-ORDER = tuple((c, k) for c in (2, 1, 3, 0) for k in range(KVH) if c or k)
-FIRST = ORDER[0][0]
+ORDER = (
+    tuple((2, k) for k in (0, 1, 3, 2))
+    + tuple((c, k) for k in (0, 1, 3, 2) for c in (1, 3))
+    + tuple((0, k) for k in (1, 3, 2))
+)
+LEAD = (2,)
+FOLLOW = (1, 3, 0)
 LATE = 3
 
 ANY = pl.BlockSpec(memory_space=pltpu.HBM)
@@ -28,17 +33,18 @@
 
 def split_index():
     z = lax.axis_index("sp")
-    return lax.div(z, KVH), lax.rem(z, KVH)
+    return lax.div(z, KVH), lax.rem(z, KVH), lax.axis_size("sp") // KVH
 
 
 def project_kernel(classes, x_ref, gain_ref, key_ref, value_ref, offset_ref, *rest):
     count = len(classes)
     outs = rest[: count * KVH]
     rows, wk, wv, gains, offsets, normed, parts, x_sems, w_sems, o_sems = rest[count * KVH :]
-    group, member = split_index()
+    group, member, groups = split_index()
+    prompts = [lax.rem(group + c, groups) for c in classes]
     block_len = x_ref.shape[1]
     loads = [
-        pltpu.make_async_copy(x_ref.at[group ^ c], rows.at[n], x_sems.at[n]) for n, c in enumerate(classes)
+        pltpu.make_async_copy(x_ref.at[prompts[n]], rows.at[n], x_sems.at[n]) for n in range(count)
     ]
     weights = [
         pltpu.make_async_copy(key_ref, wk, w_sems.at[0]),
@@ -60,10 +66,10 @@
     gain = gains[...].reshape(1, -1)
     line = lax.broadcasted_iota(jnp.int32, (EXTRA, HD), 0)
     prompt = lax.broadcasted_iota(jnp.int32, (x_ref.shape[0], 1), 0)
-    for n, c in enumerate(classes):
+    for n in range(count):
         for h in range(KVH):
             own = offsets[h].astype(jnp.float32)
-            own = jnp.sum(jnp.where(prompt == (group ^ c), own, 0.0), axis=0, keepdims=True)
+            own = jnp.sum(jnp.where(prompt == prompts[n], own, 0.0), axis=0, keepdims=True)
             extra = jnp.zeros((EXTRA, HD), jnp.float32)
             for j in range(block_len // HD):
                 extra = jnp.where(line == j, own[:, j * HD : (j + 1) * HD], extra)
@@ -145,8 +151,8 @@
         rest = rest[5:]
     scores, out_sems = rest
     block_len = rows.shape[2]
-    group, member = split_index()
-    blocks = [(group ^ c) * KVH + (member ^ k) for c, k in pieces]
+    group, member, groups = split_index()
+    blocks = [lax.rem(group + groups - c, groups) * KVH + (member ^ k) for c, k in pieces]
     stores = []
     for i in range(count):
         place = pl.ds(pl.multiple_of(blocks[i] * block_len, block_len), block_len)
@@ -244,17 +250,16 @@
 def shards(layer_input, input_gain, key_weight, value_weight, stick_offsets, head_bias, queries):
     _, block_len, _ = layer_input.shape
     sp_count = lax.axis_size("sp")
-    others = tuple(dict.fromkeys(c for c, _ in ORDER if c != FIRST))
+    groups = sp_count // KVH
 
     def pairs(c, k):
-        return [(z, ((z // KVH) ^ c) * KVH + ((z % KVH) ^ k)) for z in range(sp_count)]
+        return [(z, (z // KVH + c) % groups * KVH + (z % KVH ^ k)) for z in range(sp_count)]
 
     args = (layer_input, input_gain, key_weight, value_weight, stick_offsets)
     made = {}
-    for k, piece in enumerate(project((FIRST,), *args)):
-        made[FIRST, k] = piece
-    for i, piece in enumerate(project(others, *args)):
-        made[others[i // KVH], i % KVH] = piece
+    for classes in (LEAD, FOLLOW):
+        for i, piece in enumerate(project(classes, *args)):
+            made[classes[i // KVH], i % KVH] = piece
     got = {(0, 0): made[0, 0]}
     for c, k in ORDER:
         got[c, k] = lax.ppermute(made[c, k], "sp", pairs(c, k))

time: 226 us -> 192 us (0.85)
  starting transfers between devices: 170 us -> 110 us
  waiting for transfers between devices: 29.9 us -> 55.9 us
    ppermute x15, starting transfers between devices: 170 us -> 110 us  [shards(): got[c, k] = lax.ppermute(made[c, k], 'sp', pairs(c, k))]
    ppermute x15, waiting for transfers between devices: 29.9 us -> 55.9 us  [shards(): got[c, k] = lax.ppermute(made[c, k], 'sp', pairs(c, k))]
  transfers between devices with their start and end apart: 15 -> 15, of which waited for: 4 -> 6; matrix products, arithmetic and copies ran while one was open for 0% -> 0% of each run, Pallas kernels for 7% -> 8%
where the time goes in v3:
time: 192 us
  starting transfers between devices  110 us (57%)
  waiting for transfers between devices  55.9 us (29%)
  Pallas kernels  25.2 us (13%)
    ppermute x15, starting transfers between devices, shards(): got[c, k] = lax.ppermute(made[c, k], 'sp', pairs(c, k))  110 us
    ppermute x15, waiting for transfers between devices, shards(): got[c, k] = lax.ppermute(made[c, k], 'sp', pairs(c, k))  55.9 us
    pallas_call x2, Pallas kernels, project(): pl.pallas_call(functools.partial(project_kernel, classes), out_shape=[pie...  19.3 us
    pallas_call x2, Pallas kernels, read(): pl.pallas_call(functools.partial(read_kernel, pieces, final), out_shape=c...  5.93 us
  transfers between devices with their start and end apart: 15, of which 6 were waited for; matrix products, arithmetic and copies ran while one was open for 0% of the time, Pallas kernels for 8%

profile of v3, /device:TPU:36, one launch (start us, length us, event | category | flops | bytes accessed | tf_op | source)
XLA Modules:
  0.0 191.8 jit_solution(5857121541185606558)
XLA Ops:
  0.6 6.4 %project.3 = (bf16[776,128]{1,0:T(8,128)(2,1)S(1)}, bf16[776,128]{1,0:T(8,128)(2,1)S(1)}, bf16[776,128]{1,0:T(8,128)(2,1)S(1)}, bf16[776,128]{1,0:T(8,128)(2,1)S(1)}) custom-call(bf16[4,384,2048]{2,1,0:T(8,128)(2,1)} %x_ref.3, f32[2048]{0:T(1024)} %gain_ref.3, bf16[2048,512]{1,0:T(8,128)(2,1)} %key_ref.3, bf16[2048,512]{1,0:T(8,128)(2,1)} %value_ref.3, ...), custom_call_target="tpu_custom_call" | custom-call | flops 1610612736 | bytes 5767168 | tf_op jit(solution)/shard_map/project/pallas_call | solution.py:110
  7.0 20.8 %collective-permute-start.3 = (bf16[776,128]{1,0:T(8,128)(2,1)S(1)}, bf16[776,128]{1,0:T(8,128)(2,1)S(1)}, u32[]{:S(2)}, u32[]{:S(2)}) collective-permute-start(bf16[776,128]{1,0:T(8,128)(2,1)S(1)} %get-tuple-element.29), channel_id=1, source_target_pairs={{0,64},{8,72},{16,80},{24,88},{32,96},{40,104},{48,112},{56,120},{... | collective-permute-start | bytes 595976 | tf_op jit(solution)/shard_map/ppermute | solution.py:265
  27.8 0.6 collective-permute-start.4
  28.4 10.1 %collective-permute-start.5 = (bf16[776,128]{1,0:T(8,128)(2,1)S(1)}, bf16[776,128]{1,0:T(8,128)(2,1)S(1)}, u32[]{:S(2)}, u32[]{:S(2)}) collective-permute-start(bf16[776,128]{1,0:T(8,128)(2,1)S(1)} %get-tuple-element.31), channel_id=1, source_target_pairs={{0,88},{8,80},{16,72},{24,64},{32,120},{40,112},{48,104},{56,96},{... | collective-permute-start | bytes 595976 | tf_op jit(solution)/shard_map/ppermute | solution.py:265
  38.5 0.0 copy-start
  38.5 0.0 copy-start.1
  38.5 1.3 collective-permute-start.6
  39.8 12.9 %project.2 = (bf16[776,128]{1,0:T(8,128)(2,1)S(1)}, bf16[776,128]{1,0:T(8,128)(2,1)S(1)}, bf16[776,128]{1,0:T(8,128)(2,1)S(1)}, bf16[776,128]{1,0:T(8,128)(2,1)S...) custom-call(bf16[4,384,2048]{2,1,0:T(8,128)(2,1)} %x_ref.3, ...), custom_call_target="tpu_custom_call" | custom-call | flops 4831838208 | bytes 8912896 | tf_op jit(solution)/shard_map/project/pallas_call | solution.py:110
  52.8 5.9 %collective-permute-start.7 = (bf16[776,128]{1,0:T(8,128)(2,1)S(1)}, bf16[776,128]{1,0:T(8,128)(2,1)S(1)}, u32[]{:S(2)}, u32[]{:S(2)}) collective-permute-start(bf16[776,128]{1,0:T(8,128)(2,1)S(1)} %get-tuple-element.33), channel_id=1, source_target_pairs={{0,32},{8,40},{16,48},{24,56},{32,64},{40,72},{48,80},{56,88},{64,... | collective-permute-start | bytes 595976 | tf_op jit(solution)/shard_map/ppermute | solution.py:265
  58.7 0.0 collective-permute-done.3.rest_1_
  58.7 12.7 %collective-permute-start.8 = (bf16[776,128]{1,0:T(8,128)(2,1)S(1)}, bf16[776,128]{1,0:T(8,128)(2,1)S(1)}, u32[]{:S(2)}, u32[]{:S(2)}) collective-permute-start(bf16[776,128]{1,0:T(8,128)(2,1)S(1)} %get-tuple-element.34), channel_id=1, source_target_pairs={{0,96},{8,104},{16,112},{24,120},{32,0},{40,8},{48,16},{56,24},{64... | collective-permute-start | bytes 595976 | tf_op jit(solution)/shard_map/ppermute | solution.py:265
  71.4 21.3 %collective-permute-done.4.rest_2_ = bf16[776,128]{1,0:T(8,128)(2,1)S(1)} collective-permute-done((bf16[776,128]{1,0:T(8,128)(2,1)S(1)}, bf16[776,128]{1,0:T(8,128)(2,1)S(1)}, u32[]{:S(2)}, u32[]{:S(2)}) %collective-permute-start.4) | collective-permute-done | bytes 198688 | tf_op jit(solution)/shard_map/ppermute | solution.py:265
  92.8 6.3 %collective-permute-start.9 = (bf16[776,128]{1,0:T(8,128)(2,1)S(1)}, bf16[776,128]{1,0:T(8,128)(2,1)S(1)}, u32[]{:S(2)}, u32[]{:S(2)}) collective-permute-start(bf16[776,128]{1,0:T(8,128)(2,1)S(1)} %get-tuple-element.35), channel_id=1, source_target_pairs={{0,40},{8,32},{16,56},{24,48},{32,72},{40,64},{48,88},{56,80},{64,... | collective-permute-start | bytes 595976 | tf_op jit(solution)/shard_map/ppermute | solution.py:265
  99.1 0.0 collective-permute-done.5.rest_3_
  99.1 5.3 %collective-permute-start.10 = (bf16[776,128]{1,0:T(8,128)(2,1)S(1)}, bf16[776,128]{1,0:T(8,128)(2,1)S(1)}, u32[]{:S(2)}, u32[]{:S(2)}) collective-permute-start(bf16[776,128]{1,0:T(8,128)(2,1)S(1)} %get-tuple-element.36), channel_id=1, source_target_pairs={{0,104},{8,96},{16,120},{24,112},{32,8},{40,0},{48,24},{56,16},{64... | collective-permute-start | bytes 595976 | tf_op jit(solution)/shard_map/ppermute | solution.py:265
  104.4 2.8 %collective-permute-done.6.rest_4_ = bf16[776,128]{1,0:T(8,128)(2,1)S(1)} collective-permute-done((bf16[776,128]{1,0:T(8,128)(2,1)S(1)}, bf16[776,128]{1,0:T(8,128)(2,1)S(1)}, u32[]{:S(2)}, u32[]{:S(2)}) %collective-permute-start.6) | collective-permute-done | bytes 198688 | tf_op jit(solution)/shard_map/ppermute | solution.py:265
  107.2 22.5 %collective-permute-start.11 = (bf16[776,128]{1,0:T(8,128)(2,1)S(1)}, bf16[776,128]{1,0:T(8,128)(2,1)S(1)}, u32[]{:S(2)}, u32[]{:S(2)}) collective-permute-start(bf16[776,128]{1,0:T(8,128)(2,1)S(1)} %get-tuple-element.37), channel_id=1, source_target_pairs={{0,56},{8,48},{16,40},{24,32},{32,88},{40,80},{48,72},{56,64},{64,... | collective-permute-start | bytes 595976 | tf_op jit(solution)/shard_map/ppermute | solution.py:265
  129.7 0.0 collective-permute-done.7.rest_5_
  129.7 0.0 collective-permute-start.12
  129.7 0.0 collective-permute-done.8.rest_6_
  129.7 3.7 %collective-permute-start.13 = (bf16[776,128]{1,0:T(8,128)(2,1)S(1)}, bf16[776,128]{1,0:T(8,128)(2,1)S(1)}, u32[]{:S(2)}, u32[]{:S(2)}) collective-permute-start(bf16[776,128]{1,0:T(8,128)(2,1)S(1)} %get-tuple-element.39), channel_id=1, source_target_pairs={{0,48},{8,56},{16,32},{24,40},{32,80},{40,88},{48,64},{56,72},{64,... | collective-permute-start | bytes 595976 | tf_op jit(solution)/shard_map/ppermute | solution.py:265
  133.4 0.0 collective-permute-done.9.rest_7_
  133.4 0.5 collective-permute-start.14
  133.9 0.0 collective-permute-done.10.rest_8_
  133.9 14.8 %collective-permute-start = (bf16[776,128]{1,0:T(8,128)(2,1)S(1)}, bf16[776,128]{1,0:T(8,128)(2,1)S(1)}, u32[]{:S(2)}, u32[]{:S(2)}) collective-permute-start(bf16[776,128]{1,0:T(8,128)(2,1)S(1)} %get-tuple-element.25), channel_id=1, source_target_pairs={{0,8},{8,0},{16,24},{24,16},{32,40},{40,32},{48,56},{56,48},{64,72... | collective-permute-start | bytes 595976 | tf_op jit(solution)/shard_map/ppermute | solution.py:265
  148.8 12.0 %collective-permute-done.11.rest_9_ = bf16[776,128]{1,0:T(8,128)(2,1)S(1)} collective-permute-done((bf16[776,128]{1,0:T(8,128)(2,1)S(1)}, bf16[776,128]{1,0:T(8,128)(2,1)S(1)}, u32[]{:S(2)}, u32[]{:S(2)}) %collective-permute-start.11) | collective-permute-done | bytes 198688 | tf_op jit(solution)/shard_map/ppermute | solution.py:265
  160.8 1.2 collective-permute-start.1
  162.0 0.0 collective-permute-done.12.rest_10_
  162.0 3.9 %collective-permute-start.2 = (bf16[776,128]{1,0:T(8,128)(2,1)S(1)}, bf16[776,128]{1,0:T(8,128)(2,1)S(1)}, u32[]{:S(2)}, u32[]{:S(2)}) collective-permute-start(bf16[776,128]{1,0:T(8,128)(2,1)S(1)} %get-tuple-element.27), channel_id=1, source_target_pairs={{0,16},{8,24},{16,0},{24,8},{32,48},{40,56},{48,32},{56,40},{64,80... | collective-permute-start | bytes 595976 | tf_op jit(solution)/shard_map/ppermute | solution.py:265
  165.9 0.0 collective-permute-done.13.rest_11_
  165.9 0.0 collective-permute-done.14.rest_12_
  165.9 0.0 copy-done
  165.9 0.0 copy-done.1
  165.9 3.3 %read.2 = (bf16[1,1,6144,128]{3,2,1,0:T(8,128)(2,1)}, bf16[1,1,6144,128]{3,2,1,0:T(8,128)(2,1)}, f32[16,8,128]{2,1,0:T(8,128)S(1)}, f32[16,8,128]{2,1,0:T(8,128)S(1)}, f32[16,1,384]{2,1,0:T(1,128)S(1)}) custom-call(bf16[1,1,512]{2,1,0:T(2,128)(2,1)S(1)} %copy-done, f32[16]{0:T(128)S(1)} %copy-done.1, bf16[776,128]{1,0:T(8,128)(2,1)S(1)} %get-tuple-element.28.rest_0_, ...), custom_call_target="tpu_custom_call" | custom-call | flops 40894464 | bytes 5111808 | tf_op jit(solution)/shard_map/read/pallas_call | solution.py:231
  169.3 2.1 %collective-permute-done.rest_0_ = bf16[776,128]{1,0:T(8,128)(2,1)S(1)} collective-permute-done((bf16[776,128]{1,0:T(8,128)(2,1)S(1)}, bf16[776,128]{1,0:T(8,128)(2,1)S(1)}, u32[]{:S(2)}, u32[]{:S(2)}) %collective-permute-start) | collective-permute-done | bytes 198688 | tf_op jit(solution)/shard_map/ppermute | solution.py:265
  171.4 10.2 %collective-permute-done.1.rest_1_ = bf16[776,128]{1,0:T(8,128)(2,1)S(1)} collective-permute-done((bf16[776,128]{1,0:T(8,128)(2,1)S(1)}, bf16[776,128]{1,0:T(8,128)(2,1)S(1)}, u32[]{:S(2)}, u32[]{:S(2)}) %collective-permute-start.1) | collective-permute-done | bytes 198688 | tf_op jit(solution)/shard_map/ppermute | solution.py:265
  181.6 7.5 %collective-permute-done.2.rest_2_ = bf16[776,128]{1,0:T(8,128)(2,1)S(1)} collective-permute-done((bf16[776,128]{1,0:T(8,128)(2,1)S(1)}, bf16[776,128]{1,0:T(8,128)(2,1)S(1)}, u32[]{:S(2)}, u32[]{:S(2)}) %collective-permute-start.2) | collective-permute-done | bytes 198688 | tf_op jit(solution)/shard_map/ppermute | solution.py:265
  189.0 2.6 %read.3 = (bf16[1,1,6144,128]{3,2,1,0:T(8,128)(2,1)}, bf16[1,1,6144,128]{3,2,1,0:T(8,128)(2,1)}, bf16[1,1,6144]{2,1,0:T(2,128)(2,1)}, bf16[1,1,512]{2,1,0:T(2,128)(2,1)}) custom-call(bf16[1,1,512]{2,1,0:T(2,128)(2,1)S(1)} %copy-done, f32[16]{0:T(128)S(1)} %copy-done.1, ...), custom_call_target="tpu_custom_call", output_to_operand_aliasing={{0}: (8, {}), {1}: (9, {})} | custom-call | flops 9437184 | bytes 1179648 | tf_op jit(solution)/shard_map/read/pallas_call | solution.py:231
Async XLA Ops:
  7.0 51.7 %collective-permute-start.3 = (bf16[776,128]{1,0:T(8,128)(2,1)S(1)}, bf16[776,128]{1,0:T(8,128)(2,1)S(1)}, u32[]{:S(2)}, u32[]{:S(2)}) collective-permute-start(bf16[776,128]{1,0:T(8,128)(2,1)S(1)} %get-tuple-element.29), channel_id=1, source_target_pairs={{0,64},{8,72},{16,80},{24,88},{32,96},{40,104},{48,112},{56,120},{... | collective-permute-start | bytes 595976 | tf_op jit(solution)/shard_map/ppermute | solution.py:265
  27.8 65.0 %collective-permute-start.4 = (bf16[776,128]{1,0:T(8,128)(2,1)S(1)}, bf16[776,128]{1,0:T(8,128)(2,1)S(1)}, u32[]{:S(2)}, u32[]{:S(2)}) collective-permute-start(bf16[776,128]{1,0:T(8,128)(2,1)S(1)} %get-tuple-element.30), channel_id=1, source_target_pairs={{0,72},{8,64},{16,88},{24,80},{32,104},{40,96},{48,120},{56,112},{... | collective-permute-start | bytes 595976 | tf_op jit(solution)/shard_map/ppermute | solution.py:265
  28.4 70.7 %collective-permute-start.5 = (bf16[776,128]{1,0:T(8,128)(2,1)S(1)}, bf16[776,128]{1,0:T(8,128)(2,1)S(1)}, u32[]{:S(2)}, u32[]{:S(2)}) collective-permute-start(bf16[776,128]{1,0:T(8,128)(2,1)S(1)} %get-tuple-element.31), channel_id=1, source_target_pairs={{0,88},{8,80},{16,72},{24,64},{32,120},{40,112},{48,104},{56,96},{... | collective-permute-start | bytes 595976 | tf_op jit(solution)/shard_map/ppermute | solution.py:265
  38.5 127.4 %copy-start = (bf16[1,1,512]{2,1,0:T(2,128)(2,1)S(1)}, bf16[1,1,512]{2,1,0:T(2,128)(2,1)}, u32[]{:S(2)}) copy-start(bf16[1,1,512]{2,1,0:T(2,128)(2,1)} %q_ref.3) | copy-start | bytes 3076
  38.5 127.4 %copy-start.1 = (f32[16]{0:T(128)S(1)}, f32[16]{0:T(128)}, u32[]{:S(2)}) copy-start(f32[16]{0:T(128)} %bias_ref.3) | copy-start | bytes 196
  38.5 68.7 %collective-permute-start.6 = (bf16[776,128]{1,0:T(8,128)(2,1)S(1)}, bf16[776,128]{1,0:T(8,128)(2,1)S(1)}, u32[]{:S(2)}, u32[]{:S(2)}) collective-permute-start(bf16[776,128]{1,0:T(8,128)(2,1)S(1)} %get-tuple-element.32), channel_id=1, source_target_pairs={{0,80},{8,88},{16,64},{24,72},{32,112},{40,120},{48,96},{56,104},{... | collective-permute-start | bytes 595976 | tf_op jit(solution)/shard_map/ppermute | solution.py:265
  52.8 76.9 %collective-permute-start.7 = (bf16[776,128]{1,0:T(8,128)(2,1)S(1)}, bf16[776,128]{1,0:T(8,128)(2,1)S(1)}, u32[]{:S(2)}, u32[]{:S(2)}) collective-permute-start(bf16[776,128]{1,0:T(8,128)(2,1)S(1)} %get-tuple-element.33), channel_id=1, source_target_pairs={{0,32},{8,40},{16,48},{24,56},{32,64},{40,72},{48,80},{56,88},{64,... | collective-permute-start | bytes 595976 | tf_op jit(solution)/shard_map/ppermute | solution.py:265
  58.7 71.0 %collective-permute-start.8 = (bf16[776,128]{1,0:T(8,128)(2,1)S(1)}, bf16[776,128]{1,0:T(8,128)(2,1)S(1)}, u32[]{:S(2)}, u32[]{:S(2)}) collective-permute-start(bf16[776,128]{1,0:T(8,128)(2,1)S(1)} %get-tuple-element.34), channel_id=1, source_target_pairs={{0,96},{8,104},{16,112},{24,120},{32,0},{40,8},{48,16},{56,24},{64... | collective-permute-start | bytes 595976 | tf_op jit(solution)/shard_map/ppermute | solution.py:265
  92.8 40.6 %collective-permute-start.9 = (bf16[776,128]{1,0:T(8,128)(2,1)S(1)}, bf16[776,128]{1,0:T(8,128)(2,1)S(1)}, u32[]{:S(2)}, u32[]{:S(2)}) collective-permute-start(bf16[776,128]{1,0:T(8,128)(2,1)S(1)} %get-tuple-element.35), channel_id=1, source_target_pairs={{0,40},{8,32},{16,56},{24,48},{32,72},{40,64},{48,88},{56,80},{64,... | collective-permute-start | bytes 595976 | tf_op jit(solution)/shard_map/ppermute | solution.py:265
  99.1 34.8 %collective-permute-start.10 = (bf16[776,128]{1,0:T(8,128)(2,1)S(1)}, bf16[776,128]{1,0:T(8,128)(2,1)S(1)}, u32[]{:S(2)}, u32[]{:S(2)}) collective-permute-start(bf16[776,128]{1,0:T(8,128)(2,1)S(1)} %get-tuple-element.36), channel_id=1, source_target_pairs={{0,104},{8,96},{16,120},{24,112},{32,8},{40,0},{48,24},{56,16},{64... | collective-permute-start | bytes 595976 | tf_op jit(solution)/shard_map/ppermute | solution.py:265
  107.2 53.6 %collective-permute-start.11 = (bf16[776,128]{1,0:T(8,128)(2,1)S(1)}, bf16[776,128]{1,0:T(8,128)(2,1)S(1)}, u32[]{:S(2)}, u32[]{:S(2)}) collective-permute-start(bf16[776,128]{1,0:T(8,128)(2,1)S(1)} %get-tuple-element.37), channel_id=1, source_target_pairs={{0,56},{8,48},{16,40},{24,32},{32,88},{40,80},{48,72},{56,64},{64,... | collective-permute-start | bytes 595976 | tf_op jit(solution)/shard_map/ppermute | solution.py:265
  129.7 32.3 %collective-permute-start.12 = (bf16[776,128]{1,0:T(8,128)(2,1)S(1)}, bf16[776,128]{1,0:T(8,128)(2,1)S(1)}, u32[]{:S(2)}, u32[]{:S(2)}) collective-permute-start(bf16[776,128]{1,0:T(8,128)(2,1)S(1)} %get-tuple-element.38), channel_id=1, source_target_pairs={{0,120},{8,112},{16,104},{24,96},{32,24},{40,16},{48,8},{56,0},{64... | collective-permute-start | bytes 595976 | tf_op jit(solution)/shard_map/ppermute | solution.py:265
  129.7 36.2 %collective-permute-start.13 = (bf16[776,128]{1,0:T(8,128)(2,1)S(1)}, bf16[776,128]{1,0:T(8,128)(2,1)S(1)}, u32[]{:S(2)}, u32[]{:S(2)}) collective-permute-start(bf16[776,128]{1,0:T(8,128)(2,1)S(1)} %get-tuple-element.39), channel_id=1, source_target_pairs={{0,48},{8,56},{16,32},{24,40},{32,80},{40,88},{48,64},{56,72},{64,... | collective-permute-start | bytes 595976 | tf_op jit(solution)/shard_map/ppermute | solution.py:265
  133.4 32.5 %collective-permute-start.14 = (bf16[776,128]{1,0:T(8,128)(2,1)S(1)}, bf16[776,128]{1,0:T(8,128)(2,1)S(1)}, u32[]{:S(2)}, u32[]{:S(2)}) collective-permute-start(bf16[776,128]{1,0:T(8,128)(2,1)S(1)} %get-tuple-element.40), channel_id=1, source_target_pairs={{0,112},{8,120},{16,96},{24,104},{32,16},{40,24},{48,0},{56,8},{64... | collective-permute-start | bytes 595976 | tf_op jit(solution)/shard_map/ppermute | solution.py:265
  133.9 37.4 %collective-permute-start = (bf16[776,128]{1,0:T(8,128)(2,1)S(1)}, bf16[776,128]{1,0:T(8,128)(2,1)S(1)}, u32[]{:S(2)}, u32[]{:S(2)}) collective-permute-start(bf16[776,128]{1,0:T(8,128)(2,1)S(1)} %get-tuple-element.25), channel_id=1, source_target_pairs={{0,8},{8,0},{16,24},{24,16},{32,40},{40,32},{48,56},{56,48},{64,72... | collective-permute-start | bytes 595976 | tf_op jit(solution)/shard_map/ppermute | solution.py:265
  160.8 20.8 %collective-permute-start.1 = (bf16[776,128]{1,0:T(8,128)(2,1)S(1)}, bf16[776,128]{1,0:T(8,128)(2,1)S(1)}, u32[]{:S(2)}, u32[]{:S(2)}) collective-permute-start(bf16[776,128]{1,0:T(8,128)(2,1)S(1)} %get-tuple-element.26), channel_id=1, source_target_pairs={{0,24},{8,16},{16,8},{24,0},{32,56},{40,48},{48,40},{56,32},{64,88... | collective-permute-start | bytes 595976 | tf_op jit(solution)/shard_map/ppermute | solution.py:265
  162.0 27.0 %collective-permute-start.2 = (bf16[776,128]{1,0:T(8,128)(2,1)S(1)}, bf16[776,128]{1,0:T(8,128)(2,1)S(1)}, u32[]{:S(2)}, u32[]{:S(2)}) collective-permute-start(bf16[776,128]{1,0:T(8,128)(2,1)S(1)} %get-tuple-element.27), channel_id=1, source_target_pairs={{0,16},{8,24},{16,0},{24,8},{32,48},{40,56},{48,32},{56,40},{64,80... | collective-permute-start | bytes 595976 | tf_op jit(solution)/shard_map/ppermute | solution.py:265

commit v4 on v3

--- a/solution.py
+++ b/solution.py
@@ -24,6 +24,8 @@
 )
 LEAD = (2,)
 FOLLOW = (1, 3, 0)
+CHUNKS = 3
+STEP = 16
 LATE = 3
 
 ANY = pl.BlockSpec(memory_space=pltpu.HBM)
@@ -36,107 +38,123 @@
     return lax.div(z, KVH), lax.rem(z, KVH), lax.axis_size("sp") // KVH
 
 
-def project_kernel(classes, x_ref, gain_ref, key_ref, value_ref, offset_ref, *rest):
+def project_kernel(classes, heads, given, keep, x_ref, gain_ref, key_ref, value_ref, offset_ref, *rest):
     count = len(classes)
-    outs = rest[: count * KVH]
-    rows, wk, wv, gains, offsets, normed, parts, x_sems, w_sems, o_sems = rest[count * KVH :]
+    outs = rest[: count * len(heads)]
+    rest = rest[count * len(heads) :]
+    normed, *rest = rest
+    weights, offsets, w_sems = rest[:3]
     group, member, groups = split_index()
     prompts = [lax.rem(group + c, groups) for c in classes]
-    block_len = x_ref.shape[1]
+    block_len = normed.shape[0] // count
+    small = pltpu.make_async_copy(offset_ref, offsets, w_sems.at[2 * len(heads)])
+    columns = [pl.ds(pl.multiple_of((member ^ k) * HD, HD), HD) for k in heads]
     loads = [
-        pltpu.make_async_copy(x_ref.at[prompts[n]], rows.at[n], x_sems.at[n]) for n in range(count)
+        pltpu.make_async_copy(ref.at[:, columns[i]], weights.at[i, :, w * HD : (w + 1) * HD], w_sems.at[2 * i + w])
+        for i in range(len(heads))
+        for w, ref in enumerate((key_ref, value_ref))
     ]
-    weights = [
-        pltpu.make_async_copy(key_ref, wk, w_sems.at[0]),
-        pltpu.make_async_copy(value_ref, wv, w_sems.at[1]),
-    ]
-    small = [
-        pltpu.make_async_copy(gain_ref, gains, w_sems.at[2]),
-        pltpu.make_async_copy(offset_ref, offsets, w_sems.at[3]),
-    ]
-    for load in small:
+    if not given:
+        rows, gains, x_sems = rest[3:]
+        gain_load = pltpu.make_async_copy(gain_ref, gains, w_sems.at[2 * len(heads) + 1])
+        gain_load.start()
+        chunk = block_len // CHUNKS
+        reads = [
+            pltpu.make_async_copy(
+                x_ref.at[prompts[n], pl.ds(i * chunk, chunk)],
+                rows.at[pl.ds(n * block_len + i * chunk, chunk)],
+                x_sems.at[n * CHUNKS + i],
+            )
+            for n in range(count)
+            for i in range(CHUNKS)
+        ]
+        for load in reads[:CHUNKS]:
+            load.start()
+    for load in loads:
         load.start()
-    loads[0].start()
-    weights[0].start()
-    weights[1].start()
-    for load in loads[1:]:
-        load.start()
-    for load in small:
-        load.wait()
-    gain = gains[...].reshape(1, -1)
+    small.start()
+    if not given:
+        for load in reads[CHUNKS:]:
+            load.start()
+        gain_load.wait()
+        gain = gains[...].reshape(1, -1)
+        for i, load in enumerate(reads):
+            load.wait()
+
+            def normalize(r, _, i=i):
+                start = pl.multiple_of(i * chunk + r * STEP, STEP)
+                wide = rows[pl.ds(start, STEP), :].astype(jnp.float32)
+                mean = jnp.mean(wide * wide, axis=-1, keepdims=True)
+                normed[pl.ds(start, STEP), :] = (wide * lax.rsqrt(mean + EPSILON) * gain).astype(jnp.bfloat16)
+                return 0
+
+            lax.fori_loop(0, chunk // STEP, normalize, 0, unroll=True)
+    else:
+        normed = x_ref
+    small.wait()
     line = lax.broadcasted_iota(jnp.int32, (EXTRA, HD), 0)
-    prompt = lax.broadcasted_iota(jnp.int32, (x_ref.shape[0], 1), 0)
+    prompt = lax.broadcasted_iota(jnp.int32, (offsets.shape[1], 1), 0)
     for n in range(count):
-        for h in range(KVH):
-            own = offsets[h].astype(jnp.float32)
+        for i, k in enumerate(heads):
+            own = offsets[member ^ k].astype(jnp.float32)
             own = jnp.sum(jnp.where(prompt == prompts[n], own, 0.0), axis=0, keepdims=True)
             extra = jnp.zeros((EXTRA, HD), jnp.float32)
             for j in range(block_len // HD):
                 extra = jnp.where(line == j, own[:, j * HD : (j + 1) * HD], extra)
-            parts[n, h, 2 * block_len :, :] = extra.astype(jnp.bfloat16)
-    stores = []
-    for n in range(count):
-        loads[n].wait()
-        step = 64
-
-        def normalize(r, _, n=n):
-            start = pl.multiple_of(r * step, step)
-            wide = rows[n, pl.ds(start, step), :].astype(jnp.float32)
-            mean = jnp.mean(wide * wide, axis=-1, keepdims=True)
-            normed[pl.ds(start, step), :] = (wide * lax.rsqrt(mean + EPSILON) * gain).astype(jnp.bfloat16)
-            return 0
-
-        lax.fori_loop(0, block_len // step, normalize, 0, unroll=True)
-        for w, weight in enumerate((wk, wv)):
-            if n == 0:
-                weights[w].wait()
-            product = jnp.dot(normed[...], weight[...], preferred_element_type=jnp.float32).astype(jnp.bfloat16)
-            for h in range(KVH):
-                parts[n, h, w * block_len : (w + 1) * block_len, :] = product[:, h * HD : (h + 1) * HD]
-        for k in range(KVH):
-            i = n * KVH + k
-            store = pltpu.make_async_copy(parts.at[n, member ^ k], outs[i], o_sems.at[i])
-            store.start()
-            stores.append(store)
-    for store in stores:
-        store.wait()
-
-
-def project(classes, layer_input, input_gain, key_weight, value_weight, stick_offsets):
-    _, block_len, width = layer_input.shape
-    columns = key_weight.shape[1]
+            outs[n * len(heads) + i][2 * block_len :, :] = extra.astype(jnp.bfloat16)
+    for i in range(len(heads)):
+        loads[2 * i].wait()
+        loads[2 * i + 1].wait()
+        product = jnp.dot(normed[...], weights[i], preferred_element_type=jnp.float32).astype(jnp.bfloat16)
+        for n in range(count):
+            out = outs[n * len(heads) + i]
+            for w in range(2):
+                out[w * block_len : (w + 1) * block_len, :] = product[
+                    n * block_len : (n + 1) * block_len, w * HD : (w + 1) * HD
+                ]
+
+
+def project(classes, heads, source, input_gain, key_weight, value_weight, stick_offsets, keep=False):
+    given = source.ndim == 2
+    width = source.shape[-1]
+    block_len = source.shape[-2]
     count = len(classes)
     piece = jax.ShapeDtypeStruct((2 * block_len + EXTRA, HD), jnp.bfloat16)
-    return pl.pallas_call(
-        functools.partial(project_kernel, classes),
-        out_shape=[piece] * (count * KVH),
-        in_specs=[ANY] * 5,
-        out_specs=[ANY] * (count * KVH),
-        scratch_shapes=[
-            pltpu.VMEM((count, block_len, width), jnp.bfloat16),
-            pltpu.VMEM((width, columns), jnp.bfloat16),
-            pltpu.VMEM((width, columns), jnp.bfloat16),
+    normed = (count * block_len, width)
+    scratch = [] if keep else [pltpu.VMEM(normed if not given else (block_len, HD), jnp.bfloat16)]
+    scratch += [
+        pltpu.VMEM((len(heads), width, 2 * HD), jnp.bfloat16),
+        pltpu.VMEM(stick_offsets.shape, stick_offsets.dtype),
+        pltpu.SemaphoreType.DMA((2 * len(heads) + 2,)),
+    ]
+    if not given:
+        scratch += [
+            pltpu.VMEM(normed, jnp.bfloat16),
             pltpu.VMEM(input_gain.shape, input_gain.dtype),
-            pltpu.VMEM(stick_offsets.shape, stick_offsets.dtype),
-            pltpu.VMEM((block_len, width), jnp.bfloat16),
-            pltpu.VMEM((count, KVH, 2 * block_len + EXTRA, HD), jnp.bfloat16),
-            pltpu.SemaphoreType.DMA((count,)),
-            pltpu.SemaphoreType.DMA((4,)),
-            pltpu.SemaphoreType.DMA((count * KVH,)),
-        ],
+            pltpu.SemaphoreType.DMA((count * CHUNKS,)),
+        ]
+    made = pl.pallas_call(
+        functools.partial(project_kernel, classes, heads, given, keep),
+        out_shape=[piece] * (count * len(heads)) + ([jax.ShapeDtypeStruct(normed, jnp.bfloat16)] if keep else []),
+        in_specs=[VMEM if given else ANY] + [ANY] * 4,
+        out_specs=[VMEM] * (count * len(heads) + keep),
+        scratch_shapes=scratch,
         compiler_params=pltpu.CompilerParams(vmem_limit_bytes=48 * 1024 * 1024),
         cost_estimate=pl.CostEstimate(
-            flops=4 * count * block_len * width * columns,
-            bytes_accessed=count * block_len * width * 2 + 4 * width * columns,
+            flops=4 * count * len(heads) * block_len * width * HD,
+            bytes_accessed=count * block_len * width * 2 + 4 * width * HD * len(heads),
             transcendentals=0,
         ),
         name="project",
     )(
+        source if given else pltpu.with_memory_space_constraint(source, pltpu.HBM),
         *(
             pltpu.with_memory_space_constraint(value, pltpu.HBM)
-            for value in (layer_input, input_gain, key_weight, value_weight, stick_offsets)
-        )
+            for value in (input_gain, key_weight, value_weight, stick_offsets)
+        ),
     )
+    pieces = {(c, k): made[n * len(heads) + i] for n, c in enumerate(classes) for i, k in enumerate(heads)}
+    return pieces, made[-1]
 
 
 def read_kernel(pieces, final, q_ref, bias_ref, *rest):
@@ -185,20 +203,25 @@
     soft = jnp.log1p(jnp.exp(-jnp.abs(z)))
     spread = jnp.maximum(z, 0.0) + soft
     after = (
-        lax.broadcasted_iota(jnp.int32, (block_len, block_len), 0)
-        > lax.broadcasted_iota(jnp.int32, (block_len, block_len), 1)
+        lax.broadcasted_iota(jnp.int32, (HD, HD), 0) > lax.broadcasted_iota(jnp.int32, (HD, HD), 1)
     ).astype(jnp.bfloat16)
-    high = spread.astype(jnp.bfloat16)
-    left = spread - high.astype(jnp.float32)
-    middle = left.astype(jnp.bfloat16)
-    low = (left - middle.astype(jnp.float32)).astype(jnp.bfloat16)
-    inside = (
-        jnp.dot(low, after, preferred_element_type=jnp.float32)
-        + jnp.dot(middle, after, preferred_element_type=jnp.float32)
-        + jnp.dot(high, after, preferred_element_type=jnp.float32)
-    )
+    strips = block_len // HD
+    lanes = [slice(j * HD, (j + 1) * HD) for j in range(strips)]
+    stacked = jnp.concatenate([spread[:, lane] for lane in lanes], axis=0)
+    high = stacked.astype(jnp.bfloat16).astype(jnp.float32)
+    middle = (stacked - high).astype(jnp.bfloat16).astype(jnp.float32)
+    thirds = jnp.concatenate([stacked - high - middle, middle, high], axis=0).astype(jnp.bfloat16)
+    found = jnp.dot(thirds, after, preferred_element_type=jnp.float32)
+    size = count * ROWS
+    found = found[: strips * size] + found[strips * size : 2 * strips * size] + found[2 * strips * size :]
+    sums = jnp.zeros((size, 1), jnp.float32)
+    parts = []
+    for j in reversed(range(strips)):
+        inner = found[j * size : (j + 1) * size]
+        parts.append(inner + sums)
+        sums = sums + inner[:, :1] + spread[:, j * HD : j * HD + 1]
+    inside = jnp.concatenate(parts[::-1], axis=1)
     weights = jnp.exp(jnp.minimum(z, 0.0) - soft - inside).astype(jnp.bfloat16)
-    sums = jnp.sum(spread, axis=-1, keepdims=True)
     for i in range(count):
         lines = slice(i * ROWS, (i + 1) * ROWS)
         totals[blocks[i]] = jnp.broadcast_to(sums[lines], (ROWS, HD))
@@ -255,11 +278,10 @@
     def pairs(c, k):
         return [(z, (z // KVH + c) % groups * KVH + (z % KVH ^ k)) for z in range(sp_count)]
 
-    args = (layer_input, input_gain, key_weight, value_weight, stick_offsets)
-    made = {}
-    for classes in (LEAD, FOLLOW):
-        for i, piece in enumerate(project(classes, *args)):
-            made[classes[i // KVH], i % KVH] = piece
+    args = (input_gain, key_weight, value_weight, stick_offsets)
+    made, normed = project(LEAD, ORDER[0][1:], layer_input, *args, keep=True)
+    made.update(project(LEAD, tuple(k for k in range(KVH) if k != ORDER[0][1]), normed, *args)[0])
+    made.update(project(FOLLOW, tuple(range(KVH)), layer_input, *args)[0])
     got = {(0, 0): made[0, 0]}
     for c, k in ORDER:
         got[c, k] = lax.ppermute(made[c, k], "sp", pairs(c, k))

time: 192 us -> 186 us (0.969)
  starting transfers between devices: 110 us -> 97.6 us
  waiting for transfers between devices: 55.9 us -> 59 us
  Pallas kernels: 25.2 us -> 27.6 us
    ppermute x15, starting transfers between devices: 110 us -> 97.6 us  [shards(): got[c, k] = lax.ppermute(made[c, k], 'sp', pairs(c, k))]
    ppermute x15, waiting for transfers between devices: 55.9 us -> 59 us  [shards(): got[c, k] = lax.ppermute(made[c, k], 'sp', pairs(c, k))]
    pallas_call x2 -> x3, Pallas kernels: 19.3 us -> 21.5 us  [project(): pl.pallas_call(functools.partial(project_kernel, classes, heads, given, k...]
  transfers between devices with their start and end apart: 15 -> 15, of which waited for: 6 -> 7; matrix products, arithmetic and copies ran while one was open for 0% -> 0% of each run, Pallas kernels for 8% -> 12%
where the time goes in v4:
time: 186 us; the launch traced here: 185 us
  starting transfers between devices  97.6 us (52%)
  waiting for transfers between devices  59 us (32%)
  Pallas kernels  27.6 us (15%)
    ppermute x15, starting transfers between devices, shards(): got[c, k] = lax.ppermute(made[c, k], 'sp', pairs(c, k))  97.6 us
    ppermute x15, waiting for transfers between devices, shards(): got[c, k] = lax.ppermute(made[c, k], 'sp', pairs(c, k))  59 us
    pallas_call x3, Pallas kernels, project(): pl.pallas_call(functools.partial(project_kernel, classes, heads, given, k...  21.5 us
    pallas_call x2, Pallas kernels, read(): pl.pallas_call(functools.partial(read_kernel, pieces, final), out_shape=c...  6.07 us
  transfers between devices with their start and end apart: 15, of which 7 were waited for; matrix products, arithmetic and copies ran while one was open for 0% of the time, Pallas kernels for 12%

profile of v4, /device:TPU:36, one launch (start us, length us, event | category | flops | bytes accessed | tf_op | source)
XLA Modules:
  0.0 185.1 jit_solution(6070706608846497464)
XLA Ops:
  0.6 2.6 %project.4 = (bf16[776,128]{1,0:T(8,128)(2,1)S(1)}, bf16[384,2048]{1,0:T(8,128)(2,1)S(1)}) custom-call(bf16[4,384,2048]{2,1,0:T(8,128)(2,1)} %x_ref.3, f32[2048]{0:T(1024)} %gain_ref.5, bf16[2048,512]{1,0:T(8,128)(2,1)} %key_ref.5, bf16[2048,512]{1,0:T(8,128)(2,1)} %value_ref.5, bf16[4,4,384]{2,1,0:T(4,128)(2,1)} %offset_ref.5), custom_call_target="tpu_custom_call" | custom-call | flops 402653184 | bytes 2621440 | tf_op jit(solution)/shard_map/project/pallas_call | solution.py:136
  3.2 20.8 %collective-permute-start.3 = (bf16[776,128]{1,0:T(8,128)(2,1)S(1)}, bf16[776,128]{1,0:T(8,128)(2,1)S(1)}, u32[]{:S(2)}, u32[]{:S(2)}) collective-permute-start(bf16[776,128]{1,0:T(8,128)(2,1)S(1)} %get-tuple-element.30), channel_id=1, source_target_pairs={{0,64},{8,72},{16,80},{24,88},{32,96},{40,104},{48,112},{56,120},{... | collective-permute-start | bytes 595976 | tf_op jit(solution)/shard_map/ppermute | solution.py:287
  24.1 4.4 %project.5 = (bf16[776,128]{1,0:T(8,128)(2,1)S(1)}, bf16[776,128]{1,0:T(8,128)(2,1)S(1)}, bf16[776,128]{1,0:T(8,128)(2,1)S(1)}) custom-call(bf16[384,2048]{1,0:T(8,128)(2,1)S(1)} %get-tuple-element.31.x_ref, f32[2048]{0:T(1024)} %gain_ref.5, bf16[2048,512]{1,0:T(8,128)(2,1)} %key_ref.5, bf16[2048,512]{1,0:T(8,128)(2,1)} %value_ref.5, ...), custom_call_target="tpu_custom_call" | custom-call | flops 1207959552 | bytes 4718592 | tf_op jit(solution)/shard_map/project/pallas_call | solution.py:136
  28.4 0.6 collective-permute-start.4
  29.0 10.2 %collective-permute-start.5 = (bf16[776,128]{1,0:T(8,128)(2,1)S(1)}, bf16[776,128]{1,0:T(8,128)(2,1)S(1)}, u32[]{:S(2)}, u32[]{:S(2)}) collective-permute-start(bf16[776,128]{1,0:T(8,128)(2,1)S(1)} %get-tuple-element.33), channel_id=1, source_target_pairs={{0,88},{8,80},{16,72},{24,64},{32,120},{40,112},{48,104},{56,96},{... | collective-permute-start | bytes 595976 | tf_op jit(solution)/shard_map/ppermute | solution.py:287
  39.2 0.0 copy-start
  39.2 0.0 copy-start.1
  39.2 1.3 collective-permute-start.6
  40.6 14.6 %project.3 = (bf16[776,128]{1,0:T(8,128)(2,1)S(1)}, bf16[776,128]{1,0:T(8,128)(2,1)S(1)}, bf16[776,128]{1,0:T(8,128)(2,1)S(1)}, bf16[776,128]{1,0:T(8,128)(2,1)S...) custom-call(bf16[4,384,2048]{2,1,0:T(8,128)(2,1)} %x_ref.3, ...), custom_call_target="tpu_custom_call" | custom-call | flops 4831838208 | bytes 8912896 | tf_op jit(solution)/shard_map/project/pallas_call | solution.py:136
  55.1 5.9 %collective-permute-start.7 = (bf16[776,128]{1,0:T(8,128)(2,1)S(1)}, bf16[776,128]{1,0:T(8,128)(2,1)S(1)}, u32[]{:S(2)}, u32[]{:S(2)}) collective-permute-start(bf16[776,128]{1,0:T(8,128)(2,1)S(1)} %get-tuple-element.35), channel_id=1, source_target_pairs={{0,32},{8,40},{16,48},{24,56},{32,64},{40,72},{48,80},{56,88},{64,... | collective-permute-start | bytes 595976 | tf_op jit(solution)/shard_map/ppermute | solution.py:287
  61.1 0.0 collective-permute-done.3.rest_1_
  61.1 2.5 %collective-permute-start.8 = (bf16[776,128]{1,0:T(8,128)(2,1)S(1)}, bf16[776,128]{1,0:T(8,128)(2,1)S(1)}, u32[]{:S(2)}, u32[]{:S(2)}) collective-permute-start(bf16[776,128]{1,0:T(8,128)(2,1)S(1)} %get-tuple-element.36), channel_id=1, source_target_pairs={{0,96},{8,104},{16,112},{24,120},{32,0},{40,8},{48,16},{56,24},{64... | collective-permute-start | bytes 595976 | tf_op jit(solution)/shard_map/ppermute | solution.py:287
  63.5 21.7 %collective-permute-done.4.rest_2_ = bf16[776,128]{1,0:T(8,128)(2,1)S(1)} collective-permute-done((bf16[776,128]{1,0:T(8,128)(2,1)S(1)}, bf16[776,128]{1,0:T(8,128)(2,1)S(1)}, u32[]{:S(2)}, u32[]{:S(2)}) %collective-permute-start.4) | collective-permute-done | bytes 198688 | tf_op jit(solution)/shard_map/ppermute | solution.py:287
  85.2 13.6 %collective-permute-start.9 = (bf16[776,128]{1,0:T(8,128)(2,1)S(1)}, bf16[776,128]{1,0:T(8,128)(2,1)S(1)}, u32[]{:S(2)}, u32[]{:S(2)}) collective-permute-start(bf16[776,128]{1,0:T(8,128)(2,1)S(1)} %get-tuple-element.37), channel_id=1, source_target_pairs={{0,40},{8,32},{16,56},{24,48},{32,72},{40,64},{48,88},{56,80},{64,... | collective-permute-start | bytes 595976 | tf_op jit(solution)/shard_map/ppermute | solution.py:287
  98.8 13.5 %collective-permute-done.5.rest_3_ = bf16[776,128]{1,0:T(8,128)(2,1)S(1)} collective-permute-done((bf16[776,128]{1,0:T(8,128)(2,1)S(1)}, bf16[776,128]{1,0:T(8,128)(2,1)S(1)}, u32[]{:S(2)}, u32[]{:S(2)}) %collective-permute-start.5) | collective-permute-done | bytes 198688 | tf_op jit(solution)/shard_map/ppermute | solution.py:287
  112.3 0.0 collective-permute-start.10
  112.3 0.0 collective-permute-done.6.rest_4_
  112.3 10.7 %collective-permute-start.11 = (bf16[776,128]{1,0:T(8,128)(2,1)S(1)}, bf16[776,128]{1,0:T(8,128)(2,1)S(1)}, u32[]{:S(2)}, u32[]{:S(2)}) collective-permute-start(bf16[776,128]{1,0:T(8,128)(2,1)S(1)} %get-tuple-element.39), channel_id=1, source_target_pairs={{0,56},{8,48},{16,40},{24,32},{32,88},{40,80},{48,72},{56,64},{64,... | collective-permute-start | bytes 595976 | tf_op jit(solution)/shard_map/ppermute | solution.py:287
  123.0 0.0 collective-permute-done.7.rest_5_
  123.0 7.0 %collective-permute-start.12 = (bf16[776,128]{1,0:T(8,128)(2,1)S(1)}, bf16[776,128]{1,0:T(8,128)(2,1)S(1)}, u32[]{:S(2)}, u32[]{:S(2)}) collective-permute-start(bf16[776,128]{1,0:T(8,128)(2,1)S(1)} %get-tuple-element.40), channel_id=1, source_target_pairs={{0,120},{8,112},{16,104},{24,96},{32,24},{40,16},{48,8},{56,0},{64... | collective-permute-start | bytes 595976 | tf_op jit(solution)/shard_map/ppermute | solution.py:287
  130.1 0.0 collective-permute-done.8.rest_6_
  130.1 2.6 %collective-permute-start.13 = (bf16[776,128]{1,0:T(8,128)(2,1)S(1)}, bf16[776,128]{1,0:T(8,128)(2,1)S(1)}, u32[]{:S(2)}, u32[]{:S(2)}) collective-permute-start(bf16[776,128]{1,0:T(8,128)(2,1)S(1)} %get-tuple-element.41), channel_id=1, source_target_pairs={{0,48},{8,56},{16,32},{24,40},{32,80},{40,88},{48,64},{56,72},{64,... | collective-permute-start | bytes 595976 | tf_op jit(solution)/shard_map/ppermute | solution.py:287
  132.7 0.0 collective-permute-done.9.rest_7_
  132.7 14.2 %collective-permute-start.14 = (bf16[776,128]{1,0:T(8,128)(2,1)S(1)}, bf16[776,128]{1,0:T(8,128)(2,1)S(1)}, u32[]{:S(2)}, u32[]{:S(2)}) collective-permute-start(bf16[776,128]{1,0:T(8,128)(2,1)S(1)} %get-tuple-element.42), channel_id=1, source_target_pairs={{0,112},{8,120},{16,96},{24,104},{32,16},{40,24},{48,0},{56,8},{64... | collective-permute-start | bytes 595976 | tf_op jit(solution)/shard_map/ppermute | solution.py:287
  146.9 0.0 collective-permute-done.10.rest_8_
  146.9 0.0 collective-permute-start
  146.9 2.7 %collective-permute-done.11.rest_9_ = bf16[776,128]{1,0:T(8,128)(2,1)S(1)} collective-permute-done((bf16[776,128]{1,0:T(8,128)(2,1)S(1)}, bf16[776,128]{1,0:T(8,128)(2,1)S(1)}, u32[]{:S(2)}, u32[]{:S(2)}) %collective-permute-start.11) | collective-permute-done | bytes 198688 | tf_op jit(solution)/shard_map/ppermute | solution.py:287
  149.6 8.1 %collective-permute-start.1 = (bf16[776,128]{1,0:T(8,128)(2,1)S(1)}, bf16[776,128]{1,0:T(8,128)(2,1)S(1)}, u32[]{:S(2)}, u32[]{:S(2)}) collective-permute-start(bf16[776,128]{1,0:T(8,128)(2,1)S(1)} %get-tuple-element.27), channel_id=1, source_target_pairs={{0,24},{8,16},{16,8},{24,0},{32,56},{40,48},{48,40},{56,32},{64,88... | collective-permute-start | bytes 595976 | tf_op jit(solution)/shard_map/ppermute | solution.py:287
  157.7 4.1 %collective-permute-done.12.rest_10_ = bf16[776,128]{1,0:T(8,128)(2,1)S(1)} collective-permute-done((bf16[776,128]{1,0:T(8,128)(2,1)S(1)}, bf16[776,128]{1,0:T(8,128)(2,1)S(1)}, u32[]{:S(2)}, u32[]{:S(2)}) %collective-permute-start.12) | collective-permute-done | bytes 198688 | tf_op jit(solution)/shard_map/ppermute | solution.py:287
  161.8 0.0 collective-permute-start.2
  161.8 0.0 collective-permute-done.13.rest_11_
  161.8 7.3 %collective-permute-done.14.rest_12_ = bf16[776,128]{1,0:T(8,128)(2,1)S(1)} collective-permute-done((bf16[776,128]{1,0:T(8,128)(2,1)S(1)}, bf16[776,128]{1,0:T(8,128)(2,1)S(1)}, u32[]{:S(2)}, u32[]{:S(2)}) %collective-permute-start.14) | collective-permute-done | bytes 198688 | tf_op jit(solution)/shard_map/ppermute | solution.py:287
  169.1 0.0 copy-done
  169.1 0.0 copy-done.1
  169.1 3.5 %read.2 = (bf16[1,1,6144,128]{3,2,1,0:T(8,128)(2,1)}, bf16[1,1,6144,128]{3,2,1,0:T(8,128)(2,1)}, f32[16,8,128]{2,1,0:T(8,128)S(1)}, f32[16,8,128]{2,1,0:T(8,128)S(1)}, f32[16,1,384]{2,1,0:T(1,128)S(1)}) custom-call(bf16[1,1,512]{2,1,0:T(2,128)(2,1)S(1)} %copy-done, f32[16]{0:T(128)S(1)} %copy-done.1, bf16[776,128]{1,0:T(8,128)(2,1)S(1)} %get-tuple-element.29.rest_0_, ...), custom_call_target="tpu_custom_call" | custom-call | flops 40894464 | bytes 5111808 | tf_op jit(solution)/shard_map/read/pallas_call | solution.py:254
  172.7 3.3 %collective-permute-done.rest_0_ = bf16[776,128]{1,0:T(8,128)(2,1)S(1)} collective-permute-done((bf16[776,128]{1,0:T(8,128)(2,1)S(1)}, bf16[776,128]{1,0:T(8,128)(2,1)S(1)}, u32[]{:S(2)}, u32[]{:S(2)}) %collective-permute-start) | collective-permute-done | bytes 198688 | tf_op jit(solution)/shard_map/ppermute | solution.py:287
  175.9 0.0 collective-permute-done.1.rest_1_
  175.9 6.4 %collective-permute-done.2.rest_2_ = bf16[776,128]{1,0:T(8,128)(2,1)S(1)} collective-permute-done((bf16[776,128]{1,0:T(8,128)(2,1)S(1)}, bf16[776,128]{1,0:T(8,128)(2,1)S(1)}, u32[]{:S(2)}, u32[]{:S(2)}) %collective-permute-start.2) | collective-permute-done | bytes 198688 | tf_op jit(solution)/shard_map/ppermute | solution.py:287
  182.4 2.5 %read.3 = (bf16[1,1,6144,128]{3,2,1,0:T(8,128)(2,1)}, bf16[1,1,6144,128]{3,2,1,0:T(8,128)(2,1)}, bf16[1,1,6144]{2,1,0:T(2,128)(2,1)}, bf16[1,1,512]{2,1,0:T(2,128)(2,1)}) custom-call(bf16[1,1,512]{2,1,0:T(2,128)(2,1)S(1)} %copy-done, f32[16]{0:T(128)S(1)} %copy-done.1, ...), custom_call_target="tpu_custom_call", output_to_operand_aliasing={{0}: (8, {}), {1}: (9, {})} | custom-call | flops 9437184 | bytes 1179648 | tf_op jit(solution)/shard_map/read/pallas_call | solution.py:254
Async XLA Ops:
  3.2 57.8 %collective-permute-start.3 = (bf16[776,128]{1,0:T(8,128)(2,1)S(1)}, bf16[776,128]{1,0:T(8,128)(2,1)S(1)}, u32[]{:S(2)}, u32[]{:S(2)}) collective-permute-start(bf16[776,128]{1,0:T(8,128)(2,1)S(1)} %get-tuple-element.30), channel_id=1, source_target_pairs={{0,64},{8,72},{16,80},{24,88},{32,96},{40,104},{48,112},{56,120},{... | collective-permute-start | bytes 595976 | tf_op jit(solution)/shard_map/ppermute | solution.py:287
  28.4 56.8 %collective-permute-start.4 = (bf16[776,128]{1,0:T(8,128)(2,1)S(1)}, bf16[776,128]{1,0:T(8,128)(2,1)S(1)}, u32[]{:S(2)}, u32[]{:S(2)}) collective-permute-start(bf16[776,128]{1,0:T(8,128)(2,1)S(1)} %get-tuple-element.32), channel_id=1, source_target_pairs={{0,72},{8,64},{16,88},{24,80},{32,104},{40,96},{48,120},{56,112},{... | collective-permute-start | bytes 595976 | tf_op jit(solution)/shard_map/ppermute | solution.py:287
  29.0 83.3 %collective-permute-start.5 = (bf16[776,128]{1,0:T(8,128)(2,1)S(1)}, bf16[776,128]{1,0:T(8,128)(2,1)S(1)}, u32[]{:S(2)}, u32[]{:S(2)}) collective-permute-start(bf16[776,128]{1,0:T(8,128)(2,1)S(1)} %get-tuple-element.33), channel_id=1, source_target_pairs={{0,88},{8,80},{16,72},{24,64},{32,120},{40,112},{48,104},{56,96},{... | collective-permute-start | bytes 595976 | tf_op jit(solution)/shard_map/ppermute | solution.py:287
  39.2 129.9 %copy-start = (bf16[1,1,512]{2,1,0:T(2,128)(2,1)S(1)}, bf16[1,1,512]{2,1,0:T(2,128)(2,1)}, u32[]{:S(2)}) copy-start(bf16[1,1,512]{2,1,0:T(2,128)(2,1)} %q_ref.3) | copy-start | bytes 3076
  39.2 129.9 %copy-start.1 = (f32[16]{0:T(128)S(1)}, f32[16]{0:T(128)}, u32[]{:S(2)}) copy-start(f32[16]{0:T(128)} %bias_ref.3) | copy-start | bytes 196
  39.2 73.1 %collective-permute-start.6 = (bf16[776,128]{1,0:T(8,128)(2,1)S(1)}, bf16[776,128]{1,0:T(8,128)(2,1)S(1)}, u32[]{:S(2)}, u32[]{:S(2)}) collective-permute-start(bf16[776,128]{1,0:T(8,128)(2,1)S(1)} %get-tuple-element.34), channel_id=1, source_target_pairs={{0,80},{8,88},{16,64},{24,72},{32,112},{40,120},{48,96},{56,104},{... | collective-permute-start | bytes 595976 | tf_op jit(solution)/shard_map/ppermute | solution.py:287
  55.1 67.9 %collective-permute-start.7 = (bf16[776,128]{1,0:T(8,128)(2,1)S(1)}, bf16[776,128]{1,0:T(8,128)(2,1)S(1)}, u32[]{:S(2)}, u32[]{:S(2)}) collective-permute-start(bf16[776,128]{1,0:T(8,128)(2,1)S(1)} %get-tuple-element.35), channel_id=1, source_target_pairs={{0,32},{8,40},{16,48},{24,56},{32,64},{40,72},{48,80},{56,88},{64,... | collective-permute-start | bytes 595976 | tf_op jit(solution)/shard_map/ppermute | solution.py:287
  61.1 69.0 %collective-permute-start.8 = (bf16[776,128]{1,0:T(8,128)(2,1)S(1)}, bf16[776,128]{1,0:T(8,128)(2,1)S(1)}, u32[]{:S(2)}, u32[]{:S(2)}) collective-permute-start(bf16[776,128]{1,0:T(8,128)(2,1)S(1)} %get-tuple-element.36), channel_id=1, source_target_pairs={{0,96},{8,104},{16,112},{24,120},{32,0},{40,8},{48,16},{56,24},{64... | collective-permute-start | bytes 595976 | tf_op jit(solution)/shard_map/ppermute | solution.py:287
  85.2 47.5 %collective-permute-start.9 = (bf16[776,128]{1,0:T(8,128)(2,1)S(1)}, bf16[776,128]{1,0:T(8,128)(2,1)S(1)}, u32[]{:S(2)}, u32[]{:S(2)}) collective-permute-start(bf16[776,128]{1,0:T(8,128)(2,1)S(1)} %get-tuple-element.37), channel_id=1, source_target_pairs={{0,40},{8,32},{16,56},{24,48},{32,72},{40,64},{48,88},{56,80},{64,... | collective-permute-start | bytes 595976 | tf_op jit(solution)/shard_map/ppermute | solution.py:287
  112.3 34.6 %collective-permute-start.10 = (bf16[776,128]{1,0:T(8,128)(2,1)S(1)}, bf16[776,128]{1,0:T(8,128)(2,1)S(1)}, u32[]{:S(2)}, u32[]{:S(2)}) collective-permute-start(bf16[776,128]{1,0:T(8,128)(2,1)S(1)} %get-tuple-element.38), channel_id=1, source_target_pairs={{0,104},{8,96},{16,120},{24,112},{32,8},{40,0},{48,24},{56,16},{64... | collective-permute-start | bytes 595976 | tf_op jit(solution)/shard_map/ppermute | solution.py:287
  112.3 37.3 %collective-permute-start.11 = (bf16[776,128]{1,0:T(8,128)(2,1)S(1)}, bf16[776,128]{1,0:T(8,128)(2,1)S(1)}, u32[]{:S(2)}, u32[]{:S(2)}) collective-permute-start(bf16[776,128]{1,0:T(8,128)(2,1)S(1)} %get-tuple-element.39), channel_id=1, source_target_pairs={{0,56},{8,48},{16,40},{24,32},{32,88},{40,80},{48,72},{56,64},{64,... | collective-permute-start | bytes 595976 | tf_op jit(solution)/shard_map/ppermute | solution.py:287
  123.0 38.7 %collective-permute-start.12 = (bf16[776,128]{1,0:T(8,128)(2,1)S(1)}, bf16[776,128]{1,0:T(8,128)(2,1)S(1)}, u32[]{:S(2)}, u32[]{:S(2)}) collective-permute-start(bf16[776,128]{1,0:T(8,128)(2,1)S(1)} %get-tuple-element.40), channel_id=1, source_target_pairs={{0,120},{8,112},{16,104},{24,96},{32,24},{40,16},{48,8},{56,0},{64... | collective-permute-start | bytes 595976 | tf_op jit(solution)/shard_map/ppermute | solution.py:287
  130.1 31.7 %collective-permute-start.13 = (bf16[776,128]{1,0:T(8,128)(2,1)S(1)}, bf16[776,128]{1,0:T(8,128)(2,1)S(1)}, u32[]{:S(2)}, u32[]{:S(2)}) collective-permute-start(bf16[776,128]{1,0:T(8,128)(2,1)S(1)} %get-tuple-element.41), channel_id=1, source_target_pairs={{0,48},{8,56},{16,32},{24,40},{32,80},{40,88},{48,64},{56,72},{64,... | collective-permute-start | bytes 595976 | tf_op jit(solution)/shard_map/ppermute | solution.py:287
  132.7 36.4 %collective-permute-start.14 = (bf16[776,128]{1,0:T(8,128)(2,1)S(1)}, bf16[776,128]{1,0:T(8,128)(2,1)S(1)}, u32[]{:S(2)}, u32[]{:S(2)}) collective-permute-start(bf16[776,128]{1,0:T(8,128)(2,1)S(1)} %get-tuple-element.42), channel_id=1, source_target_pairs={{0,112},{8,120},{16,96},{24,104},{32,16},{40,24},{48,0},{56,8},{64... | collective-permute-start | bytes 595976 | tf_op jit(solution)/shard_map/ppermute | solution.py:287
  146.9 29.0 %collective-permute-start = (bf16[776,128]{1,0:T(8,128)(2,1)S(1)}, bf16[776,128]{1,0:T(8,128)(2,1)S(1)}, u32[]{:S(2)}, u32[]{:S(2)}) collective-permute-start(bf16[776,128]{1,0:T(8,128)(2,1)S(1)} %get-tuple-element.26), channel_id=1, source_target_pairs={{0,8},{8,0},{16,24},{24,16},{32,40},{40,32},{48,56},{56,48},{64,72... | collective-permute-start | bytes 595976 | tf_op jit(solution)/shard_map/ppermute | solution.py:287
  149.6 26.3 %collective-permute-start.1 = (bf16[776,128]{1,0:T(8,128)(2,1)S(1)}, bf16[776,128]{1,0:T(8,128)(2,1)S(1)}, u32[]{:S(2)}, u32[]{:S(2)}) collective-permute-start(bf16[776,128]{1,0:T(8,128)(2,1)S(1)} %get-tuple-element.27), channel_id=1, source_target_pairs={{0,24},{8,16},{16,8},{24,0},{32,56},{40,48},{48,40},{56,32},{64,88... | collective-permute-start | bytes 595976 | tf_op jit(solution)/shard_map/ppermute | solution.py:287
  161.8 20.6 %collective-permute-start.2 = (bf16[776,128]{1,0:T(8,128)(2,1)S(1)}, bf16[776,128]{1,0:T(8,128)(2,1)S(1)}, u32[]{:S(2)}, u32[]{:S(2)}) collective-permute-start(bf16[776,128]{1,0:T(8,128)(2,1)S(1)} %get-tuple-element.28), channel_id=1, source_target_pairs={{0,16},{8,24},{16,0},{24,8},{32,48},{40,56},{48,32},{56,40},{64,80... | collective-permute-start | bytes 595976 | tf_op jit(solution)/shard_map/ppermute | solution.py:287

commit v5 on v4

--- a/solution.py
+++ b/solution.py
@@ -18,9 +18,11 @@
 EXTRA = 8
 
 ORDER = (
-    tuple((2, k) for k in (0, 1, 3, 2))
-    + tuple((c, k) for k in (0, 1, 3, 2) for c in (1, 3))
-    + tuple((0, k) for k in (1, 3, 2))
+    ((2, 0), (2, 3))
+    + ((1, 0), (3, 1), (1, 2), (3, 0))
+    + ((2, 2), (2, 1))
+    + ((1, 3), (3, 2), (1, 1), (3, 3))
+    + ((0, 2), (0, 3), (0, 1))
 )
 LEAD = (2,)
 FOLLOW = (1, 3, 0)
@@ -88,7 +90,7 @@
                 normed[pl.ds(start, STEP), :] = (wide * lax.rsqrt(mean + EPSILON) * gain).astype(jnp.bfloat16)
                 return 0
 
-            lax.fori_loop(0, chunk // STEP, normalize, 0, unroll=True)
+            lax.fori_loop(0, chunk // STEP, normalize, 0, unroll=4)
     else:
         normed = x_ref
     small.wait()

time: 186 us -> 184 us (0.989)
  waiting for transfers between devices: 59 us -> 53.2 us
    ppermute x15, waiting for transfers between devices: 59 us -> 53.2 us  [shards(): got[c, k] = lax.ppermute(made[c, k], 'sp', pairs(c, k))]
  transfers between devices with their start and end apart: 15 -> 15, of which waited for: 7 -> 5; matrix products, arithmetic and copies ran while one was open for 0% -> 0% of each run, Pallas kernels for 12% -> 13%
where the time goes in v5:
time: 184 us; the launch traced here: 181 us
  starting transfers between devices  99.1 us (54%)
  waiting for transfers between devices  53.2 us (29%)
  Pallas kernels  28.1 us (15%)
    ppermute x15, starting transfers between devices, shards(): got[c, k] = lax.ppermute(made[c, k], 'sp', pairs(c, k))  99.1 us
    ppermute x15, waiting for transfers between devices, shards(): got[c, k] = lax.ppermute(made[c, k], 'sp', pairs(c, k))  53.2 us
    pallas_call x3, Pallas kernels, project(): pl.pallas_call(functools.partial(project_kernel, classes, heads, given, k...  22 us
    pallas_call x2, Pallas kernels, read(): pl.pallas_call(functools.partial(read_kernel, pieces, final), out_shape=c...  6.09 us
  transfers between devices with their start and end apart: 15, of which 5 were waited for; matrix products, arithmetic and copies ran while one was open for 0% of the time, Pallas kernels for 13%

profile of v5, /device:TPU:36, one launch (start us, length us, event | category | flops | bytes accessed | tf_op | source)
XLA Modules:
  0.0 181.2 jit_solution(16689463015096143374)
XLA Ops:
  0.6 2.9 %project.4 = (bf16[776,128]{1,0:T(8,128)(2,1)S(1)}, bf16[384,2048]{1,0:T(8,128)(2,1)S(1)}) custom-call(bf16[4,384,2048]{2,1,0:T(8,128)(2,1)} %x_ref.3, f32[2048]{0:T(1024)} %gain_ref.5, bf16[2048,512]{1,0:T(8,128)(2,1)} %key_ref.5, bf16[2048,512]{1,0:T(8,128)(2,1)} %value_ref.5, bf16[4,4,384]{2,1,0:T(4,128)(2,1)} %offset_ref.5), custom_call_target="tpu_custom_call" | custom-call | flops 402653184 | bytes 2621440 | tf_op jit(solution)/shard_map/project/pallas_call | solution.py:138
  3.5 20.8 %collective-permute-start.3 = (bf16[776,128]{1,0:T(8,128)(2,1)S(1)}, bf16[776,128]{1,0:T(8,128)(2,1)S(1)}, u32[]{:S(2)}, u32[]{:S(2)}) collective-permute-start(bf16[776,128]{1,0:T(8,128)(2,1)S(1)} %get-tuple-element.30), channel_id=1, source_target_pairs={{0,64},{8,72},{16,80},{24,88},{32,96},{40,104},{48,112},{56,120},{... | collective-permute-start | bytes 595976 | tf_op jit(solution)/shard_map/ppermute | solution.py:289
  24.3 4.4 %project.5 = (bf16[776,128]{1,0:T(8,128)(2,1)S(1)}, bf16[776,128]{1,0:T(8,128)(2,1)S(1)}, bf16[776,128]{1,0:T(8,128)(2,1)S(1)}) custom-call(bf16[384,2048]{1,0:T(8,128)(2,1)S(1)} %get-tuple-element.31.x_ref, f32[2048]{0:T(1024)} %gain_ref.5, bf16[2048,512]{1,0:T(8,128)(2,1)} %key_ref.5, bf16[2048,512]{1,0:T(8,128)(2,1)} %value_ref.5, ...), custom_call_target="tpu_custom_call" | custom-call | flops 1207959552 | bytes 4718592 | tf_op jit(solution)/shard_map/project/pallas_call | solution.py:138
  28.7 1.4 collective-permute-start.4
  30.1 9.0 %collective-permute-start.9 = (bf16[776,128]{1,0:T(8,128)(2,1)S(1)}, bf16[776,128]{1,0:T(8,128)(2,1)S(1)}, u32[]{:S(2)}, u32[]{:S(2)}) collective-permute-start(bf16[776,128]{1,0:T(8,128)(2,1)S(1)} %get-tuple-element.37), channel_id=1, source_target_pairs={{0,80},{8,88},{16,64},{24,72},{32,112},{40,120},{48,96},{56,104},{... | collective-permute-start | bytes 595976 | tf_op jit(solution)/shard_map/ppermute | solution.py:289
  39.1 0.0 copy-start
  39.1 0.0 copy-start.1
  39.1 1.9 %collective-permute-start.10 = (bf16[776,128]{1,0:T(8,128)(2,1)S(1)}, bf16[776,128]{1,0:T(8,128)(2,1)S(1)}, u32[]{:S(2)}, u32[]{:S(2)}) collective-permute-start(bf16[776,128]{1,0:T(8,128)(2,1)S(1)} %get-tuple-element.38), channel_id=1, source_target_pairs={{0,72},{8,64},{16,88},{24,80},{32,104},{40,96},{48,120},{56,112},{... | collective-permute-start | bytes 595976 | tf_op jit(solution)/shard_map/ppermute | solution.py:289
  40.9 14.8 %project.3 = (bf16[776,128]{1,0:T(8,128)(2,1)S(1)}, bf16[776,128]{1,0:T(8,128)(2,1)S(1)}, bf16[776,128]{1,0:T(8,128)(2,1)S(1)}, bf16[776,128]{1,0:T(8,128)(2,1)S...) custom-call(bf16[4,384,2048]{2,1,0:T(8,128)(2,1)} %x_ref.3, ...), custom_call_target="tpu_custom_call" | custom-call | flops 4831838208 | bytes 8912896 | tf_op jit(solution)/shard_map/project/pallas_call | solution.py:138
  55.7 6.1 %collective-permute-start.5 = (bf16[776,128]{1,0:T(8,128)(2,1)S(1)}, bf16[776,128]{1,0:T(8,128)(2,1)S(1)}, u32[]{:S(2)}, u32[]{:S(2)}) collective-permute-start(bf16[776,128]{1,0:T(8,128)(2,1)S(1)} %get-tuple-element.33), channel_id=1, source_target_pairs={{0,32},{8,40},{16,48},{24,56},{32,64},{40,72},{48,80},{56,88},{64,... | collective-permute-start | bytes 595976 | tf_op jit(solution)/shard_map/ppermute | solution.py:289
  61.8 0.0 collective-permute-done.3.rest_1_
  61.8 2.7 %collective-permute-start.6 = (bf16[776,128]{1,0:T(8,128)(2,1)S(1)}, bf16[776,128]{1,0:T(8,128)(2,1)S(1)}, u32[]{:S(2)}, u32[]{:S(2)}) collective-permute-start(bf16[776,128]{1,0:T(8,128)(2,1)S(1)} %get-tuple-element.34), channel_id=1, source_target_pairs={{0,104},{8,96},{16,120},{24,112},{32,8},{40,0},{48,24},{56,16},{64... | collective-permute-start | bytes 595976 | tf_op jit(solution)/shard_map/ppermute | solution.py:289
  64.6 24.4 %collective-permute-done.4.rest_2_ = bf16[776,128]{1,0:T(8,128)(2,1)S(1)} collective-permute-done((bf16[776,128]{1,0:T(8,128)(2,1)S(1)}, bf16[776,128]{1,0:T(8,128)(2,1)S(1)}, u32[]{:S(2)}, u32[]{:S(2)}) %collective-permute-start.4) | collective-permute-done | bytes 198688 | tf_op jit(solution)/shard_map/ppermute | solution.py:289
  88.9 0.0 collective-permute-start.7
  89.0 5.0 %collective-permute-done.9.rest_7_ = bf16[776,128]{1,0:T(8,128)(2,1)S(1)} collective-permute-done((bf16[776,128]{1,0:T(8,128)(2,1)S(1)}, bf16[776,128]{1,0:T(8,128)(2,1)S(1)}, u32[]{:S(2)}, u32[]{:S(2)}) %collective-permute-start.9) | collective-permute-done | bytes 198688 | tf_op jit(solution)/shard_map/ppermute | solution.py:289
  93.9 20.8 %collective-permute-start.8 = (bf16[776,128]{1,0:T(8,128)(2,1)S(1)}, bf16[776,128]{1,0:T(8,128)(2,1)S(1)}, u32[]{:S(2)}, u32[]{:S(2)}) collective-permute-start(bf16[776,128]{1,0:T(8,128)(2,1)S(1)} %get-tuple-element.36), channel_id=1, source_target_pairs={{0,96},{8,104},{16,112},{24,120},{32,0},{40,8},{48,16},{56,24},{64... | collective-permute-start | bytes 595976 | tf_op jit(solution)/shard_map/ppermute | solution.py:289
  114.7 0.0 collective-permute-done.10.rest_8_
  114.7 7.4 %collective-permute-start.11 = (bf16[776,128]{1,0:T(8,128)(2,1)S(1)}, bf16[776,128]{1,0:T(8,128)(2,1)S(1)}, u32[]{:S(2)}, u32[]{:S(2)}) collective-permute-start(bf16[776,128]{1,0:T(8,128)(2,1)S(1)} %get-tuple-element.39), channel_id=1, source_target_pairs={{0,56},{8,48},{16,40},{24,32},{32,88},{40,80},{48,72},{56,64},{64,... | collective-permute-start | bytes 595976 | tf_op jit(solution)/shard_map/ppermute | solution.py:289
  122.1 0.0 collective-permute-done.5.rest_3_
  122.1 4.1 %collective-permute-start.12 = (bf16[776,128]{1,0:T(8,128)(2,1)S(1)}, bf16[776,128]{1,0:T(8,128)(2,1)S(1)}, u32[]{:S(2)}, u32[]{:S(2)}) collective-permute-start(bf16[776,128]{1,0:T(8,128)(2,1)S(1)} %get-tuple-element.40), channel_id=1, source_target_pairs={{0,112},{8,120},{16,96},{24,104},{32,16},{40,24},{48,0},{56,8},{64... | collective-permute-start | bytes 595976 | tf_op jit(solution)/shard_map/ppermute | solution.py:289
  126.2 0.0 collective-permute-done.6.rest_4_
  126.2 0.2 collective-permute-start.13
  126.5 0.0 collective-permute-done.7.rest_5_
  126.5 23.5 %collective-permute-start.14 = (bf16[776,128]{1,0:T(8,128)(2,1)S(1)}, bf16[776,128]{1,0:T(8,128)(2,1)S(1)}, u32[]{:S(2)}, u32[]{:S(2)}) collective-permute-start(bf16[776,128]{1,0:T(8,128)(2,1)S(1)} %get-tuple-element.42), channel_id=1, source_target_pairs={{0,120},{8,112},{16,104},{24,96},{32,24},{40,16},{48,8},{56,0},{64... | collective-permute-start | bytes 595976 | tf_op jit(solution)/shard_map/ppermute | solution.py:289
  149.9 1.2 collective-permute-done.8.rest_6_
  151.1 0.0 collective-permute-start
  151.1 0.0 collective-permute-done.11.rest_9_
  151.1 1.1 collective-permute-start.1
  152.2 9.5 %collective-permute-done.12.rest_10_ = bf16[776,128]{1,0:T(8,128)(2,1)S(1)} collective-permute-done((bf16[776,128]{1,0:T(8,128)(2,1)S(1)}, bf16[776,128]{1,0:T(8,128)(2,1)S(1)}, u32[]{:S(2)}, u32[]{:S(2)}) %collective-permute-start.12) | collective-permute-done | bytes 198688 | tf_op jit(solution)/shard_map/ppermute | solution.py:289
  161.7 0.0 collective-permute-start.2
  161.7 13.2 %collective-permute-done.13.rest_11_ = bf16[776,128]{1,0:T(8,128)(2,1)S(1)} collective-permute-done((bf16[776,128]{1,0:T(8,128)(2,1)S(1)}, bf16[776,128]{1,0:T(8,128)(2,1)S(1)}, u32[]{:S(2)}, u32[]{:S(2)}) %collective-permute-start.13) | collective-permute-done | bytes 198688 | tf_op jit(solution)/shard_map/ppermute | solution.py:289
  174.9 0.0 collective-permute-done.14.rest_12_
  174.9 0.0 copy-done
  174.9 0.0 copy-done.1
  174.9 3.6 %read.2 = (bf16[1,1,6144,128]{3,2,1,0:T(8,128)(2,1)}, bf16[1,1,6144,128]{3,2,1,0:T(8,128)(2,1)}, f32[16,8,128]{2,1,0:T(8,128)S(1)}, f32[16,8,128]{2,1,0:T(8,128)S(1)}, f32[16,1,384]{2,1,0:T(1,128)S(1)}) custom-call(bf16[1,1,512]{2,1,0:T(2,128)(2,1)S(1)} %copy-done, f32[16]{0:T(128)S(1)} %copy-done.1, bf16[776,128]{1,0:T(8,128)(2,1)S(1)} %get-tuple-element.29.rest_0_, ...), custom_call_target="tpu_custom_call" | custom-call | flops 40894464 | bytes 5111808 | tf_op jit(solution)/shard_map/read/pallas_call | solution.py:256
  178.5 0.0 collective-permute-done.rest_0_
  178.5 0.0 collective-permute-done.1.rest_1_
  178.5 0.0 collective-permute-done.2.rest_2_
  178.5 2.5 %read.3 = (bf16[1,1,6144,128]{3,2,1,0:T(8,128)(2,1)}, bf16[1,1,6144,128]{3,2,1,0:T(8,128)(2,1)}, bf16[1,1,6144]{2,1,0:T(2,128)(2,1)}, bf16[1,1,512]{2,1,0:T(2,128)(2,1)}) custom-call(bf16[1,1,512]{2,1,0:T(2,128)(2,1)S(1)} %copy-done, f32[16]{0:T(128)S(1)} %copy-done.1, ...), custom_call_target="tpu_custom_call", output_to_operand_aliasing={{0}: (8, {}), {1}: (9, {})} | custom-call | flops 9437184 | bytes 1179648 | tf_op jit(solution)/shard_map/read/pallas_call | solution.py:256
Async XLA Ops:
  3.5 58.3 %collective-permute-start.3 = (bf16[776,128]{1,0:T(8,128)(2,1)S(1)}, bf16[776,128]{1,0:T(8,128)(2,1)S(1)}, u32[]{:S(2)}, u32[]{:S(2)}) collective-permute-start(bf16[776,128]{1,0:T(8,128)(2,1)S(1)} %get-tuple-element.30), channel_id=1, source_target_pairs={{0,64},{8,72},{16,80},{24,88},{32,96},{40,104},{48,112},{56,120},{... | collective-permute-start | bytes 595976 | tf_op jit(solution)/shard_map/ppermute | solution.py:289
  28.7 60.3 %collective-permute-start.4 = (bf16[776,128]{1,0:T(8,128)(2,1)S(1)}, bf16[776,128]{1,0:T(8,128)(2,1)S(1)}, u32[]{:S(2)}, u32[]{:S(2)}) collective-permute-start(bf16[776,128]{1,0:T(8,128)(2,1)S(1)} %get-tuple-element.32), channel_id=1, source_target_pairs={{0,88},{8,80},{16,72},{24,64},{32,120},{40,112},{48,104},{56,96},{... | collective-permute-start | bytes 595976 | tf_op jit(solution)/shard_map/ppermute | solution.py:289
  30.1 63.8 %collective-permute-start.9 = (bf16[776,128]{1,0:T(8,128)(2,1)S(1)}, bf16[776,128]{1,0:T(8,128)(2,1)S(1)}, u32[]{:S(2)}, u32[]{:S(2)}) collective-permute-start(bf16[776,128]{1,0:T(8,128)(2,1)S(1)} %get-tuple-element.37), channel_id=1, source_target_pairs={{0,80},{8,88},{16,64},{24,72},{32,112},{40,120},{48,96},{56,104},{... | collective-permute-start | bytes 595976 | tf_op jit(solution)/shard_map/ppermute | solution.py:289
  39.1 135.9 %copy-start = (bf16[1,1,512]{2,1,0:T(2,128)(2,1)S(1)}, bf16[1,1,512]{2,1,0:T(2,128)(2,1)}, u32[]{:S(2)}) copy-start(bf16[1,1,512]{2,1,0:T(2,128)(2,1)} %q_ref.3) | copy-start | bytes 3076
  39.1 135.9 %copy-start.1 = (f32[16]{0:T(128)S(1)}, f32[16]{0:T(128)}, u32[]{:S(2)}) copy-start(f32[16]{0:T(128)} %bias_ref.3) | copy-start | bytes 196
  39.1 75.6 %collective-permute-start.10 = (bf16[776,128]{1,0:T(8,128)(2,1)S(1)}, bf16[776,128]{1,0:T(8,128)(2,1)S(1)}, u32[]{:S(2)}, u32[]{:S(2)}) collective-permute-start(bf16[776,128]{1,0:T(8,128)(2,1)S(1)} %get-tuple-element.38), channel_id=1, source_target_pairs={{0,72},{8,64},{16,88},{24,80},{32,104},{40,96},{48,120},{56,112},{... | collective-permute-start | bytes 595976 | tf_op jit(solution)/shard_map/ppermute | solution.py:289
  55.7 66.4 %collective-permute-start.5 = (bf16[776,128]{1,0:T(8,128)(2,1)S(1)}, bf16[776,128]{1,0:T(8,128)(2,1)S(1)}, u32[]{:S(2)}, u32[]{:S(2)}) collective-permute-start(bf16[776,128]{1,0:T(8,128)(2,1)S(1)} %get-tuple-element.33), channel_id=1, source_target_pairs={{0,32},{8,40},{16,48},{24,56},{32,64},{40,72},{48,80},{56,88},{64,... | collective-permute-start | bytes 595976 | tf_op jit(solution)/shard_map/ppermute | solution.py:289
  61.8 64.4 %collective-permute-start.6 = (bf16[776,128]{1,0:T(8,128)(2,1)S(1)}, bf16[776,128]{1,0:T(8,128)(2,1)S(1)}, u32[]{:S(2)}, u32[]{:S(2)}) collective-permute-start(bf16[776,128]{1,0:T(8,128)(2,1)S(1)} %get-tuple-element.34), channel_id=1, source_target_pairs={{0,104},{8,96},{16,120},{24,112},{32,8},{40,0},{48,24},{56,16},{64... | collective-permute-start | bytes 595976 | tf_op jit(solution)/shard_map/ppermute | solution.py:289
  88.9 37.5 %collective-permute-start.7 = (bf16[776,128]{1,0:T(8,128)(2,1)S(1)}, bf16[776,128]{1,0:T(8,128)(2,1)S(1)}, u32[]{:S(2)}, u32[]{:S(2)}) collective-permute-start(bf16[776,128]{1,0:T(8,128)(2,1)S(1)} %get-tuple-element.35), channel_id=1, source_target_pairs={{0,48},{8,56},{16,32},{24,40},{32,80},{40,88},{48,64},{56,72},{64,... | collective-permute-start | bytes 595976 | tf_op jit(solution)/shard_map/ppermute | solution.py:289
  93.9 57.2 %collective-permute-start.8 = (bf16[776,128]{1,0:T(8,128)(2,1)S(1)}, bf16[776,128]{1,0:T(8,128)(2,1)S(1)}, u32[]{:S(2)}, u32[]{:S(2)}) collective-permute-start(bf16[776,128]{1,0:T(8,128)(2,1)S(1)} %get-tuple-element.36), channel_id=1, source_target_pairs={{0,96},{8,104},{16,112},{24,120},{32,0},{40,8},{48,16},{56,24},{64... | collective-permute-start | bytes 595976 | tf_op jit(solution)/shard_map/ppermute | solution.py:289
  114.7 36.4 %collective-permute-start.11 = (bf16[776,128]{1,0:T(8,128)(2,1)S(1)}, bf16[776,128]{1,0:T(8,128)(2,1)S(1)}, u32[]{:S(2)}, u32[]{:S(2)}) collective-permute-start(bf16[776,128]{1,0:T(8,128)(2,1)S(1)} %get-tuple-element.39), channel_id=1, source_target_pairs={{0,56},{8,48},{16,40},{24,32},{32,88},{40,80},{48,72},{56,64},{64,... | collective-permute-start | bytes 595976 | tf_op jit(solution)/shard_map/ppermute | solution.py:289
  122.1 39.6 %collective-permute-start.12 = (bf16[776,128]{1,0:T(8,128)(2,1)S(1)}, bf16[776,128]{1,0:T(8,128)(2,1)S(1)}, u32[]{:S(2)}, u32[]{:S(2)}) collective-permute-start(bf16[776,128]{1,0:T(8,128)(2,1)S(1)} %get-tuple-element.40), channel_id=1, source_target_pairs={{0,112},{8,120},{16,96},{24,104},{32,16},{40,24},{48,0},{56,8},{64... | collective-permute-start | bytes 595976 | tf_op jit(solution)/shard_map/ppermute | solution.py:289
  126.2 48.7 %collective-permute-start.13 = (bf16[776,128]{1,0:T(8,128)(2,1)S(1)}, bf16[776,128]{1,0:T(8,128)(2,1)S(1)}, u32[]{:S(2)}, u32[]{:S(2)}) collective-permute-start(bf16[776,128]{1,0:T(8,128)(2,1)S(1)} %get-tuple-element.41), channel_id=1, source_target_pairs={{0,40},{8,32},{16,56},{24,48},{32,72},{40,64},{48,88},{56,80},{64,... | collective-permute-start | bytes 595976 | tf_op jit(solution)/shard_map/ppermute | solution.py:289
  126.5 48.5 %collective-permute-start.14 = (bf16[776,128]{1,0:T(8,128)(2,1)S(1)}, bf16[776,128]{1,0:T(8,128)(2,1)S(1)}, u32[]{:S(2)}, u32[]{:S(2)}) collective-permute-start(bf16[776,128]{1,0:T(8,128)(2,1)S(1)} %get-tuple-element.42), channel_id=1, source_target_pairs={{0,120},{8,112},{16,104},{24,96},{32,24},{40,16},{48,8},{56,0},{64... | collective-permute-start | bytes 595976 | tf_op jit(solution)/shard_map/ppermute | solution.py:289
  151.1 27.4 %collective-permute-start = (bf16[776,128]{1,0:T(8,128)(2,1)S(1)}, bf16[776,128]{1,0:T(8,128)(2,1)S(1)}, u32[]{:S(2)}, u32[]{:S(2)}) collective-permute-start(bf16[776,128]{1,0:T(8,128)(2,1)S(1)} %get-tuple-element.26), channel_id=1, source_target_pairs={{0,16},{8,24},{16,0},{24,8},{32,48},{40,56},{48,32},{56,40},{64,80... | collective-permute-start | bytes 595976 | tf_op jit(solution)/shard_map/ppermute | solution.py:289
  151.1 27.4 %collective-permute-start.1 = (bf16[776,128]{1,0:T(8,128)(2,1)S(1)}, bf16[776,128]{1,0:T(8,128)(2,1)S(1)}, u32[]{:S(2)}, u32[]{:S(2)}) collective-permute-start(bf16[776,128]{1,0:T(8,128)(2,1)S(1)} %get-tuple-element.27), channel_id=1, source_target_pairs={{0,24},{8,16},{16,8},{24,0},{32,56},{40,48},{48,40},{56,32},{64,88... | collective-permute-start | bytes 595976 | tf_op jit(solution)/shard_map/ppermute | solution.py:289
  161.7 16.8 %collective-permute-start.2 = (bf16[776,128]{1,0:T(8,128)(2,1)S(1)}, bf16[776,128]{1,0:T(8,128)(2,1)S(1)}, u32[]{:S(2)}, u32[]{:S(2)}) collective-permute-start(bf16[776,128]{1,0:T(8,128)(2,1)S(1)} %get-tuple-element.28), channel_id=1, source_target_pairs={{0,8},{8,0},{16,24},{24,16},{32,40},{40,32},{48,56},{56,48},{64,72... | collective-permute-start | bytes 595976 | tf_op jit(solution)/shard_map/ppermute | solution.py:289

commit v6 on v5

--- a/solution.py
+++ b/solution.py
@@ -25,7 +25,7 @@
     + ((0, 2), (0, 3), (0, 1))
 )
 LEAD = (2,)
-FOLLOW = (1, 3, 0)
+FOLLOW = (((1, 3), 1), ((0,), 9))
 CHUNKS = 3
 STEP = 16
 LATE = 3
@@ -283,7 +283,8 @@
     args = (input_gain, key_weight, value_weight, stick_offsets)
     made, normed = project(LEAD, ORDER[0][1:], layer_input, *args, keep=True)
     made.update(project(LEAD, tuple(k for k in range(KVH) if k != ORDER[0][1]), normed, *args)[0])
-    made.update(project(FOLLOW, tuple(range(KVH)), layer_input, *args)[0])
+    for classes, _ in FOLLOW:
+        made.update(project(classes, tuple(range(KVH)), layer_input, *args)[0])
     got = {(0, 0): made[0, 0]}
     for c, k in ORDER:
         got[c, k] = lax.ppermute(made[c, k], "sp", pairs(c, k))

time: 184 us -> 189 us (1.027); the launches traced: 181 us -> 189 us
  starting transfers between devices: 99.1 us -> 134 us
  waiting for transfers between devices: 53.2 us -> 22.3 us
  Pallas kernels: 28.1 us -> 31.5 us
    ppermute x15, starting transfers between devices: 99.1 us -> 134 us  [shards(): got[c, k] = lax.ppermute(made[c, k], 'sp', pairs(c, k))]
    ppermute x15, waiting for transfers between devices: 53.2 us -> 22.3 us  [shards(): got[c, k] = lax.ppermute(made[c, k], 'sp', pairs(c, k))]
    pallas_call x3 -> x4, Pallas kernels: 22 us -> 25.4 us  [project(): pl.pallas_call(functools.partial(project_kernel, classes, heads, given, k...]
  transfers between devices with their start and end apart: 15 -> 15, of which waited for: 5 -> 2; matrix products, arithmetic and copies ran while one was open for 0% -> 0% of each run, Pallas kernels for 13% -> 10%
where the time goes in v6:
time: 189 us
  starting transfers between devices  134 us (71%)
  Pallas kernels  31.5 us (17%)
  waiting for transfers between devices  22.3 us (12%)
    ppermute x15, starting transfers between devices, shards(): got[c, k] = lax.ppermute(made[c, k], 'sp', pairs(c, k))  134 us
    pallas_call x4, Pallas kernels, project(): pl.pallas_call(functools.partial(project_kernel, classes, heads, given, k...  25.4 us
    ppermute x15, waiting for transfers between devices, shards(): got[c, k] = lax.ppermute(made[c, k], 'sp', pairs(c, k))  22.3 us
    pallas_call x2, Pallas kernels, read(): pl.pallas_call(functools.partial(read_kernel, pieces, final), out_shape=c...  6.07 us
  transfers between devices with their start and end apart: 15, of which 2 were waited for; matrix products, arithmetic and copies ran while one was open for 0% of the time, Pallas kernels for 10%

profile of v6, /device:TPU:36, one launch (start us, length us, event | category | flops | bytes accessed | tf_op | source)
XLA Modules:
  0.0 188.6 jit_solution(2671514958928403343)
XLA Ops:
  0.6 11.0 %project.7 = (bf16[776,128]{1,0:T(8,128)(2,1)S(1)}, bf16[776,128]{1,0:T(8,128)(2,1)S(1)}, bf16[776,128]{1,0:T(8,128)(2,1)S(1)}, bf16[776,128]{1,0:T(8,128)(2,1)S...) custom-call(bf16[4,384,2048]{2,1,0:T(8,128)(2,1)} %x_ref.5, ...), custom_call_target="tpu_custom_call" | custom-call | flops 3221225472 | bytes 7340032 | tf_op jit(solution)/shard_map/project/pallas_call | solution.py:138
  11.6 10.7 %collective-permute-start.5 = (bf16[776,128]{1,0:T(8,128)(2,1)S(1)}, bf16[776,128]{1,0:T(8,128)(2,1)S(1)}, u32[]{:S(2)}, u32[]{:S(2)}) collective-permute-start(bf16[776,128]{1,0:T(8,128)(2,1)S(1)} %get-tuple-element.33), channel_id=1, source_target_pairs={{0,32},{8,40},{16,48},{24,56},{32,64},{40,72},{48,80},{56,88},{64,... | collective-permute-start | bytes 595976 | tf_op jit(solution)/shard_map/ppermute | solution.py:290
  22.4 11.1 %collective-permute-start.6 = (bf16[776,128]{1,0:T(8,128)(2,1)S(1)}, bf16[776,128]{1,0:T(8,128)(2,1)S(1)}, u32[]{:S(2)}, u32[]{:S(2)}) collective-permute-start(bf16[776,128]{1,0:T(8,128)(2,1)S(1)} %get-tuple-element.34), channel_id=1, source_target_pairs={{0,104},{8,96},{16,120},{24,112},{32,8},{40,0},{48,24},{56,16},{64... | collective-permute-start | bytes 595976 | tf_op jit(solution)/shard_map/ppermute | solution.py:290
  33.4 2.2 %collective-permute-start.7 = (bf16[776,128]{1,0:T(8,128)(2,1)S(1)}, bf16[776,128]{1,0:T(8,128)(2,1)S(1)}, u32[]{:S(2)}, u32[]{:S(2)}) collective-permute-start(bf16[776,128]{1,0:T(8,128)(2,1)S(1)} %get-tuple-element.35), channel_id=1, source_target_pairs={{0,48},{8,56},{16,32},{24,40},{32,80},{40,88},{48,64},{56,72},{64,... | collective-permute-start | bytes 595976 | tf_op jit(solution)/shard_map/ppermute | solution.py:290
  35.6 6.4 %collective-permute-start.8 = (bf16[776,128]{1,0:T(8,128)(2,1)S(1)}, bf16[776,128]{1,0:T(8,128)(2,1)S(1)}, u32[]{:S(2)}, u32[]{:S(2)}) collective-permute-start(bf16[776,128]{1,0:T(8,128)(2,1)S(1)} %get-tuple-element.36), channel_id=1, source_target_pairs={{0,96},{8,104},{16,112},{24,120},{32,0},{40,8},{48,16},{56,24},{64... | collective-permute-start | bytes 595976 | tf_op jit(solution)/shard_map/ppermute | solution.py:290
  42.0 0.5 collective-permute-start.11
  42.5 0.0 collective-permute-done.5.rest_3_
  42.5 25.2 %collective-permute-start.12 = (bf16[776,128]{1,0:T(8,128)(2,1)S(1)}, bf16[776,128]{1,0:T(8,128)(2,1)S(1)}, u32[]{:S(2)}, u32[]{:S(2)}) collective-permute-start(bf16[776,128]{1,0:T(8,128)(2,1)S(1)} %get-tuple-element.40), channel_id=1, source_target_pairs={{0,112},{8,120},{16,96},{24,104},{32,16},{40,24},{48,0},{56,8},{64... | collective-permute-start | bytes 595976 | tf_op jit(solution)/shard_map/ppermute | solution.py:290
  67.7 0.0 collective-permute-done.6.rest_4_
  67.7 0.0 collective-permute-start.13
  67.7 2.9 %project.5 = (bf16[776,128]{1,0:T(8,128)(2,1)S(1)}, bf16[384,2048]{1,0:T(8,128)(2,1)S(1)}) custom-call(bf16[4,384,2048]{2,1,0:T(8,128)(2,1)} %x_ref.5, f32[2048]{0:T(1024)} %gain_ref.7, bf16[2048,512]{1,0:T(8,128)(2,1)} %key_ref.7, bf16[2048,512]{1,0:T(8,128)(2,1)} %value_ref.7, bf16[4,4,384]{2,1,0:T(4,128)(2,1)} %offset_ref.7), custom_call_target="tpu_custom_call" | custom-call | flops 402653184 | bytes 2621440 | tf_op jit(solution)/shard_map/project/pallas_call | solution.py:138
  70.6 4.4 %project.6 = (bf16[776,128]{1,0:T(8,128)(2,1)S(1)}, bf16[776,128]{1,0:T(8,128)(2,1)S(1)}, bf16[776,128]{1,0:T(8,128)(2,1)S(1)}) custom-call(bf16[384,2048]{1,0:T(8,128)(2,1)S(1)} %get-tuple-element.31.x_ref, f32[2048]{0:T(1024)} %gain_ref.7, bf16[2048,512]{1,0:T(8,128)(2,1)} %key_ref.7, bf16[2048,512]{1,0:T(8,128)(2,1)} %value_ref.7, ...), custom_call_target="tpu_custom_call" | custom-call | flops 1207959552 | bytes 4718592 | tf_op jit(solution)/shard_map/project/pallas_call | solution.py:138
  75.0 0.0 collective-permute-done.7.rest_5_
  75.0 0.1 collective-permute-start.14
  75.1 0.0 collective-permute-done.8.rest_6_
  75.1 10.1 %collective-permute-start.3 = (bf16[776,128]{1,0:T(8,128)(2,1)S(1)}, bf16[776,128]{1,0:T(8,128)(2,1)S(1)}, u32[]{:S(2)}, u32[]{:S(2)}) collective-permute-start(bf16[776,128]{1,0:T(8,128)(2,1)S(1)} %get-tuple-element.30), channel_id=1, source_target_pairs={{0,64},{8,72},{16,80},{24,88},{32,96},{40,104},{48,112},{56,120},{... | collective-permute-start | bytes 595976 | tf_op jit(solution)/shard_map/ppermute | solution.py:290
  85.2 3.1 %collective-permute-done.11.rest_9_ = bf16[776,128]{1,0:T(8,128)(2,1)S(1)} collective-permute-done((bf16[776,128]{1,0:T(8,128)(2,1)S(1)}, bf16[776,128]{1,0:T(8,128)(2,1)S(1)}, u32[]{:S(2)}, u32[]{:S(2)}) %collective-permute-start.11) | collective-permute-done | bytes 198688 | tf_op jit(solution)/shard_map/ppermute | solution.py:290
  88.3 16.7 %collective-permute-start.4 = (bf16[776,128]{1,0:T(8,128)(2,1)S(1)}, bf16[776,128]{1,0:T(8,128)(2,1)S(1)}, u32[]{:S(2)}, u32[]{:S(2)}) collective-permute-start(bf16[776,128]{1,0:T(8,128)(2,1)S(1)} %get-tuple-element.32), channel_id=1, source_target_pairs={{0,88},{8,80},{16,72},{24,64},{32,120},{40,112},{48,104},{56,96},{... | collective-permute-start | bytes 595976 | tf_op jit(solution)/shard_map/ppermute | solution.py:290
  105.0 0.0 collective-permute-done.12.rest_10_
  105.0 4.5 %collective-permute-start.9 = (bf16[776,128]{1,0:T(8,128)(2,1)S(1)}, bf16[776,128]{1,0:T(8,128)(2,1)S(1)}, u32[]{:S(2)}, u32[]{:S(2)}) collective-permute-start(bf16[776,128]{1,0:T(8,128)(2,1)S(1)} %get-tuple-element.37), channel_id=1, source_target_pairs={{0,80},{8,88},{16,64},{24,72},{32,112},{40,120},{48,96},{56,104},{... | collective-permute-start | bytes 595976 | tf_op jit(solution)/shard_map/ppermute | solution.py:290
  109.5 0.0 collective-permute-done.13.rest_11_
  109.5 0.0 copy-start
  109.5 0.0 copy-start.1
  109.5 29.1 %collective-permute-start.10 = (bf16[776,128]{1,0:T(8,128)(2,1)S(1)}, bf16[776,128]{1,0:T(8,128)(2,1)S(1)}, u32[]{:S(2)}, u32[]{:S(2)}) collective-permute-start(bf16[776,128]{1,0:T(8,128)(2,1)S(1)} %get-tuple-element.38), channel_id=1, source_target_pairs={{0,72},{8,64},{16,88},{24,80},{32,104},{40,96},{48,120},{56,112},{... | collective-permute-start | bytes 595976 | tf_op jit(solution)/shard_map/ppermute | solution.py:290
  138.6 7.2 %project.4 = (bf16[776,128]{1,0:T(8,128)(2,1)S(1)}, bf16[776,128]{1,0:T(8,128)(2,1)S(1)}, bf16[776,128]{1,0:T(8,128)(2,1)S(1)}, bf16[776,128]{1,0:T(8,128)(2,1)S(1)}) custom-call(bf16[4,384,2048]{2,1,0:T(8,128)(2,1)} %x_ref.5, f32[2048]{0:T(1024)} %gain_ref.7, bf16[2048,512]{1,0:T(8,128)(2,1)} %key_ref.7, bf16[2048,512]{1,0:T(8,128)(2,1)} %value_ref.7, ...), custom_call_target="tpu_custom_call" | custom-call | flops 1610612736 | bytes 5767168 | tf_op jit(solution)/shard_map/project/pallas_call | solution.py:138
  145.8 0.0 collective-permute-done.14.rest_12_
  145.8 10.6 %collective-permute-start = (bf16[776,128]{1,0:T(8,128)(2,1)S(1)}, bf16[776,128]{1,0:T(8,128)(2,1)S(1)}, u32[]{:S(2)}, u32[]{:S(2)}) collective-permute-start(bf16[776,128]{1,0:T(8,128)(2,1)S(1)} %get-tuple-element.26), channel_id=1, source_target_pairs={{0,16},{8,24},{16,0},{24,8},{32,48},{40,56},{48,32},{56,40},{64,80... | collective-permute-start | bytes 595976 | tf_op jit(solution)/shard_map/ppermute | solution.py:290
  156.4 0.0 collective-permute-done.3.rest_1_
  156.4 6.8 %collective-permute-start.1 = (bf16[776,128]{1,0:T(8,128)(2,1)S(1)}, bf16[776,128]{1,0:T(8,128)(2,1)S(1)}, u32[]{:S(2)}, u32[]{:S(2)}) collective-permute-start(bf16[776,128]{1,0:T(8,128)(2,1)S(1)} %get-tuple-element.27), channel_id=1, source_target_pairs={{0,24},{8,16},{16,8},{24,0},{32,56},{40,48},{48,40},{56,32},{64,88... | collective-permute-start | bytes 595976 | tf_op jit(solution)/shard_map/ppermute | solution.py:290
  163.2 0.0 collective-permute-done.4.rest_2_
  163.2 0.0 collective-permute-start.2
  163.2 0.0 collective-permute-done.9.rest_7_
  163.2 19.1 %collective-permute-done.10.rest_8_ = bf16[776,128]{1,0:T(8,128)(2,1)S(1)} collective-permute-done((bf16[776,128]{1,0:T(8,128)(2,1)S(1)}, bf16[776,128]{1,0:T(8,128)(2,1)S(1)}, u32[]{:S(2)}, u32[]{:S(2)}) %collective-permute-start.10) | collective-permute-done | bytes 198688 | tf_op jit(solution)/shard_map/ppermute | solution.py:290
  182.3 0.0 copy-done
  182.3 0.0 copy-done.1
  182.3 3.5 %read.2 = (bf16[1,1,6144,128]{3,2,1,0:T(8,128)(2,1)}, bf16[1,1,6144,128]{3,2,1,0:T(8,128)(2,1)}, f32[16,8,128]{2,1,0:T(8,128)S(1)}, f32[16,8,128]{2,1,0:T(8,128)S(1)}, f32[16,1,384]{2,1,0:T(1,128)S(1)}) custom-call(bf16[1,1,512]{2,1,0:T(2,128)(2,1)S(1)} %copy-done, f32[16]{0:T(128)S(1)} %copy-done.1, bf16[776,128]{1,0:T(8,128)(2,1)S(1)} %get-tuple-element.29.rest_0_, ...), custom_call_target="tpu_custom_call" | custom-call | flops 40894464 | bytes 5111808 | tf_op jit(solution)/shard_map/read/pallas_call | solution.py:256
  185.9 0.0 collective-permute-done.rest_0_
  185.9 0.0 collective-permute-done.1.rest_1_
  185.9 0.0 collective-permute-done.2.rest_2_
  185.9 2.5 %read.3 = (bf16[1,1,6144,128]{3,2,1,0:T(8,128)(2,1)}, bf16[1,1,6144,128]{3,2,1,0:T(8,128)(2,1)}, bf16[1,1,6144]{2,1,0:T(2,128)(2,1)}, bf16[1,1,512]{2,1,0:T(2,128)(2,1)}) custom-call(bf16[1,1,512]{2,1,0:T(2,128)(2,1)S(1)} %copy-done, f32[16]{0:T(128)S(1)} %copy-done.1, ...), custom_call_target="tpu_custom_call", output_to_operand_aliasing={{0}: (8, {}), {1}: (9, {})} | custom-call | flops 9437184 | bytes 1179648 | tf_op jit(solution)/shard_map/read/pallas_call | solution.py:256
Async XLA Ops:
  11.6 30.9 %collective-permute-start.5 = (bf16[776,128]{1,0:T(8,128)(2,1)S(1)}, bf16[776,128]{1,0:T(8,128)(2,1)S(1)}, u32[]{:S(2)}, u32[]{:S(2)}) collective-permute-start(bf16[776,128]{1,0:T(8,128)(2,1)S(1)} %get-tuple-element.33), channel_id=1, source_target_pairs={{0,32},{8,40},{16,48},{24,56},{32,64},{40,72},{48,80},{56,88},{64,... | collective-permute-start | bytes 595976 | tf_op jit(solution)/shard_map/ppermute | solution.py:290
  22.4 45.3 %collective-permute-start.6 = (bf16[776,128]{1,0:T(8,128)(2,1)S(1)}, bf16[776,128]{1,0:T(8,128)(2,1)S(1)}, u32[]{:S(2)}, u32[]{:S(2)}) collective-permute-start(bf16[776,128]{1,0:T(8,128)(2,1)S(1)} %get-tuple-element.34), channel_id=1, source_target_pairs={{0,104},{8,96},{16,120},{24,112},{32,8},{40,0},{48,24},{56,16},{64... | collective-permute-start | bytes 595976 | tf_op jit(solution)/shard_map/ppermute | solution.py:290
  33.4 41.5 %collective-permute-start.7 = (bf16[776,128]{1,0:T(8,128)(2,1)S(1)}, bf16[776,128]{1,0:T(8,128)(2,1)S(1)}, u32[]{:S(2)}, u32[]{:S(2)}) collective-permute-start(bf16[776,128]{1,0:T(8,128)(2,1)S(1)} %get-tuple-element.35), channel_id=1, source_target_pairs={{0,48},{8,56},{16,32},{24,40},{32,80},{40,88},{48,64},{56,72},{64,... | collective-permute-start | bytes 595976 | tf_op jit(solution)/shard_map/ppermute | solution.py:290
  35.6 39.5 %collective-permute-start.8 = (bf16[776,128]{1,0:T(8,128)(2,1)S(1)}, bf16[776,128]{1,0:T(8,128)(2,1)S(1)}, u32[]{:S(2)}, u32[]{:S(2)}) collective-permute-start(bf16[776,128]{1,0:T(8,128)(2,1)S(1)} %get-tuple-element.36), channel_id=1, source_target_pairs={{0,96},{8,104},{16,112},{24,120},{32,0},{40,8},{48,16},{56,24},{64... | collective-permute-start | bytes 595976 | tf_op jit(solution)/shard_map/ppermute | solution.py:290
  42.0 46.3 %collective-permute-start.11 = (bf16[776,128]{1,0:T(8,128)(2,1)S(1)}, bf16[776,128]{1,0:T(8,128)(2,1)S(1)}, u32[]{:S(2)}, u32[]{:S(2)}) collective-permute-start(bf16[776,128]{1,0:T(8,128)(2,1)S(1)} %get-tuple-element.39), channel_id=1, source_target_pairs={{0,56},{8,48},{16,40},{24,32},{32,88},{40,80},{48,72},{56,64},{64,... | collective-permute-start | bytes 595976 | tf_op jit(solution)/shard_map/ppermute | solution.py:290
  42.5 62.5 %collective-permute-start.12 = (bf16[776,128]{1,0:T(8,128)(2,1)S(1)}, bf16[776,128]{1,0:T(8,128)(2,1)S(1)}, u32[]{:S(2)}, u32[]{:S(2)}) collective-permute-start(bf16[776,128]{1,0:T(8,128)(2,1)S(1)} %get-tuple-element.40), channel_id=1, source_target_pairs={{0,112},{8,120},{16,96},{24,104},{32,16},{40,24},{48,0},{56,8},{64... | collective-permute-start | bytes 595976 | tf_op jit(solution)/shard_map/ppermute | solution.py:290
  67.7 41.8 %collective-permute-start.13 = (bf16[776,128]{1,0:T(8,128)(2,1)S(1)}, bf16[776,128]{1,0:T(8,128)(2,1)S(1)}, u32[]{:S(2)}, u32[]{:S(2)}) collective-permute-start(bf16[776,128]{1,0:T(8,128)(2,1)S(1)} %get-tuple-element.41), channel_id=1, source_target_pairs={{0,40},{8,32},{16,56},{24,48},{32,72},{40,64},{48,88},{56,80},{64,... | collective-permute-start | bytes 595976 | tf_op jit(solution)/shard_map/ppermute | solution.py:290
  75.0 70.8 %collective-permute-start.14 = (bf16[776,128]{1,0:T(8,128)(2,1)S(1)}, bf16[776,128]{1,0:T(8,128)(2,1)S(1)}, u32[]{:S(2)}, u32[]{:S(2)}) collective-permute-start(bf16[776,128]{1,0:T(8,128)(2,1)S(1)} %get-tuple-element.42), channel_id=1, source_target_pairs={{0,120},{8,112},{16,104},{24,96},{32,24},{40,16},{48,8},{56,0},{64... | collective-permute-start | bytes 595976 | tf_op jit(solution)/shard_map/ppermute | solution.py:290
  75.1 81.3 %collective-permute-start.3 = (bf16[776,128]{1,0:T(8,128)(2,1)S(1)}, bf16[776,128]{1,0:T(8,128)(2,1)S(1)}, u32[]{:S(2)}, u32[]{:S(2)}) collective-permute-start(bf16[776,128]{1,0:T(8,128)(2,1)S(1)} %get-tuple-element.30), channel_id=1, source_target_pairs={{0,64},{8,72},{16,80},{24,88},{32,96},{40,104},{48,112},{56,120},{... | collective-permute-start | bytes 595976 | tf_op jit(solution)/shard_map/ppermute | solution.py:290
  88.3 74.9 %collective-permute-start.4 = (bf16[776,128]{1,0:T(8,128)(2,1)S(1)}, bf16[776,128]{1,0:T(8,128)(2,1)S(1)}, u32[]{:S(2)}, u32[]{:S(2)}) collective-permute-start(bf16[776,128]{1,0:T(8,128)(2,1)S(1)} %get-tuple-element.32), channel_id=1, source_target_pairs={{0,88},{8,80},{16,72},{24,64},{32,120},{40,112},{48,104},{56,96},{... | collective-permute-start | bytes 595976 | tf_op jit(solution)/shard_map/ppermute | solution.py:290
  105.0 58.2 %collective-permute-start.9 = (bf16[776,128]{1,0:T(8,128)(2,1)S(1)}, bf16[776,128]{1,0:T(8,128)(2,1)S(1)}, u32[]{:S(2)}, u32[]{:S(2)}) collective-permute-start(bf16[776,128]{1,0:T(8,128)(2,1)S(1)} %get-tuple-element.37), channel_id=1, source_target_pairs={{0,80},{8,88},{16,64},{24,72},{32,112},{40,120},{48,96},{56,104},{... | collective-permute-start | bytes 595976 | tf_op jit(solution)/shard_map/ppermute | solution.py:290
  109.5 72.8 %copy-start = (bf16[1,1,512]{2,1,0:T(2,128)(2,1)S(1)}, bf16[1,1,512]{2,1,0:T(2,128)(2,1)}, u32[]{:S(2)}) copy-start(bf16[1,1,512]{2,1,0:T(2,128)(2,1)} %q_ref.3) | copy-start | bytes 3076
  109.5 72.8 %copy-start.1 = (f32[16]{0:T(128)S(1)}, f32[16]{0:T(128)}, u32[]{:S(2)}) copy-start(f32[16]{0:T(128)} %bias_ref.3) | copy-start | bytes 196
  109.5 72.8 %collective-permute-start.10 = (bf16[776,128]{1,0:T(8,128)(2,1)S(1)}, bf16[776,128]{1,0:T(8,128)(2,1)S(1)}, u32[]{:S(2)}, u32[]{:S(2)}) collective-permute-start(bf16[776,128]{1,0:T(8,128)(2,1)S(1)} %get-tuple-element.38), channel_id=1, source_target_pairs={{0,72},{8,64},{16,88},{24,80},{32,104},{40,96},{48,120},{56,112},{... | collective-permute-start | bytes 595976 | tf_op jit(solution)/shard_map/ppermute | solution.py:290
  145.8 40.1 %collective-permute-start = (bf16[776,128]{1,0:T(8,128)(2,1)S(1)}, bf16[776,128]{1,0:T(8,128)(2,1)S(1)}, u32[]{:S(2)}, u32[]{:S(2)}) collective-permute-start(bf16[776,128]{1,0:T(8,128)(2,1)S(1)} %get-tuple-element.26), channel_id=1, source_target_pairs={{0,16},{8,24},{16,0},{24,8},{32,48},{40,56},{48,32},{56,40},{64,80... | collective-permute-start | bytes 595976 | tf_op jit(solution)/shard_map/ppermute | solution.py:290
  156.4 29.5 %collective-permute-start.1 = (bf16[776,128]{1,0:T(8,128)(2,1)S(1)}, bf16[776,128]{1,0:T(8,128)(2,1)S(1)}, u32[]{:S(2)}, u32[]{:S(2)}) collective-permute-start(bf16[776,128]{1,0:T(8,128)(2,1)S(1)} %get-tuple-element.27), channel_id=1, source_target_pairs={{0,24},{8,16},{16,8},{24,0},{32,56},{40,48},{48,40},{56,32},{64,88... | collective-permute-start | bytes 595976 | tf_op jit(solution)/shard_map/ppermute | solution.py:290
  163.2 22.7 %collective-permute-start.2 = (bf16[776,128]{1,0:T(8,128)(2,1)S(1)}, bf16[776,128]{1,0:T(8,128)(2,1)S(1)}, u32[]{:S(2)}, u32[]{:S(2)}) collective-permute-start(bf16[776,128]{1,0:T(8,128)(2,1)S(1)} %get-tuple-element.28), channel_id=1, source_target_pairs={{0,8},{8,0},{16,24},{24,16},{32,40},{40,32},{48,56},{56,48},{64,72... | collective-permute-start | bytes 595976 | tf_op jit(solution)/shard_map/ppermute | solution.py:290
